TPU v7x, 256 devices: a 4x2x16 block of a 4x16x16 slice. The times are simulated.
256 devices in a mesh: grp: 2 (over y), fs: 16 (over z), tp: 8 (over x, core).
Axes of the slice: x: 4, y: 2, z: 16, core: 2. Of those that a mesh axis runs over, the one named last changes fastest.
The devices are a block of a 4x16x16 slice.
Arguments:
- tokens: bfloat16 [24576, 2048], P(('grp', 'fs'), 'tp'), parts along dimension 0, may hold values from -6 to 6
- mix_gain: float32 [2048], replicated, may hold values from 0.1 to 1.9
- w_u: float32 [2048, 1024], P('fs', 'tp'), may hold values from -0.125 to 0.125
- w_v: float32 [2048, 1024], P('fs', 'tp'), may hold values from -0.125 to 0.125
- u_scale: float32 [1024], P('tp'), may hold values from 0.5 to 2
- v_scale: float32 [1024], P('tp'), may hold values from 0.5 to 2
- spatial: bfloat16 [8, 128, 128], P('tp'), may hold values from -0.5 to 0.5
- spatial_bias: float32 [8, 128], P('tp'), may hold values from 0.1 to 1.9
- w_mix: float32 [1024, 2048], P('tp', 'fs'), may hold values from -0.1875 to 0.1875
- mix_scale: float32 [1, 2048], P(None, 'fs'), may hold values from 0.5 to 2
- ffn_gain: float32 [2048], replicated, may hold values from 0.1 to 1.9
- w_gate: float32 [2048, 5632], P('fs', 'tp'), may hold values from -0.125 to 0.125
- w_up: float32 [2048, 5632], P('fs', 'tp'), may hold values from -0.125 to 0.125
- gate_scale: float32 [5632], P('tp'), may hold values from 0.5 to 2
- up_scale: float32 [5632], P('tp'), may hold values from 0.5 to 2
- w_down: float32 [5632, 2048], P('tp', 'fs'), may hold values from -0.078125 to 0.078125
- down_scale: float32 [1, 2048], P(None, 'fs'), may hold values from 0.5 to 2
Outputs:
- layer_out: bfloat16 [24576, 2048], P(('grp', 'fs'), 'tp'), parts along dimension 0
There are 2 independent parts, one for each index of `grp`. A program takes and returns all parts, laid end to end along the dimension named above; an argument that names none is the same for every part. Nothing has to cross between parts.
All inputs are finite; a program needn't handle non-finite values.
Results may differ from a plain program's by a relative error of at most 0.024.
Values may be sent and summed in bfloat16 or wider, within the bound.
No kernel may reach another device: no remote copies, remote signals or barrier semaphores. Data moves between devices by JAX's collectives and lax.ppermute only.
A program may use at most 128 MiB of HBM per device.

v0:
```python
import functools

import jax
import jax.numpy as jnp
from jax import lax
from jax.experimental import pallas as pl
from jax.experimental.pallas import tpu as pltpu
from jax.sharding import PartitionSpec as P

eps = 1e-06
CORES = 2


def swap_cores(x):
    count = lax.axis_size("tp")
    return lax.ppermute(x, "tp", [(i, i ^ 1) for i in range(count)])


def to_chip(x, step):
    count = lax.axis_size("tp")
    return lax.ppermute(x, "tp", [(i, (i + CORES * step) % count) for i in range(count)])


def gather_features(shard):
    chips = lax.axis_size("tp") // CORES
    got = [to_chip(shard, step) for step in range(1, chips)]
    near = swap_cores(jnp.stack([got[0], got[-1]]))
    swapped = [near[0], *[swap_cores(g) for g in got[1:-1]], near[1]]
    return [shard, swap_cores(shard), *[p for pair in zip(got, swapped) for p in pair]]


def chunk_order(me, count):
    chips = count // CORES
    chip, core = lax.div(me, CORES), lax.rem(me, CORES)
    order = []
    for step in range(chips):
        source = CORES * lax.rem(chip + chips - step, chips)
        order += [source + core, source + 1 - core]
    return order


def chip_sums(mine, theirs):
    other = swap_cores(theirs)
    chips = lax.axis_size("tp") // CORES
    pair = [mine[s].astype(jnp.float32) + other[s].astype(jnp.float32) for s in range(chips)]
    return [pair[0]] + [p.astype(jnp.bfloat16) for p in pair[1:]]


def sum_chips(pair):
    total = pair[0]
    for step, p in enumerate(pair[1:], 1):
        total = total + to_chip(p, step).astype(jnp.float32)
    return total


def dot_f32(a, b, dims=(((1,), (0,)), ((), ()))):
    return lax.dot_general(a, b, dims, preferred_element_type=jnp.float32)


def pass_on(x, step):
    count = lax.axis_size("fs")
    return lax.ppermute(x, "fs", [(i, (i + step) % count) for i in range(count)])


class Ring:
    def __init__(self, shard):
        self.count = lax.axis_size("fs")
        self.ahead = self.behind = shard
        self.held = [shard]
        self.before = [shard, shard]
        self.step = 0

    def after(self, *others):
        self.ahead, *_ = lax.optimization_barrier((self.ahead, *others))

    def advance(self):
        self.step += 1
        before, self.before = self.before, [self.ahead, self.behind]
        self.ahead, _ = lax.optimization_barrier((self.ahead, before[1]))
        self.behind, _ = lax.optimization_barrier((self.behind, before[0]))
        self.ahead = pass_on(self.ahead, 1)
        new = [self.ahead]
        if 2 * self.step < self.count:
            self.behind = pass_on(self.behind, -1)
            new.append(self.behind)
        self.held += new
        return new


def ring_order(me, count):
    order = [me]
    for step in range(1, count // 2 + 1):
        order.append(lax.rem(me + count - step, count))
        if 2 * step < count:
            order.append(lax.rem(me + step, count))
    return order


def lane_block(index, width):
    return pl.ds(pl.multiple_of(index * width, width), width)


def copy_all(pairs, sems, base):
    copies = [
        pltpu.make_async_copy(source, target, sems.at[base + i])
        for i, (source, target) in enumerate(pairs)
    ]
    for copy in copies:
        copy.start()

    def wait():
        for copy in copies:
            copy.wait()

    return wait, base + len(copies)


def load_rows(xs, buf, sems, base):
    width = xs[0].shape[1]
    places = chunk_order(lax.axis_index("tp"), len(xs))
    return copy_all(
        [(x, buf.at[:, lane_block(place, width)]) for x, place in zip(xs, places)], sems, base
    )


def row_factor(x):
    wide = x.astype(jnp.float32)
    return lax.rsqrt(jnp.mean(wide * wide, axis=1, keepdims=True) + eps)


def store_shares(value, weights, chunks, rows, mine_ref, theirs_ref):
    width = mine_ref.shape[2]
    chips = chunks // CORES
    me = lax.axis_index("tp")
    chip, core = lax.div(me, CORES), lax.rem(me, CORES)

    def fill(ref, which):
        def share(step, carry):
            target = CORES * lax.rem(chip + step, chips) + which
            w = weights(lane_block(target, width))
            ref[step, rows, :] = dot_f32(value, w).astype(jnp.bfloat16)
            return carry

        lax.fori_loop(0, chips, share, 0)

    fill(mine_ref, core)
    fill(theirs_ref, 1 - core)


def gating_kernel(*refs, chunks, shards, tall):
    xs, refs = refs[:chunks], refs[chunks:]
    near_ref, spatial_ref, bias_ref, mine_ref, theirs_ref, x_buf, in_buf, out_buf, sems = refs
    span = spatial_ref.shape[0]
    lanes = near_ref.shape[2] - 2 * span
    x_here, at = load_rows(xs, x_buf, sems, 0)
    in_here, at = copy_all([(near_ref.at[:, :, : 2 * span], in_buf)], sems, at)
    out_here, at = copy_all(
        [
            (near_ref.at[z, :, 2 * span :], out_buf.at[:, z * lanes : (z + 1) * lanes])
            for z in range(shards)
        ],
        sems,
        at,
    )
    later = lax.broadcasted_iota(jnp.int32, (span, span), 0)
    earlier = lax.broadcasted_iota(jnp.int32, (span, span), 1)
    bias = jnp.broadcast_to(bias_ref[...], (span, span)).T
    mixing = spatial_ref[...]
    mixing = jnp.where(later >= earlier, mixing, jnp.zeros_like(mixing))
    x_here()
    in_here()
    out_here()

    def block(i, carry):
        rows = pl.ds(pl.multiple_of(i * tall, tall), tall)
        x = x_buf[rows, :]
        weights = in_buf[...].reshape(x.shape[1], 2 * span)
        pre = dot_f32(x, weights) * row_factor(x)
        act = 0.5 * pre * (1.0 + lax.erf(pre * (0.5**0.5)))
        u = act[:, :span]
        v = act[:, span:].astype(jnp.bfloat16)
        gated = []
        for b in range(tall // span):
            at = slice(b * span, (b + 1) * span)
            placed = dot_f32(mixing, v[at]) + bias
            gated.append((u[at] * placed).astype(jnp.bfloat16))
        gated = jnp.concatenate(gated, axis=0)
        store_shares(gated, lambda at: out_buf[:, at], chunks, rows, mine_ref, theirs_ref)
        return carry

    lax.fori_loop(0, xs[0].shape[0] // tall, block, 0)


def channel_kernel(*refs, chunks, shards, tall):
    xs, refs = refs[:chunks], refs[chunks:]
    gate_scale_ref, up_scale_ref, refs = *refs[:2], refs[2:]
    ring, refs = refs[:shards], refs[shards:]
    mine_ref, theirs_ref, x_buf, gate_buf, up_buf, down_buf, sems = refs
    lanes = ring[0].shape[1]
    hidden = down_buf.shape[0]
    around = ring_order(lax.axis_index("fs"), shards)

    def load(part, buf, base):
        rows = slice(part * hidden, (part + 1) * hidden)
        return copy_all(
            [(w.at[rows, :], buf.at[:, lane_block(z, lanes)]) for z, w in zip(around, ring)],
            sems,
            base,
        )

    x_here, at = load_rows(xs, x_buf, sems, 0)
    gate_here, at = load(0, gate_buf, at)
    up_here, at = load(1, up_buf, at)
    down_here, at = load(2, down_buf, at)
    across = (((1,), (1,)), ((), ()))
    x_here()
    gate_here()
    up_here()
    down_here()

    def block(i, carry):
        rows = pl.ds(pl.multiple_of(i * tall, tall), tall)
        x = x_buf[rows, :]
        factor = row_factor(x)
        gate = dot_f32(x, gate_buf[...], across) * factor * gate_scale_ref[...][None, :]
        up = dot_f32(x, up_buf[...], across) * factor * up_scale_ref[...][None, :]
        act = (gate / (1.0 + jnp.exp(-gate)) * up).astype(jnp.bfloat16)
        store_shares(act, lambda at: down_buf[:, at], chunks, rows, mine_ref, theirs_ref)
        return carry

    lax.fori_loop(0, xs[0].shape[0] // tall, block, 0)


def gain_rows(gain_ref):
    row = gain_ref[pl.ds(lax.axis_index("fs"), 1), :]
    return jnp.broadcast_to(row, (row.shape[1], row.shape[1]))


def fold_kernel(
    in_gain_ref,
    u_ref,
    v_ref,
    mix_ref,
    u_scale_ref,
    v_scale_ref,
    mix_scale_ref,
    mid_gain_ref,
    gate_ref,
    up_ref,
    down_ref,
    down_scale_ref,
    near_ref,
    far_ref,
):
    gain = gain_rows(in_gain_ref).T
    parts = [
        u_ref[...] * gain * u_scale_ref[...],
        v_ref[...] * gain * v_scale_ref[...],
        mix_ref[...] * mix_scale_ref[...],
    ]
    at = 0
    for part in parts:
        near_ref[:, at : at + part.shape[1]] = part.astype(jnp.bfloat16)
        at += part.shape[1]
    gain = gain_rows(mid_gain_ref)[:1, :]
    hidden = gate_ref.shape[0]
    far_ref[:hidden, :] = (gate_ref[...] * gain).astype(jnp.bfloat16)
    far_ref[hidden : 2 * hidden, :] = (up_ref[...] * gain).astype(jnp.bfloat16)
    far_ref[2 * hidden :, :] = (down_ref[...] * down_scale_ref[...]).astype(jnp.bfloat16)


def fold(shapes, *operands):
    return pl.pallas_call(
        fold_kernel,
        grid=(1,),
        in_specs=[pl.BlockSpec(a.shape, lambda i: (0, 0)) for a in operands],
        out_specs=[pl.BlockSpec(memory_space=pltpu.VMEM)] * len(shapes),
        out_shape=[jax.ShapeDtypeStruct(shape, jnp.bfloat16) for shape in shapes],
        cost_estimate=pl.CostEstimate(flops=2**22, bytes_accessed=2**20, transcendentals=0),
        compiler_params=pltpu.CompilerParams(vmem_limit_bytes=60 * 2**20),
        name="fold",
    )(*operands)


def call(kernel, name, operands, specs, chunks, shards, tall, scratch, flops, limit):
    rows, width = operands[0].shape
    half = chunks // CORES
    vmem = pl.BlockSpec(memory_space=pltpu.VMEM)
    return pl.pallas_call(
        functools.partial(kernel, chunks=chunks, shards=shards, tall=tall),
        in_specs=[vmem if spec is None else spec for spec in specs],
        out_specs=[vmem, vmem],
        out_shape=[jax.ShapeDtypeStruct((half, rows, width), jnp.bfloat16)] * 2,
        scratch_shapes=[
            pltpu.VMEM(shape, jnp.bfloat16) if isinstance(shape, tuple) else shape
            for shape in scratch
        ],
        compiler_params=pltpu.CompilerParams(vmem_limit_bytes=limit * 2**20),
        cost_estimate=pl.CostEstimate(flops=flops, bytes_accessed=2**20, transcendentals=0),
        name=name,
    )(*operands)


def gating(pieces, near, spatial, bias):
    chunks, shards, tall = len(pieces), near.shape[0], 256
    rows, width = pieces[0].shape
    span = spatial.shape[0]
    model = chunks * width
    flops = 2 * rows * (model * 2 * span + span * span + span * model)
    scratch = [
        (rows, model),
        (shards, model // shards, 2 * span),
        (span, model),
        pltpu.SemaphoreType.DMA((chunks + 1 + shards,)),
    ]
    operands = [*pieces, near, spatial, bias]
    specs = [pl.BlockSpec(memory_space=pl.ANY)] * (chunks + 1) + [None] * 2
    return call(gating_kernel, "gating", operands, specs, chunks, shards, tall, scratch, flops, 16)


def channel(pieces, gate_scale, up_scale, ring):
    chunks, shards, tall = len(pieces), len(ring), 256
    rows, width = pieces[0].shape
    hidden = gate_scale.shape[0]
    model = chunks * width
    flops = 2 * rows * model * 3 * hidden
    scratch = [(rows, model), *[(hidden, model)] * 3]
    scratch.append(pltpu.SemaphoreType.DMA((chunks + 3 * shards,)))
    operands = [*pieces, gate_scale, up_scale, *ring]
    specs = [pl.BlockSpec(memory_space=pl.ANY)] * len(operands)
    specs[chunks] = specs[chunks + 1] = None
    return call(channel_kernel, "channel", operands, specs, chunks, shards, tall, scratch, flops, 57)


def local(
    tokens,
    mix_gain,
    w_u,
    w_v,
    u_scale,
    v_scale,
    spatial,
    spatial_bias,
    w_mix,
    mix_scale,
    ffn_gain,
    w_gate,
    w_up,
    gate_scale,
    up_scale,
    w_down,
    down_scale,
):
    depth, span = w_u.shape
    hidden, out = w_down.shape
    near, far = fold(
        [(depth, 2 * span + w_mix.shape[1]), (3 * hidden, out)],
        mix_gain.reshape(-1, depth),
        w_u,
        w_v,
        w_mix,
        u_scale[None],
        v_scale[None],
        mix_scale,
        ffn_gain.reshape(-1, depth),
        w_gate.T,
        w_up.T,
        w_down,
        down_scale,
    )

    near = lax.all_gather(near, "fs")
    ring = Ring(far)
    steps = ring.count // 2
    pieces = gather_features(tokens)
    early = steps // 2
    for _ in range(early):
        ring.advance()
    pieces[0], *_ = lax.optimization_barrier((pieces[0], *ring.held[-2:]))
    mine, theirs = gating(pieces, near, spatial[0], spatial_bias)
    ring.advance()
    pair = chip_sums(mine, theirs)
    ring.after(*pair[1:])
    ring.advance()
    resid = (tokens.astype(jnp.float32) + sum_chips(pair)).astype(jnp.bfloat16)
    ring.after(resid)
    while ring.step < steps:
        ring.advance()
    mine, theirs = channel(gather_features(resid), gate_scale, up_scale, ring.held)
    pair = chip_sums(mine, theirs)
    return (resid.astype(jnp.float32) + sum_chips(pair)).astype(jnp.bfloat16)


def solution(mesh):
    placed = (
        P(("grp", "fs"), "tp"),
        P(),
        P("fs", "tp"),
        P("fs", "tp"),
        P("tp"),
        P("tp"),
        P("tp", None, None),
        P("tp", None),
        P("tp", "fs"),
        P(None, "fs"),
        P(),
        P("fs", "tp"),
        P("fs", "tp"),
        P("tp"),
        P("tp"),
        P("tp", "fs"),
        P(None, "fs"),
    )
    return jax.shard_map(
        local, mesh=mesh, in_specs=placed, out_specs=P(("grp", "fs"), "tp"), check_vma=False
    )
```

profile of v0, /device:TPU:33, one launch (start us, length us, event | category | flops | bytes accessed | tf_op | source)
XLA Modules:
  0.0 223.9 jit_solution(9730778729606548217)
XLA Ops:
  6.6 2.4 %fold.1 = (bf16[128,384]{1,0:T(8,128)(2,1)}, bf16[2112,128]{1,0:T(8,128)(2,1)}) custom-call(f32[16,128]{1,0:T(8,128)} %bitcast.60, f32[128,128]{1,0:T(8,128)} %u_ref.1, f32[128,128]{1,0:T(8,128)} %v_ref.1, f32[128,128]{1,0:T(8,128)} %mix_ref.1, f32[1,128]{1,0:T(1,128)} %bitcast.62, f32[1,128]{1,0:T(1,128)} %bitcast.63, f32[1,128]{1,0:T(1,128)} %mix_scale_ref.1, ...), custom_call_target="tpu_custom_call" | custom-call | flops 4194304 | bytes 1048576 | tf_op jit(solution)/shard_map/fold/pallas_call | solution.py:273
  9.0 23.0 %collective-permute-start.2 = (bf16[2112,128]{1,0:T(8,128)(2,1)}, bf16[2112,128]{1,0:T(8,128)(2,1)S(1)}, u32[]{:S(2)}, u32[]{:S(2)}) collective-permute-start(bf16[2112,128]{1,0:T(8,128)(2,1)} %get-tuple-element.29.refs_10_), channel_id=1, source_target_pairs={{0,120},{8,0},{16,8},{24,16},{32,24},{40,32},{48,40},{56,48},{64,5... | collective-permute-start | bytes 1622024 | tf_op jit(solution)/shard_map/ppermute | solution.py:62
  32.0 12.5 %collective-permute-done.2.refs_12_ = bf16[2112,128]{1,0:T(8,128)(2,1)S(1)} collective-permute-done((bf16[2112,128]{1,0:T(8,128)(2,1)}, bf16[2112,128]{1,0:T(8,128)(2,1)S(1)}, u32[]{:S(2)}, u32[]{:S(2)}) %collective-permute-start.2) | collective-permute-done | bytes 540704 | tf_op jit(solution)/shard_map/ppermute | solution.py:62
  44.6 3.3 %collective-permute-start.4 = (bf16[2112,128]{1,0:T(8,128)(2,1)S(1)}, bf16[2112,128]{1,0:T(8,128)(2,1)S(1)}, u32[]{:S(2)}, u32[]{:S(2)}) collective-permute-start(bf16[2112,128]{1,0:T(8,128)(2,1)S(1)} %collective-permute-done.2.refs_12_), channel_id=1, source_target_pairs={{0,120},{8,0},{16,8},{24,16},{32,24},{40,32},{48,40},{56,48},{64,5... | collective-permute-start | bytes 1622024 | tf_op jit(solution)/shard_map/ppermute | solution.py:62
  51.6 11.4 %collective-permute-done.4.refs_14_ = bf16[2112,128]{1,0:T(8,128)(2,1)S(1)} collective-permute-done((bf16[2112,128]{1,0:T(8,128)(2,1)S(1)}, bf16[2112,128]{1,0:T(8,128)(2,1)S(1)}, u32[]{:S(2)}, u32[]{:S(2)}) %collective-permute-start.4) | collective-permute-done | bytes 540704 | tf_op jit(solution)/shard_map/ppermute | solution.py:62
  63.0 2.4 %collective-permute-done.1.refs_13_ = bf16[2112,128]{1,0:T(8,128)(2,1)S(1)} collective-permute-done((bf16[2112,128]{1,0:T(8,128)(2,1)S(1)}, bf16[2112,128]{1,0:T(8,128)(2,1)S(1)}, u32[]{:S(2)}, u32[]{:S(2)}) %collective-permute-start.1) | collective-permute-done | bytes 540704 | tf_op jit(solution)/shard_map/ppermute | solution.py:62
  65.4 2.6 %collective-permute-start.6 = (bf16[2112,128]{1,0:T(8,128)(2,1)S(1)}, bf16[2112,128]{1,0:T(8,128)(2,1)S(1)}, u32[]{:S(2)}, u32[]{:S(2)}) collective-permute-start(bf16[2112,128]{1,0:T(8,128)(2,1)S(1)} %collective-permute-done.4.refs_14_), channel_id=1, source_target_pairs={{0,120},{8,0},{16,8},{24,16},{32,24},{40,32},{48,40},{56,48},{64,5... | collective-permute-start | bytes 1622024 | tf_op jit(solution)/shard_map/ppermute | solution.py:62
  68.1 4.4 %collective-permute-start.11 = (bf16[2,768,256]{2,1,0:T(8,128)(2,1)S(1)}, bf16[2,768,256]{2,1,0:T(8,128)(2,1)S(1)}, u32[]{:S(2)}, u32[]{:S(2)}) collective-permute-start(bf16[2,768,256]{2,1,0:T(8,128)(2,1)S(1)} %pad_maximum_fusion), channel_id=1, source_target_pairs={{0,1},{1,0},{2,3},{3,2},{4,5},{5,4},{6,7},{7,6},{8,9},{9,8},{10,11... | collective-permute-start | bytes 2359304 | tf_op jit(solution)/shard_map/ppermute | solution.py:16
  72.5 3.2 %collective-permute-start.12 = (bf16[768,256]{1,0:T(8,128)(2,1)S(1)}, bf16[768,256]{1,0:T(8,128)(2,1)S(1)}, u32[]{:S(2)}, u32[]{:S(2)}) collective-permute-start(bf16[768,256]{1,0:T(8,128)(2,1)S(1)} %copy-done.1), channel_id=1, source_target_pairs={{0,4},{1,5},{2,6},{3,7},{4,0},{5,1},{6,2},{7,3},{8,12},{9,13},{10,... | collective-permute-start | bytes 1179656 | tf_op jit(solution)/shard_map/ppermute | solution.py:21
  75.8 6.5 %collective-permute-done.3.refs_15_ = bf16[2112,128]{1,0:T(8,128)(2,1)S(1)} collective-permute-done((bf16[2112,128]{1,0:T(8,128)(2,1)S(1)}, bf16[2112,128]{1,0:T(8,128)(2,1)S(1)}, u32[]{:S(2)}, u32[]{:S(2)}) %collective-permute-start.3) | collective-permute-done | bytes 540704 | tf_op jit(solution)/shard_map/ppermute | solution.py:62
  82.3 2.8 %collective-permute-start.7 = (bf16[2112,128]{1,0:T(8,128)(2,1)S(1)}, bf16[2112,128]{1,0:T(8,128)(2,1)S(1)}, u32[]{:S(2)}, u32[]{:S(2)}) collective-permute-start(bf16[2112,128]{1,0:T(8,128)(2,1)S(1)} %collective-permute-done.6.refs_16_), channel_id=1, source_target_pairs={{0,120},{8,0},{16,8},{24,16},{32,24},{40,32},{48,40},{56,48},{64,5... | collective-permute-start | bytes 1622024 | tf_op jit(solution)/shard_map/ppermute | solution.py:62
  85.0 5.5 %collective-permute-start.8 = (bf16[768,256]{1,0:T(8,128)(2,1)S(1)}, bf16[768,256]{1,0:T(8,128)(2,1)S(1)}, u32[]{:S(2)}, u32[]{:S(2)}) collective-permute-start(bf16[768,256]{1,0:T(8,128)(2,1)S(1)} %copy-done.1), channel_id=1, source_target_pairs={{0,1},{1,0},{2,3},{3,2},{4,5},{5,4},{6,7},{7,6},{8,9},{9,8},{10,11... | collective-permute-start | bytes 1179656 | tf_op jit(solution)/shard_map/ppermute | solution.py:16
  90.6 5.4 %collective-permute-done.5.refs_17_ = bf16[2112,128]{1,0:T(8,128)(2,1)S(1)} collective-permute-done((bf16[2112,128]{1,0:T(8,128)(2,1)S(1)}, bf16[2112,128]{1,0:T(8,128)(2,1)S(1)}, u32[]{:S(2)}, u32[]{:S(2)}) %collective-permute-start.5) | collective-permute-done | bytes 540704 | tf_op jit(solution)/shard_map/ppermute | solution.py:62
  98.5 7.2 %gating.1 = (bf16[4,768,256]{2,1,0:T(8,128)(2,1)S(1)}, bf16[4,768,256]{2,1,0:T(8,128)(2,1)S(1)}) custom-call(bf16[768,256]{1,0:T(8,128)(2,1)S(1)} %copy-done.1, bf16[768,256]{1,0:T(8,128)(2,1)S(1)} %collective-permute-done.8.refs_1_, bf16[768,256]{1,0:T(8,128)(2,1)S(1)} %collective-permute-done.9.refs_2_, bf16[768,256]{1,0:T(8,128)(2,1)S(1)} %get-tuple-element.60.refs_3_, ...), custom_call_target="tpu_custom_call" | custom-call | flops 1233125376 | bytes 1048576 | tf_op jit(solution)/shard_map/gating/pallas_call | solution.py:289
  105.7 4.5 %collective-permute-start.14 = (bf16[4,768,256]{2,1,0:T(8,128)(2,1)S(1)}, bf16[4,768,256]{2,1,0:T(8,128)(2,1)S(1)}, u32[]{:S(2)}, u32[]{:S(2)}) collective-permute-start(bf16[4,768,256]{2,1,0:T(8,128)(2,1)S(1)} %get-tuple-element.39), channel_id=1, source_target_pairs={{0,1},{1,0},{2,3},{3,2},{4,5},{5,4},{6,7},{7,6},{8,9},{9,8},{10,11... | collective-permute-start | bytes 4718600 | tf_op jit(solution)/shard_map/ppermute | solution.py:16
  110.1 3.0 %collective-permute-done.14 = bf16[4,768,256]{2,1,0:T(8,128)(2,1)S(1)} collective-permute-done((bf16[4,768,256]{2,1,0:T(8,128)(2,1)S(1)}, bf16[4,768,256]{2,1,0:T(8,128)(2,1)S(1)}, u32[]{:S(2)}, u32[]{:S(2)}) %collective-permute-start.14) | collective-permute-done | bytes 1572896 | tf_op jit(solution)/shard_map/ppermute | solution.py:16
  118.0 2.2 collective-permute-start.25
  120.2 4.8 %collective-permute-done.24.refs_19_ = bf16[2112,128]{1,0:T(8,128)(2,1)S(1)} collective-permute-done((bf16[2112,128]{1,0:T(8,128)(2,1)S(1)}, bf16[2112,128]{1,0:T(8,128)(2,1)S(1)}, u32[]{:S(2)}, u32[]{:S(2)}) %collective-permute-start.24) | collective-permute-done | bytes 540704 | tf_op jit(solution)/shard_map/ppermute | solution.py:62
  125.3 9.5 %collective-permute-done.16 = bf16[768,256]{1,0:T(8,128)(2,1)S(1)} collective-permute-done((bf16[768,256]{1,0:T(8,128)(2,1)S(1)}, bf16[768,256]{1,0:T(8,128)(2,1)S(1)}, u32[]{:S(2)}, u32[]{:S(2)}) %collective-permute-start.16) | collective-permute-done | bytes 393248 | tf_op jit(solution)/shard_map/ppermute | solution.py:21
  136.7 2.2 collective-permute-start.27
  139.1 5.6 %collective-permute-done.20.refs_6_ = bf16[768,256]{1,0:T(8,128)(2,1)S(1)} collective-permute-done((bf16[768,256]{1,0:T(8,128)(2,1)S(1)}, bf16[768,256]{1,0:T(8,128)(2,1)S(1)}, u32[]{:S(2)}, u32[]{:S(2)}) %collective-permute-start.20) | collective-permute-done | bytes 393248 | tf_op jit(solution)/shard_map/ppermute | solution.py:21
  144.7 1.7 collective-permute-done.19.refs_2_
  146.5 2.9 %collective-permute-start.21 = (bf16[2,768,256]{2,1,0:T(8,128)(2,1)S(1)}, bf16[2,768,256]{2,1,0:T(8,128)(2,1)S(1)}, u32[]{:S(2)}, u32[]{:S(2)}) collective-permute-start(bf16[2,768,256]{2,1,0:T(8,128)(2,1)S(1)} %pad_maximum_fusion.1), channel_id=1, source_target_pairs={{0,1},{1,0},{2,3},{3,2},{4,5},{5,4},{6,7},{7,6},{8,9},{9,8},{10,11... | collective-permute-start | bytes 2359304 | tf_op jit(solution)/shard_map/ppermute | solution.py:16
  149.4 2.8 %collective-permute-start.29 = (bf16[2112,128]{1,0:T(8,128)(2,1)S(1)}, bf16[2112,128]{1,0:T(8,128)(2,1)S(1)}, u32[]{:S(2)}, u32[]{:S(2)}) collective-permute-start(bf16[2112,128]{1,0:T(8,128)(2,1)S(1)} %collective-permute-done.27.refs_22_), channel_id=1, source_target_pairs={{0,120},{8,0},{16,8},{24,16},{32,24},{40,32},{48,40},{56,48},{64,5... | collective-permute-start | bytes 1622024 | tf_op jit(solution)/shard_map/ppermute | solution.py:62
  152.2 3.0 %collective-permute-start.18 = (bf16[768,256]{1,0:T(8,128)(2,1)S(1)}, bf16[768,256]{1,0:T(8,128)(2,1)S(1)}, u32[]{:S(2)}, u32[]{:S(2)}) collective-permute-start(bf16[768,256]{1,0:T(8,128)(2,1)S(1)} %fusion.7.refs_0_), channel_id=1, source_target_pairs={{0,1},{1,0},{2,3},{3,2},{4,5},{5,4},{6,7},{7,6},{8,9},{9,8},{10,11... | collective-permute-start | bytes 1179656 | tf_op jit(solution)/shard_map/ppermute | solution.py:16
  155.3 6.2 %collective-permute-done.22.refs_4_ = bf16[768,256]{1,0:T(8,128)(2,1)S(1)} collective-permute-done((bf16[768,256]{1,0:T(8,128)(2,1)S(1)}, bf16[768,256]{1,0:T(8,128)(2,1)S(1)}, u32[]{:S(2)}, u32[]{:S(2)}) %collective-permute-start.22) | collective-permute-done | bytes 393248 | tf_op jit(solution)/shard_map/ppermute | solution.py:21
  165.1 19.9 %channel.1 = (bf16[4,768,256]{2,1,0:T(8,128)(2,1)}, bf16[4,768,256]{2,1,0:T(8,128)(2,1)}) custom-call(bf16[768,256]{1,0:T(8,128)(2,1)} %copy-done.4, bf16[768,256]{1,0:T(8,128)(2,1)} %copy-done.26, bf16[768,256]{1,0:T(8,128)(2,1)} %copy-done.7, bf16[768,256]{1,0:T(8,128)(2,1)} %get-tuple-element.58.refs_3_, bf16[768,256]{1,0:T(8,128)(2,1)} %copy-done.25, ...), custom_call_target="tpu_custom_call" | custom-call | flops 6643777536 | bytes 1048576 | tf_op jit(solution)/shard_map/channel/pallas_call | solution.py:289
  185.0 3.9 %collective-permute-start.31 = (bf16[4,768,256]{2,1,0:T(8,128)(2,1)}, bf16[4,768,256]{2,1,0:T(8,128)(2,1)S(1)}, u32[]{:S(2)}, u32[]{:S(2)}) collective-permute-start(bf16[4,768,256]{2,1,0:T(8,128)(2,1)} %get-tuple-element.50), channel_id=1, source_target_pairs={{0,1},{1,0},{2,3},{3,2},{4,5},{5,4},{6,7},{7,6},{8,9},{9,8},{10,11... | collective-permute-start | bytes 4718600 | tf_op jit(solution)/shard_map/ppermute | solution.py:16
  188.9 3.2 %collective-permute-done.31 = bf16[4,768,256]{2,1,0:T(8,128)(2,1)S(1)} collective-permute-done((bf16[4,768,256]{2,1,0:T(8,128)(2,1)}, bf16[4,768,256]{2,1,0:T(8,128)(2,1)S(1)}, u32[]{:S(2)}, u32[]{:S(2)}) %collective-permute-start.31) | collective-permute-done | bytes 1572896 | tf_op jit(solution)/shard_map/ppermute | solution.py:16
  198.3 7.1 %collective-permute-done.32 = bf16[768,256]{1,0:T(8,128)(2,1)S(1)} collective-permute-done((bf16[768,256]{1,0:T(8,128)(2,1)S(1)}, bf16[768,256]{1,0:T(8,128)(2,1)S(1)}, u32[]{:S(2)}, u32[]{:S(2)}) %collective-permute-start.32) | collective-permute-done | bytes 393248 | tf_op jit(solution)/shard_map/ppermute | solution.py:21
  205.5 9.5 %collective-permute-done.33 = bf16[768,256]{1,0:T(8,128)(2,1)S(1)} collective-permute-done((bf16[768,256]{1,0:T(8,128)(2,1)S(1)}, bf16[768,256]{1,0:T(8,128)(2,1)S(1)}, u32[]{:S(2)}, u32[]{:S(2)}) %collective-permute-start.33) | collective-permute-done | bytes 393248 | tf_op jit(solution)/shard_map/ppermute | solution.py:21
  215.0 2.1 fusion.3
  (108 shorter events, 23.6 us)
Async XLA Ops:
  6.5 90.5 %all-gather.3.cloned.1.call-start = ((), (), s32[]{:S(2)}) async-start(), calls=%async_computation | async-start | bytes 1671168 | tf_op jit(solution)/shard_map/all_gather | solution.py:372
  9.0 35.6 %collective-permute-start.2 = (bf16[2112,128]{1,0:T(8,128)(2,1)}, bf16[2112,128]{1,0:T(8,128)(2,1)S(1)}, u32[]{:S(2)}, u32[]{:S(2)}) collective-permute-start(bf16[2112,128]{1,0:T(8,128)(2,1)} %get-tuple-element.29.refs_10_), channel_id=1, source_target_pairs={{0,120},{8,0},{16,8},{24,16},{32,24},{40,32},{48,40},{56,48},{64,5... | collective-permute-start | bytes 1622024 | tf_op jit(solution)/shard_map/ppermute | solution.py:62
  32.0 16.4 %collective-permute-start = (bf16[2112,128]{1,0:T(8,128)(2,1)}, bf16[2112,128]{1,0:T(8,128)(2,1)S(1)}, u32[]{:S(2)}, u32[]{:S(2)}) collective-permute-start(bf16[2112,128]{1,0:T(8,128)(2,1)} %get-tuple-element.29.refs_10_), channel_id=1, source_target_pairs={{0,8},{8,16},{16,24},{24,32},{32,40},{40,48},{48,56},{56,64},{64,7... | collective-permute-start | bytes 1622024 | tf_op jit(solution)/shard_map/ppermute | solution.py:62
  44.6 18.4 %collective-permute-start.4 = (bf16[2112,128]{1,0:T(8,128)(2,1)S(1)}, bf16[2112,128]{1,0:T(8,128)(2,1)S(1)}, u32[]{:S(2)}, u32[]{:S(2)}) collective-permute-start(bf16[2112,128]{1,0:T(8,128)(2,1)S(1)} %collective-permute-done.2.refs_12_), channel_id=1, source_target_pairs={{0,120},{8,0},{16,8},{24,16},{32,24},{40,32},{48,40},{56,48},{64,5... | collective-permute-start | bytes 1622024 | tf_op jit(solution)/shard_map/ppermute | solution.py:62
  48.4 16.9 %collective-permute-start.1 = (bf16[2112,128]{1,0:T(8,128)(2,1)S(1)}, bf16[2112,128]{1,0:T(8,128)(2,1)S(1)}, u32[]{:S(2)}, u32[]{:S(2)}) collective-permute-start(bf16[2112,128]{1,0:T(8,128)(2,1)S(1)} %collective-permute-done.refs_11_), channel_id=1, source_target_pairs={{0,8},{8,16},{16,24},{24,32},{32,40},{40,48},{48,56},{56,64},{64,7... | collective-permute-start | bytes 1622024 | tf_op jit(solution)/shard_map/ppermute | solution.py:62
  48.4 19.6 %collective-permute-start.9 = (bf16[768,256]{1,0:T(8,128)(2,1)}, bf16[768,256]{1,0:T(8,128)(2,1)S(1)}, u32[]{:S(2)}, u32[]{:S(2)}) collective-permute-start(bf16[768,256]{1,0:T(8,128)(2,1)} %refs_0_), channel_id=1, source_target_pairs={{0,2},{1,3},{2,4},{3,5},{4,6},{5,7},{6,0},{7,1},{8,10},{9,11},{10,... | collective-permute-start | bytes 1179656 | tf_op jit(solution)/shard_map/ppermute | solution.py:21
  49.9 18.1 %collective-permute-start.10 = (bf16[768,256]{1,0:T(8,128)(2,1)}, bf16[768,256]{1,0:T(8,128)(2,1)S(1)}, u32[]{:S(2)}, u32[]{:S(2)}) collective-permute-start(bf16[768,256]{1,0:T(8,128)(2,1)} %refs_0_), channel_id=1, source_target_pairs={{0,6},{1,7},{2,0},{3,1},{4,2},{5,3},{6,4},{7,5},{8,14},{9,15},{10,... | collective-permute-start | bytes 1179656 | tf_op jit(solution)/shard_map/ppermute | solution.py:21
  65.3 16.9 %collective-permute-start.3 = (bf16[2112,128]{1,0:T(8,128)(2,1)S(1)}, bf16[2112,128]{1,0:T(8,128)(2,1)S(1)}, u32[]{:S(2)}, u32[]{:S(2)}) collective-permute-start(bf16[2112,128]{1,0:T(8,128)(2,1)S(1)} %collective-permute-done.1.refs_13_), channel_id=1, source_target_pairs={{0,8},{8,16},{16,24},{24,32},{32,40},{40,48},{48,56},{56,64},{64,7... | collective-permute-start | bytes 1622024 | tf_op jit(solution)/shard_map/ppermute | solution.py:62
  65.4 16.8 %collective-permute-start.6 = (bf16[2112,128]{1,0:T(8,128)(2,1)S(1)}, bf16[2112,128]{1,0:T(8,128)(2,1)S(1)}, u32[]{:S(2)}, u32[]{:S(2)}) collective-permute-start(bf16[2112,128]{1,0:T(8,128)(2,1)S(1)} %collective-permute-done.4.refs_14_), channel_id=1, source_target_pairs={{0,120},{8,0},{16,8},{24,16},{32,24},{40,32},{48,40},{56,48},{64,5... | collective-permute-start | bytes 1622024 | tf_op jit(solution)/shard_map/ppermute | solution.py:62
  68.1 22.4 %collective-permute-start.11 = (bf16[2,768,256]{2,1,0:T(8,128)(2,1)S(1)}, bf16[2,768,256]{2,1,0:T(8,128)(2,1)S(1)}, u32[]{:S(2)}, u32[]{:S(2)}) collective-permute-start(bf16[2,768,256]{2,1,0:T(8,128)(2,1)S(1)} %pad_maximum_fusion), channel_id=1, source_target_pairs={{0,1},{1,0},{2,3},{3,2},{4,5},{5,4},{6,7},{7,6},{8,9},{9,8},{10,11... | collective-permute-start | bytes 2359304 | tf_op jit(solution)/shard_map/ppermute | solution.py:16
  72.5 18.0 %collective-permute-start.12 = (bf16[768,256]{1,0:T(8,128)(2,1)S(1)}, bf16[768,256]{1,0:T(8,128)(2,1)S(1)}, u32[]{:S(2)}, u32[]{:S(2)}) collective-permute-start(bf16[768,256]{1,0:T(8,128)(2,1)S(1)} %copy-done.1), channel_id=1, source_target_pairs={{0,4},{1,5},{2,6},{3,7},{4,0},{5,1},{6,2},{7,3},{8,12},{9,13},{10,... | collective-permute-start | bytes 1179656 | tf_op jit(solution)/shard_map/ppermute | solution.py:21
  82.2 13.8 %collective-permute-start.5 = (bf16[2112,128]{1,0:T(8,128)(2,1)S(1)}, bf16[2112,128]{1,0:T(8,128)(2,1)S(1)}, u32[]{:S(2)}, u32[]{:S(2)}) collective-permute-start(bf16[2112,128]{1,0:T(8,128)(2,1)S(1)} %collective-permute-done.3.refs_15_), channel_id=1, source_target_pairs={{0,8},{8,16},{16,24},{24,32},{32,40},{40,48},{48,56},{56,64},{64,7... | collective-permute-start | bytes 1622024 | tf_op jit(solution)/shard_map/ppermute | solution.py:62
  82.3 13.7 %collective-permute-start.7 = (bf16[2112,128]{1,0:T(8,128)(2,1)S(1)}, bf16[2112,128]{1,0:T(8,128)(2,1)S(1)}, u32[]{:S(2)}, u32[]{:S(2)}) collective-permute-start(bf16[2112,128]{1,0:T(8,128)(2,1)S(1)} %collective-permute-done.6.refs_16_), channel_id=1, source_target_pairs={{0,120},{8,0},{16,8},{24,16},{32,24},{40,32},{48,40},{56,48},{64,5... | collective-permute-start | bytes 1622024 | tf_op jit(solution)/shard_map/ppermute | solution.py:62
  85.0 11.0 %collective-permute-start.8 = (bf16[768,256]{1,0:T(8,128)(2,1)S(1)}, bf16[768,256]{1,0:T(8,128)(2,1)S(1)}, u32[]{:S(2)}, u32[]{:S(2)}) collective-permute-start(bf16[768,256]{1,0:T(8,128)(2,1)S(1)} %copy-done.1), channel_id=1, source_target_pairs={{0,1},{1,0},{2,3},{3,2},{4,5},{5,4},{6,7},{7,6},{8,9},{9,8},{10,11... | collective-permute-start | bytes 1179656 | tf_op jit(solution)/shard_map/ppermute | solution.py:16
  110.1 14.9 %collective-permute-start.24 = (bf16[2112,128]{1,0:T(8,128)(2,1)S(1)}, bf16[2112,128]{1,0:T(8,128)(2,1)S(1)}, u32[]{:S(2)}, u32[]{:S(2)}) collective-permute-start(bf16[2112,128]{1,0:T(8,128)(2,1)S(1)} %copy-done.15), channel_id=1, source_target_pairs={{0,8},{8,16},{16,24},{24,32},{32,40},{40,48},{48,56},{56,64},{64,7... | collective-permute-start | bytes 1622024 | tf_op jit(solution)/shard_map/ppermute | solution.py:62
  113.5 11.8 %collective-permute-start.15 = (bf16[768,256]{1,0:T(8,128)(2,1)S(1)}, bf16[768,256]{1,0:T(8,128)(2,1)S(1)}, u32[]{:S(2)}, u32[]{:S(2)}) collective-permute-start(bf16[768,256]{1,0:T(8,128)(2,1)S(1)} %get-tuple-element.54), channel_id=1, source_target_pairs={{0,2},{1,3},{2,4},{3,5},{4,6},{5,7},{6,0},{7,1},{8,10},{9,11},{10,... | collective-permute-start | bytes 1179656 | tf_op jit(solution)/shard_map/ppermute | solution.py:21
  115.1 10.2 %collective-permute-start.17 = (bf16[768,256]{1,0:T(8,128)(2,1)S(1)}, bf16[768,256]{1,0:T(8,128)(2,1)S(1)}, u32[]{:S(2)}, u32[]{:S(2)}) collective-permute-start(bf16[768,256]{1,0:T(8,128)(2,1)S(1)} %get-tuple-element.55), channel_id=1, source_target_pairs={{0,6},{1,7},{2,0},{3,1},{4,2},{5,3},{6,4},{7,5},{8,14},{9,15},{10,... | collective-permute-start | bytes 1179656 | tf_op jit(solution)/shard_map/ppermute | solution.py:21
  116.5 18.3 %collective-permute-start.16 = (bf16[768,256]{1,0:T(8,128)(2,1)S(1)}, bf16[768,256]{1,0:T(8,128)(2,1)S(1)}, u32[]{:S(2)}, u32[]{:S(2)}) collective-permute-start(bf16[768,256]{1,0:T(8,128)(2,1)S(1)} %get-tuple-element.56), channel_id=1, source_target_pairs={{0,4},{1,5},{2,6},{3,7},{4,0},{5,1},{6,2},{7,3},{8,12},{9,13},{10,... | collective-permute-start | bytes 1179656 | tf_op jit(solution)/shard_map/ppermute | solution.py:21
  118.0 18.7 %collective-permute-start.25 = (bf16[2112,128]{1,0:T(8,128)(2,1)S(1)}, bf16[2112,128]{1,0:T(8,128)(2,1)S(1)}, u32[]{:S(2)}, u32[]{:S(2)}) collective-permute-start(bf16[2112,128]{1,0:T(8,128)(2,1)S(1)} %copy-done.17), channel_id=1, source_target_pairs={{0,120},{8,0},{16,8},{24,16},{32,24},{40,32},{48,40},{56,48},{64,5... | collective-permute-start | bytes 1622024 | tf_op jit(solution)/shard_map/ppermute | solution.py:62
  125.0 14.0 %collective-permute-start.26 = (bf16[2112,128]{1,0:T(8,128)(2,1)S(1)}, bf16[2112,128]{1,0:T(8,128)(2,1)S(1)}, u32[]{:S(2)}, u32[]{:S(2)}) collective-permute-start(bf16[2112,128]{1,0:T(8,128)(2,1)S(1)} %collective-permute-done.24.refs_19_), channel_id=1, source_target_pairs={{0,8},{8,16},{16,24},{24,32},{32,40},{40,48},{48,56},{56,64},{64,7... | collective-permute-start | bytes 1622024 | tf_op jit(solution)/shard_map/ppermute | solution.py:62
  135.1 9.6 %collective-permute-start.20 = (bf16[768,256]{1,0:T(8,128)(2,1)S(1)}, bf16[768,256]{1,0:T(8,128)(2,1)S(1)}, u32[]{:S(2)}, u32[]{:S(2)}) collective-permute-start(bf16[768,256]{1,0:T(8,128)(2,1)S(1)} %fusion.7.refs_0_), channel_id=1, source_target_pairs={{0,6},{1,7},{2,0},{3,1},{4,2},{5,3},{6,4},{7,5},{8,14},{9,15},{10,... | collective-permute-start | bytes 1179656 | tf_op jit(solution)/shard_map/ppermute | solution.py:21
  136.5 9.9 %collective-permute-start.19 = (bf16[768,256]{1,0:T(8,128)(2,1)S(1)}, bf16[768,256]{1,0:T(8,128)(2,1)S(1)}, u32[]{:S(2)}, u32[]{:S(2)}) collective-permute-start(bf16[768,256]{1,0:T(8,128)(2,1)S(1)} %fusion.7.refs_0_), channel_id=1, source_target_pairs={{0,2},{1,3},{2,4},{3,5},{4,6},{5,7},{6,0},{7,1},{8,10},{9,11},{10,... | collective-permute-start | bytes 1179656 | tf_op jit(solution)/shard_map/ppermute | solution.py:21
  136.7 12.7 %collective-permute-start.27 = (bf16[2112,128]{1,0:T(8,128)(2,1)S(1)}, bf16[2112,128]{1,0:T(8,128)(2,1)S(1)}, u32[]{:S(2)}, u32[]{:S(2)}) collective-permute-start(bf16[2112,128]{1,0:T(8,128)(2,1)S(1)} %collective-permute-done.25.refs_20_), channel_id=1, source_target_pairs={{0,120},{8,0},{16,8},{24,16},{32,24},{40,32},{48,40},{56,48},{64,5... | collective-permute-start | bytes 1622024 | tf_op jit(solution)/shard_map/ppermute | solution.py:62
  139.1 13.1 %collective-permute-start.28 = (bf16[2112,128]{1,0:T(8,128)(2,1)S(1)}, bf16[2112,128]{1,0:T(8,128)(2,1)S(1)}, u32[]{:S(2)}, u32[]{:S(2)}) collective-permute-start(bf16[2112,128]{1,0:T(8,128)(2,1)S(1)} %collective-permute-done.26.refs_21_), channel_id=1, source_target_pairs={{0,8},{8,16},{16,24},{24,32},{32,40},{40,48},{48,56},{56,64},{64,7... | collective-permute-start | bytes 1622024 | tf_op jit(solution)/shard_map/ppermute | solution.py:62
  146.5 16.0 %collective-permute-start.21 = (bf16[2,768,256]{2,1,0:T(8,128)(2,1)S(1)}, bf16[2,768,256]{2,1,0:T(8,128)(2,1)S(1)}, u32[]{:S(2)}, u32[]{:S(2)}) collective-permute-start(bf16[2,768,256]{2,1,0:T(8,128)(2,1)S(1)} %pad_maximum_fusion.1), channel_id=1, source_target_pairs={{0,1},{1,0},{2,3},{3,2},{4,5},{5,4},{6,7},{7,6},{8,9},{9,8},{10,11... | collective-permute-start | bytes 2359304 | tf_op jit(solution)/shard_map/ppermute | solution.py:16
  149.4 12.0 %collective-permute-start.22 = (bf16[768,256]{1,0:T(8,128)(2,1)S(1)}, bf16[768,256]{1,0:T(8,128)(2,1)S(1)}, u32[]{:S(2)}, u32[]{:S(2)}) collective-permute-start(bf16[768,256]{1,0:T(8,128)(2,1)S(1)} %fusion.7.refs_0_), channel_id=1, source_target_pairs={{0,4},{1,5},{2,6},{3,7},{4,0},{5,1},{6,2},{7,3},{8,12},{9,13},{10,... | collective-permute-start | bytes 1179656 | tf_op jit(solution)/shard_map/ppermute | solution.py:21
  149.4 14.0 %collective-permute-start.29 = (bf16[2112,128]{1,0:T(8,128)(2,1)S(1)}, bf16[2112,128]{1,0:T(8,128)(2,1)S(1)}, u32[]{:S(2)}, u32[]{:S(2)}) collective-permute-start(bf16[2112,128]{1,0:T(8,128)(2,1)S(1)} %collective-permute-done.27.refs_22_), channel_id=1, source_target_pairs={{0,120},{8,0},{16,8},{24,16},{32,24},{40,32},{48,40},{56,48},{64,5... | collective-permute-start | bytes 1622024 | tf_op jit(solution)/shard_map/ppermute | solution.py:62
  152.2 12.1 %collective-permute-start.30 = (bf16[2112,128]{1,0:T(8,128)(2,1)S(1)}, bf16[2112,128]{1,0:T(8,128)(2,1)S(1)}, u32[]{:S(2)}, u32[]{:S(2)}) collective-permute-start(bf16[2112,128]{1,0:T(8,128)(2,1)S(1)} %collective-permute-done.28.refs_23_), channel_id=1, source_target_pairs={{0,8},{8,16},{16,24},{24,32},{32,40},{40,48},{48,56},{56,64},{64,7... | collective-permute-start | bytes 1622024 | tf_op jit(solution)/shard_map/ppermute | solution.py:62
  152.2 11.2 %collective-permute-start.18 = (bf16[768,256]{1,0:T(8,128)(2,1)S(1)}, bf16[768,256]{1,0:T(8,128)(2,1)S(1)}, u32[]{:S(2)}, u32[]{:S(2)}) collective-permute-start(bf16[768,256]{1,0:T(8,128)(2,1)S(1)} %fusion.7.refs_0_), channel_id=1, source_target_pairs={{0,1},{1,0},{2,3},{3,2},{4,5},{5,4},{6,7},{7,6},{8,9},{9,8},{10,11... | collective-permute-start | bytes 1179656 | tf_op jit(solution)/shard_map/ppermute | solution.py:16
  193.8 11.6 %collective-permute-start.32 = (bf16[768,256]{1,0:T(8,128)(2,1)S(1)}, bf16[768,256]{1,0:T(8,128)(2,1)S(1)}, u32[]{:S(2)}, u32[]{:S(2)}) collective-permute-start(bf16[768,256]{1,0:T(8,128)(2,1)S(1)} %get-tuple-element.51), channel_id=1, source_target_pairs={{0,2},{1,3},{2,4},{3,5},{4,6},{5,7},{6,0},{7,1},{8,10},{9,11},{10,... | collective-permute-start | bytes 1179656 | tf_op jit(solution)/shard_map/ppermute | solution.py:21
  195.4 10.0 %collective-permute-start.34 = (bf16[768,256]{1,0:T(8,128)(2,1)S(1)}, bf16[768,256]{1,0:T(8,128)(2,1)S(1)}, u32[]{:S(2)}, u32[]{:S(2)}) collective-permute-start(bf16[768,256]{1,0:T(8,128)(2,1)S(1)} %get-tuple-element.52), channel_id=1, source_target_pairs={{0,6},{1,7},{2,0},{3,1},{4,2},{5,3},{6,4},{7,5},{8,14},{9,15},{10,... | collective-permute-start | bytes 1179656 | tf_op jit(solution)/shard_map/ppermute | solution.py:21
  196.7 18.3 %collective-permute-start.33 = (bf16[768,256]{1,0:T(8,128)(2,1)S(1)}, bf16[768,256]{1,0:T(8,128)(2,1)S(1)}, u32[]{:S(2)}, u32[]{:S(2)}) collective-permute-start(bf16[768,256]{1,0:T(8,128)(2,1)S(1)} %get-tuple-element.53), channel_id=1, source_target_pairs={{0,4},{1,5},{2,6},{3,7},{4,0},{5,1},{6,2},{7,3},{8,12},{9,13},{10,... | collective-permute-start | bytes 1179656 | tf_op jit(solution)/shard_map/ppermute | solution.py:21
  (32 other events, 475.1 us)
Sparse Core Ops, SparseCore 0:
  9.1 79.0 all-gather.2
where the time goes:
time: 224 us
  waiting for transfers between devices  90.8 us (41%)
  starting transfers between devices  81.2 us (36%)
  Pallas kernels  29.5 us (13%)
  between operations  13.7 us (6%)
  other arithmetic  4.44 us (2%)
  local copies, waits for them, and re-layouts  4.3 us (2%)
    ppermute x15, waiting for transfers between devices, pass_on(): lax.ppermute(x, 'fs', [(i, (i + step) % count) for i in range(count)])  44.2 us
    ppermute x12, waiting for transfers between devices, to_chip(): lax.ppermute(x, 'tp', [(i, (i + CORES * step) % count) for i in range(cou...  39.9 us
    ppermute x15, starting transfers between devices, pass_on(): lax.ppermute(x, 'fs', [(i, (i + step) % count) for i in range(count)])  39 us
    pallas_call x2, Pallas kernels, call(): pl.pallas_call(functools.partial(kernel, chunks=chunks, shards=shards, ta...  27.1 us
    ppermute x8, starting transfers between devices, swap_cores(): return lax.ppermute(x, 'tp', [(i, i ^ 1) for i in range(count)])  25.2 us
    ppermute x12, starting transfers between devices, to_chip(): lax.ppermute(x, 'tp', [(i, (i + CORES * step) % count) for i in range(cou...  17.1 us
    ppermute x8, waiting for transfers between devices, swap_cores(): return lax.ppermute(x, 'tp', [(i, i ^ 1) for i in range(count)])  6.62 us
  transfers between devices with their start and end apart: 36, of which 20 were waited for; matrix products, arithmetic and copies ran while one was open for 1% of the time, Pallas kernels for 0%

commit v1 on v0

--- a/solution.py
+++ b/solution.py
@@ -96,6 +96,11 @@
     return order
 
 
+def swap_groups(x):
+    count = lax.axis_size("grp")
+    return lax.ppermute(x, "grp", [(i, i ^ 1) for i in range(count)])
+
+
 def lane_block(index, width):
     return pl.ds(pl.multiple_of(index * width, width), width)
 
@@ -128,7 +133,7 @@
     return lax.rsqrt(jnp.mean(wide * wide, axis=1, keepdims=True) + eps)
 
 
-def store_shares(value, weights, chunks, rows, mine_ref, theirs_ref):
+def store_shares(value, weights, chunks, rows, mine_ref, theirs_ref, unroll=False):
     width = mine_ref.shape[2]
     chips = chunks // CORES
     me = lax.axis_index("tp")
@@ -141,7 +146,7 @@
             ref[step, rows, :] = dot_f32(value, w).astype(jnp.bfloat16)
             return carry
 
-        lax.fori_loop(0, chips, share, 0)
+        lax.fori_loop(0, chips, share, 0, unroll=unroll)
 
     fill(mine_ref, core)
     fill(theirs_ref, 1 - core)
@@ -195,40 +200,58 @@
     xs, refs = refs[:chunks], refs[chunks:]
     gate_scale_ref, up_scale_ref, refs = *refs[:2], refs[2:]
     ring, refs = refs[:shards], refs[shards:]
-    mine_ref, theirs_ref, x_buf, gate_buf, up_buf, down_buf, sems = refs
+    others, refs = refs[:-7], refs[-7:]
+    mine_ref, theirs_ref, x_buf, first_buf, down_buf, wide_buf, sems = refs
     lanes = ring[0].shape[1]
     hidden = down_buf.shape[0]
+    side = lax.rem(lax.axis_index("grp"), 2)
     around = ring_order(lax.axis_index("fs"), shards)
-
-    def load(part, buf, base):
-        rows = slice(part * hidden, (part + 1) * hidden)
+    parts = [(o, at) for o in others for at in range(0, o.shape[0], hidden)]
+    own_buf, other_buf = first_buf.at[side], first_buf.at[1 - side]
+
+    def load(pieces, buf, base):
         return copy_all(
-            [(w.at[rows, :], buf.at[:, lane_block(z, lanes)]) for z, w in zip(around, ring)],
+            [
+                (w.at[at : at + hidden, :], buf.at[:, lane_block(z, lanes)])
+                for z, (w, at) in zip(around, pieces)
+            ],
             sems,
             base,
         )
 
     x_here, at = load_rows(xs, x_buf, sems, 0)
-    gate_here, at = load(0, gate_buf, at)
-    up_here, at = load(1, up_buf, at)
-    down_here, at = load(2, down_buf, at)
+    own_here, at = load([(w, 0) for w in ring], own_buf, at)
+    other_here, at = load(parts, other_buf, at)
+    down_here, at = load([(w, hidden) for w in ring], down_buf, at)
     across = (((1,), (1,)), ((), ()))
+    blocks = xs[0].shape[0] // tall
     x_here()
-    gate_here()
-    up_here()
+    own_here()
+
+    def project(step, carry):
+        which = lax.select(step == 0, side, 1 - side)
+        pl.when(step == 1)(other_here)
+
+        def block(i, carry):
+            rows = pl.ds(pl.multiple_of(i * tall, tall), tall)
+            wide_buf[which, rows, :] = dot_f32(x_buf[rows, :], first_buf[which], across)
+            return carry
+
+        return lax.fori_loop(0, blocks, block, carry)
+
+    lax.fori_loop(0, 2, project, 0)
     down_here()
 
     def block(i, carry):
         rows = pl.ds(pl.multiple_of(i * tall, tall), tall)
-        x = x_buf[rows, :]
-        factor = row_factor(x)
-        gate = dot_f32(x, gate_buf[...], across) * factor * gate_scale_ref[...][None, :]
-        up = dot_f32(x, up_buf[...], across) * factor * up_scale_ref[...][None, :]
+        factor = row_factor(x_buf[rows, :])
+        gate = wide_buf[0, rows, :] * factor * gate_scale_ref[...][None, :]
+        up = wide_buf[1, rows, :] * factor * up_scale_ref[...][None, :]
         act = (gate / (1.0 + jnp.exp(-gate)) * up).astype(jnp.bfloat16)
-        store_shares(act, lambda at: down_buf[:, at], chunks, rows, mine_ref, theirs_ref)
+        store_shares(act, lambda at: down_buf[:, at], chunks, rows, mine_ref, theirs_ref, True)
         return carry
 
-    lax.fori_loop(0, xs[0].shape[0] // tall, block, 0)
+    lax.fori_loop(0, blocks, block, 0)
 
 
 def gain_rows(gain_ref):
@@ -251,6 +274,7 @@
     down_scale_ref,
     near_ref,
     far_ref,
+    other_ref,
 ):
     gain = gain_rows(in_gain_ref).T
     parts = [
@@ -264,9 +288,11 @@
         at += part.shape[1]
     gain = gain_rows(mid_gain_ref)[:1, :]
     hidden = gate_ref.shape[0]
-    far_ref[:hidden, :] = (gate_ref[...] * gain).astype(jnp.bfloat16)
-    far_ref[hidden : 2 * hidden, :] = (up_ref[...] * gain).astype(jnp.bfloat16)
-    far_ref[2 * hidden :, :] = (down_ref[...] * down_scale_ref[...]).astype(jnp.bfloat16)
+    even = lax.rem(lax.axis_index("grp"), 2) == 0
+    gate, up = gate_ref[...], up_ref[...]
+    far_ref[:hidden, :] = (jnp.where(even, gate, up) * gain).astype(jnp.bfloat16)
+    far_ref[hidden:, :] = (down_ref[...] * down_scale_ref[...]).astype(jnp.bfloat16)
+    other_ref[...] = (jnp.where(even, up, gate) * gain).astype(jnp.bfloat16)
 
 
 def fold(shapes, *operands):
@@ -318,15 +344,20 @@
     return call(gating_kernel, "gating", operands, specs, chunks, shards, tall, scratch, flops, 16)
 
 
-def channel(pieces, gate_scale, up_scale, ring):
+def channel(pieces, gate_scale, up_scale, ring, others):
     chunks, shards, tall = len(pieces), len(ring), 256
     rows, width = pieces[0].shape
     hidden = gate_scale.shape[0]
     model = chunks * width
     flops = 2 * rows * model * 3 * hidden
-    scratch = [(rows, model), *[(hidden, model)] * 3]
-    scratch.append(pltpu.SemaphoreType.DMA((chunks + 3 * shards,)))
-    operands = [*pieces, gate_scale, up_scale, *ring]
+    scratch = [
+        (rows, model),
+        (2, hidden, model),
+        (hidden, model),
+        pltpu.VMEM((2, rows, hidden), jnp.float32),
+        pltpu.SemaphoreType.DMA((chunks + 3 * shards,)),
+    ]
+    operands = [*pieces, gate_scale, up_scale, *ring, *others]
     specs = [pl.BlockSpec(memory_space=pl.ANY)] * len(operands)
     specs[chunks] = specs[chunks + 1] = None
     return call(channel_kernel, "channel", operands, specs, chunks, shards, tall, scratch, flops, 57)
@@ -353,8 +384,8 @@
 ):
     depth, span = w_u.shape
     hidden, out = w_down.shape
-    near, far = fold(
-        [(depth, 2 * span + w_mix.shape[1]), (3 * hidden, out)],
+    near, far, other = fold(
+        [(depth, 2 * span + w_mix.shape[1]), (2 * hidden, out), (hidden, depth)],
         mix_gain.reshape(-1, depth),
         w_u,
         w_v,
@@ -373,20 +404,27 @@
     ring = Ring(far)
     steps = ring.count // 2
     pieces = gather_features(tokens)
-    early = steps // 2
-    for _ in range(early):
-        ring.advance()
-    pieces[0], *_ = lax.optimization_barrier((pieces[0], *ring.held[-2:]))
+    others = [other]
+
+    def two_rounds():
+        new = []
+        for _ in range(2):
+            if ring.step < steps:
+                new += ring.advance()
+        swapped = swap_groups(jnp.concatenate([piece[:hidden] for piece in new], axis=0))
+        others.append(swapped)
+
+    two_rounds()
+    two_rounds()
+    pieces[0], *_ = lax.optimization_barrier((pieces[0], *ring.held[-2:], others[1]))
     mine, theirs = gating(pieces, near, spatial[0], spatial_bias)
-    ring.advance()
+    two_rounds()
     pair = chip_sums(mine, theirs)
-    ring.after(*pair[1:])
-    ring.advance()
     resid = (tokens.astype(jnp.float32) + sum_chips(pair)).astype(jnp.bfloat16)
-    ring.after(resid)
+    ring.after(others[2], *pair[1:])
     while ring.step < steps:
-        ring.advance()
-    mine, theirs = channel(gather_features(resid), gate_scale, up_scale, ring.held)
+        two_rounds()
+    mine, theirs = channel(gather_features(resid), gate_scale, up_scale, ring.held, others)
     pair = chip_sums(mine, theirs)
     return (resid.astype(jnp.float32) + sum_chips(pair)).astype(jnp.bfloat16)
 

time: 224 us -> 231 us (1.031)
  starting transfers between devices: 81.2 us -> 94.6 us
  Pallas kernels: 29.5 us -> 24.8 us
    ppermute x0 -> x4, waiting for transfers between devices: none -> 15.1 us  [swap_groups(): return lax.ppermute(x, 'grp', [(i, i ^ 1) for i in range(count)])]
    ppermute x15, waiting for transfers between devices: 44.2 us -> 35.3 us  [pass_on(): lax.ppermute(x, 'fs', [(i, (i + step) % count) for i in range(count)])]
    ppermute x12, waiting for transfers between devices: 39.9 us -> 32 us  [to_chip(): lax.ppermute(x, 'tp', [(i, (i + CORES * step) % count) for i in range(cou...]
    ppermute x0 -> x4, starting transfers between devices: none -> 5.18 us  [swap_groups(): return lax.ppermute(x, 'grp', [(i, i ^ 1) for i in range(count)])]
    pallas_call x2, Pallas kernels: 27.1 us -> 22.4 us  [call(): pl.pallas_call(functools.partial(kernel, chunks=chunks, shards=shards, ta...]
    ppermute x15, starting transfers between devices: 39 us -> 41.8 us  [pass_on(): lax.ppermute(x, 'fs', [(i, (i + step) % count) for i in range(count)])]
    ppermute x12, starting transfers between devices: 17.1 us -> 19.8 us  [to_chip(): lax.ppermute(x, 'tp', [(i, (i + CORES * step) % count) for i in range(cou...]
    ppermute x8, starting transfers between devices: 25.2 us -> 27.8 us  [swap_cores(): return lax.ppermute(x, 'tp', [(i, i ^ 1) for i in range(count)])]
  transfers between devices with their start and end apart: 36 -> 40, of which waited for: 20 -> 24; matrix products, arithmetic and copies ran while one was open for 1% -> 1% of each run, Pallas kernels for 0% -> 0%
where the time goes in v1:
time: 231 us
  starting transfers between devices  94.6 us (41%)
  waiting for transfers between devices  88.7 us (38%)
  Pallas kernels  24.8 us (11%)
  between operations  13.9 us (6%)
  other arithmetic  4.62 us (2%)
  local copies, waits for them, and re-layouts  4.31 us (2%)
    ppermute x15, starting transfers between devices, pass_on(): lax.ppermute(x, 'fs', [(i, (i + step) % count) for i in range(count)])  41.8 us
    ppermute x15, waiting for transfers between devices, pass_on(): lax.ppermute(x, 'fs', [(i, (i + step) % count) for i in range(count)])  35.3 us
    ppermute x12, waiting for transfers between devices, to_chip(): lax.ppermute(x, 'tp', [(i, (i + CORES * step) % count) for i in range(cou...  32 us
    ppermute x8, starting transfers between devices, swap_cores(): return lax.ppermute(x, 'tp', [(i, i ^ 1) for i in range(count)])  27.8 us
    pallas_call x2, Pallas kernels, call(): pl.pallas_call(functools.partial(kernel, chunks=chunks, shards=shards, ta...  22.4 us
    ppermute x12, starting transfers between devices, to_chip(): lax.ppermute(x, 'tp', [(i, (i + CORES * step) % count) for i in range(cou...  19.8 us
    ppermute x4, waiting for transfers between devices, swap_groups(): return lax.ppermute(x, 'grp', [(i, i ^ 1) for i in range(count)])  15.1 us
    ppermute x4, starting transfers between devices, swap_groups(): return lax.ppermute(x, 'grp', [(i, i ^ 1) for i in range(count)])  5.18 us
  transfers between devices with their start and end apart: 40, of which 24 were waited for; matrix products, arithmetic and copies ran while one was open for 1% of the time, Pallas kernels for 0%

profile of v1, /device:TPU:33, one launch (start us, length us, event | category | flops | bytes accessed | tf_op | source)
XLA Modules:
  0.0 231.0 jit_solution(18390266014687513812)
XLA Ops:
  6.6 2.4 %fold.1 = (bf16[128,384]{1,0:T(8,128)(2,1)}, bf16[1408,128]{1,0:T(8,128)(2,1)}, bf16[704,128]{1,0:T(8,128)(2,1)}) custom-call(f32[16,128]{1,0:T(8,128)} %bitcast.60, f32[128,128]{1,0:T(8,128)} %u_ref.1, f32[128,128]{1,0:T(8,128)} %v_ref.1, f32[128,128]{1,0:T(8,128)} %mix_ref.1, f32[1,128]{1,0:T(1,128)} %bitcast.62, f32[1,128]{1,0:T(1,128)} %bitcast.63, ...), custom_call_target="tpu_custom_call" | custom-call | flops 4194304 | bytes 1048576 | tf_op jit(solution)/shard_map/fold/pallas_call | solution.py:299
  9.0 23.0 %collective-permute-start.2 = (bf16[1408,128]{1,0:T(8,128)(2,1)}, bf16[1408,128]{1,0:T(8,128)(2,1)S(1)}, u32[]{:S(2)}, u32[]{:S(2)}) collective-permute-start(bf16[1408,128]{1,0:T(8,128)(2,1)} %get-tuple-element.29.refs_10_), channel_id=1, source_target_pairs={{0,120},{8,0},{16,8},{24,16},{32,24},{40,32},{48,40},{56,48},{64,5... | collective-permute-start | bytes 1081352 | tf_op jit(solution)/shard_map/ppermute | solution.py:62
  34.9 5.1 %collective-permute-done.2.refs_12_ = bf16[1408,128]{1,0:T(8,128)(2,1)S(1)} collective-permute-done((bf16[1408,128]{1,0:T(8,128)(2,1)}, bf16[1408,128]{1,0:T(8,128)(2,1)S(1)}, u32[]{:S(2)}, u32[]{:S(2)}) %collective-permute-start.2) | collective-permute-done | bytes 360480 | tf_op jit(solution)/shard_map/ppermute | solution.py:62
  40.0 3.4 %collective-permute-start.4 = (bf16[1408,128]{1,0:T(8,128)(2,1)S(1)}, bf16[1408,128]{1,0:T(8,128)(2,1)S(1)}, u32[]{:S(2)}, u32[]{:S(2)}) collective-permute-start(bf16[1408,128]{1,0:T(8,128)(2,1)S(1)} %collective-permute-done.2.refs_12_), channel_id=1, source_target_pairs={{0,120},{8,0},{16,8},{24,16},{32,24},{40,32},{48,40},{56,48},{64,5... | collective-permute-start | bytes 1081352 | tf_op jit(solution)/shard_map/ppermute | solution.py:62
  45.8 3.0 %collective-permute-start.13 = (bf16[768,256]{1,0:T(8,128)(2,1)S(1)}, bf16[768,256]{1,0:T(8,128)(2,1)S(1)}, u32[]{:S(2)}, u32[]{:S(2)}) collective-permute-start(bf16[768,256]{1,0:T(8,128)(2,1)S(1)} %copy-done.1), channel_id=1, source_target_pairs={{0,4},{1,5},{2,6},{3,7},{4,0},{5,1},{6,2},{7,3},{8,12},{9,13},{10,... | collective-permute-start | bytes 1179656 | tf_op jit(solution)/shard_map/ppermute | solution.py:21
  48.9 4.2 %collective-permute-done.4.refs_14_ = bf16[1408,128]{1,0:T(8,128)(2,1)S(1)} collective-permute-done((bf16[1408,128]{1,0:T(8,128)(2,1)S(1)}, bf16[1408,128]{1,0:T(8,128)(2,1)S(1)}, u32[]{:S(2)}, u32[]{:S(2)}) %collective-permute-start.4) | collective-permute-done | bytes 360480 | tf_op jit(solution)/shard_map/ppermute | solution.py:62
  53.1 3.6 %collective-permute-start.6 = (bf16[1408,128]{1,0:T(8,128)(2,1)S(1)}, bf16[1408,128]{1,0:T(8,128)(2,1)S(1)}, u32[]{:S(2)}, u32[]{:S(2)}) collective-permute-start(bf16[1408,128]{1,0:T(8,128)(2,1)S(1)} %collective-permute-done.4.refs_14_), channel_id=1, source_target_pairs={{0,120},{8,0},{16,8},{24,16},{32,24},{40,32},{48,40},{56,48},{64,5... | collective-permute-start | bytes 1081352 | tf_op jit(solution)/shard_map/ppermute | solution.py:62
  56.9 3.2 %collective-permute-start.8 = (bf16[2816,128]{1,0:T(8,128)(2,1)S(1)}, bf16[2816,128]{1,0:T(8,128)(2,1)S(1)}, u32[]{:S(2)}, u32[]{:S(2)}) collective-permute-start(bf16[2816,128]{1,0:T(8,128)(2,1)S(1)} %pad_maximum_fusion.2), channel_id=1, source_target_pairs={{0,128},{128,0},{1,129},{129,1},{2,130},{130,2},{3,131},{131,3},{4... | collective-permute-start | bytes 2162696 | tf_op jit(solution)/shard_map/ppermute | solution.py:101
  62.1 3.3 %collective-permute-done.6.refs_16_ = bf16[1408,128]{1,0:T(8,128)(2,1)S(1)} collective-permute-done((bf16[1408,128]{1,0:T(8,128)(2,1)S(1)}, bf16[1408,128]{1,0:T(8,128)(2,1)S(1)}, u32[]{:S(2)}, u32[]{:S(2)}) %collective-permute-start.6) | collective-permute-done | bytes 360480 | tf_op jit(solution)/shard_map/ppermute | solution.py:62
  65.3 3.3 %collective-permute-start.14 = (bf16[768,256]{1,0:T(8,128)(2,1)S(1)}, bf16[768,256]{1,0:T(8,128)(2,1)S(1)}, u32[]{:S(2)}, u32[]{:S(2)}) collective-permute-start(bf16[768,256]{1,0:T(8,128)(2,1)S(1)} %collective-permute-done.13.refs_4_), channel_id=1, source_target_pairs={{0,1},{1,0},{2,3},{3,2},{4,5},{5,4},{6,7},{7,6},{8,9},{9,8},{10,11... | collective-permute-start | bytes 1179656 | tf_op jit(solution)/shard_map/ppermute | solution.py:16
  68.9 3.2 %collective-permute-start.7 = (bf16[1408,128]{1,0:T(8,128)(2,1)S(1)}, bf16[1408,128]{1,0:T(8,128)(2,1)S(1)}, u32[]{:S(2)}, u32[]{:S(2)}) collective-permute-start(bf16[1408,128]{1,0:T(8,128)(2,1)S(1)} %collective-permute-done.6.refs_16_), channel_id=1, source_target_pairs={{0,120},{8,0},{16,8},{24,16},{32,24},{40,32},{48,40},{56,48},{64,5... | collective-permute-start | bytes 1081352 | tf_op jit(solution)/shard_map/ppermute | solution.py:62
  72.1 2.9 %collective-permute-done.8.refs_27_ = bf16[2816,128]{1,0:T(8,128)(2,1)S(1)} collective-permute-done((bf16[2816,128]{1,0:T(8,128)(2,1)S(1)}, bf16[2816,128]{1,0:T(8,128)(2,1)S(1)}, u32[]{:S(2)}, u32[]{:S(2)}) %collective-permute-start.8) | collective-permute-done | bytes 720928 | tf_op jit(solution)/shard_map/ppermute | solution.py:101
  75.1 8.5 %collective-permute-done.7.refs_18_ = bf16[1408,128]{1,0:T(8,128)(2,1)S(1)} collective-permute-done((bf16[1408,128]{1,0:T(8,128)(2,1)S(1)}, bf16[1408,128]{1,0:T(8,128)(2,1)S(1)}, u32[]{:S(2)}, u32[]{:S(2)}) %collective-permute-start.7) | collective-permute-done | bytes 360480 | tf_op jit(solution)/shard_map/ppermute | solution.py:62
  83.5 2.4 %collective-permute-done.5.refs_17_ = bf16[1408,128]{1,0:T(8,128)(2,1)S(1)} collective-permute-done((bf16[1408,128]{1,0:T(8,128)(2,1)S(1)}, bf16[1408,128]{1,0:T(8,128)(2,1)S(1)}, u32[]{:S(2)}, u32[]{:S(2)}) %collective-permute-start.5) | collective-permute-done | bytes 360480 | tf_op jit(solution)/shard_map/ppermute | solution.py:62
  89.2 7.2 %gating.1 = (bf16[4,768,256]{2,1,0:T(8,128)(2,1)S(1)}, bf16[4,768,256]{2,1,0:T(8,128)(2,1)S(1)}) custom-call(bf16[768,256]{1,0:T(8,128)(2,1)S(1)} %copy-done.1, bf16[768,256]{1,0:T(8,128)(2,1)S(1)} %collective-permute-done.9.refs_1_, bf16[768,256]{1,0:T(8,128)(2,1)S(1)} %collective-permute-done.10.refs_2_, bf16[768,256]{1,0:T(8,128)(2,1)S(1)} %get-tuple-element.60.refs_3_, ...), custom_call_target="tpu_custom_call" | custom-call | flops 1233125376 | bytes 1048576 | tf_op jit(solution)/shard_map/gating/pallas_call | solution.py:315
  96.4 9.2 %collective-permute-start.15 = (bf16[4,768,256]{2,1,0:T(8,128)(2,1)S(1)}, bf16[4,768,256]{2,1,0:T(8,128)(2,1)S(1)}, u32[]{:S(2)}, u32[]{:S(2)}) collective-permute-start(bf16[4,768,256]{2,1,0:T(8,128)(2,1)S(1)} %get-tuple-element.39), channel_id=1, source_target_pairs={{0,1},{1,0},{2,3},{3,2},{4,5},{5,4},{6,7},{7,6},{8,9},{9,8},{10,11... | collective-permute-start | bytes 4718600 | tf_op jit(solution)/shard_map/ppermute | solution.py:16
  111.9 2.4 %collective-permute-start.17 = (bf16[768,256]{1,0:T(8,128)(2,1)S(1)}, bf16[768,256]{1,0:T(8,128)(2,1)S(1)}, u32[]{:S(2)}, u32[]{:S(2)}) collective-permute-start(bf16[768,256]{1,0:T(8,128)(2,1)S(1)} %get-tuple-element.56), channel_id=1, source_target_pairs={{0,4},{1,5},{2,6},{3,7},{4,0},{5,1},{6,2},{7,3},{8,12},{9,13},{10,... | collective-permute-start | bytes 1179656 | tf_op jit(solution)/shard_map/ppermute | solution.py:21
  118.0 3.1 %collective-permute-done.16 = bf16[768,256]{1,0:T(8,128)(2,1)S(1)} collective-permute-done((bf16[768,256]{1,0:T(8,128)(2,1)S(1)}, bf16[768,256]{1,0:T(8,128)(2,1)S(1)}, u32[]{:S(2)}, u32[]{:S(2)}) %collective-permute-start.16) | collective-permute-done | bytes 393248 | tf_op jit(solution)/shard_map/ppermute | solution.py:21
  121.6 8.8 %collective-permute-done.17 = bf16[768,256]{1,0:T(8,128)(2,1)S(1)} collective-permute-done((bf16[768,256]{1,0:T(8,128)(2,1)S(1)}, bf16[768,256]{1,0:T(8,128)(2,1)S(1)}, u32[]{:S(2)}, u32[]{:S(2)}) %collective-permute-start.17) | collective-permute-done | bytes 393248 | tf_op jit(solution)/shard_map/ppermute | solution.py:21
  131.4 2.3 collective-permute-start.20
  137.4 6.4 %collective-permute-done.28.refs_22_ = bf16[1408,128]{1,0:T(8,128)(2,1)S(1)} collective-permute-done((bf16[1408,128]{1,0:T(8,128)(2,1)S(1)}, bf16[1408,128]{1,0:T(8,128)(2,1)S(1)}, u32[]{:S(2)}, u32[]{:S(2)}) %collective-permute-start.28) | collective-permute-done | bytes 360480 | tf_op jit(solution)/shard_map/ppermute | solution.py:62
  143.8 3.3 %collective-permute-start.31 = (bf16[1408,128]{1,0:T(8,128)(2,1)S(1)}, bf16[1408,128]{1,0:T(8,128)(2,1)S(1)}, u32[]{:S(2)}, u32[]{:S(2)}) collective-permute-start(bf16[1408,128]{1,0:T(8,128)(2,1)S(1)} %collective-permute-done.28.refs_22_), channel_id=1, source_target_pairs={{0,120},{8,0},{16,8},{24,16},{32,24},{40,32},{48,40},{56,48},{64,5... | collective-permute-start | bytes 1081352 | tf_op jit(solution)/shard_map/ppermute | solution.py:62
  147.7 2.5 %collective-permute-start.22 = (bf16[2,768,256]{2,1,0:T(8,128)(2,1)S(1)}, bf16[2,768,256]{2,1,0:T(8,128)(2,1)S(1)}, u32[]{:S(2)}, u32[]{:S(2)}) collective-permute-start(bf16[2,768,256]{2,1,0:T(8,128)(2,1)S(1)} %pad_maximum_fusion.1), channel_id=1, source_target_pairs={{0,1},{1,0},{2,3},{3,2},{4,5},{5,4},{6,7},{7,6},{8,9},{9,8},{10,11... | collective-permute-start | bytes 2359304 | tf_op jit(solution)/shard_map/ppermute | solution.py:16
  150.6 2.2 collective-permute-done.31.refs_24_
  156.7 3.5 %collective-permute-start.19 = (bf16[768,256]{1,0:T(8,128)(2,1)S(1)}, bf16[768,256]{1,0:T(8,128)(2,1)S(1)}, u32[]{:S(2)}, u32[]{:S(2)}) collective-permute-start(bf16[768,256]{1,0:T(8,128)(2,1)S(1)} %fusion.7.refs_0_), channel_id=1, source_target_pairs={{0,1},{1,0},{2,3},{3,2},{4,5},{5,4},{6,7},{7,6},{8,9},{9,8},{10,11... | collective-permute-start | bytes 1179656 | tf_op jit(solution)/shard_map/ppermute | solution.py:16
  162.2 3.8 %collective-permute-start.24 = (bf16[768,256]{1,0:T(8,128)(2,1)S(1)}, bf16[768,256]{1,0:T(8,128)(2,1)S(1)}, u32[]{:S(2)}, u32[]{:S(2)}) collective-permute-start(bf16[768,256]{1,0:T(8,128)(2,1)S(1)} %collective-permute-done.23.refs_4_), channel_id=1, source_target_pairs={{0,1},{1,0},{2,3},{3,2},{4,5},{5,4},{6,7},{7,6},{8,9},{9,8},{10,11... | collective-permute-start | bytes 1179656 | tf_op jit(solution)/shard_map/ppermute | solution.py:16
  167.8 11.6 %collective-permute-done.34.refs_30_ = bf16[2112,128]{1,0:T(8,128)(2,1)S(1)} collective-permute-done((bf16[2112,128]{1,0:T(8,128)(2,1)S(1)}, bf16[2112,128]{1,0:T(8,128)(2,1)S(1)}, u32[]{:S(2)}, u32[]{:S(2)}) %collective-permute-start.34) | collective-permute-done | bytes 540704 | tf_op jit(solution)/shard_map/ppermute | solution.py:101
  180.1 15.2 %channel.1 = (bf16[4,768,256]{2,1,0:T(8,128)(2,1)}, bf16[4,768,256]{2,1,0:T(8,128)(2,1)}) custom-call(bf16[768,256]{1,0:T(8,128)(2,1)} %copy-done.4, bf16[768,256]{1,0:T(8,128)(2,1)} %copy-done.32, bf16[768,256]{1,0:T(8,128)(2,1)} %copy-done.8, bf16[768,256]{1,0:T(8,128)(2,1)} %get-tuple-element.58.refs_3_, bf16[768,256]{1,0:T(8,128)(2,1)} %copy-done.31, ...), custom_call_target="tpu_custom_call" | custom-call | flops 6643777536 | bytes 1048576 | tf_op jit(solution)/shard_map/channel/pallas_call | solution.py:315
  196.8 3.2 %collective-permute-done.35 = bf16[4,768,256]{2,1,0:T(8,128)(2,1)S(1)} collective-permute-done((bf16[4,768,256]{2,1,0:T(8,128)(2,1)}, bf16[4,768,256]{2,1,0:T(8,128)(2,1)S(1)}, u32[]{:S(2)}, u32[]{:S(2)}) %collective-permute-start.35) | collective-permute-done | bytes 1572896 | tf_op jit(solution)/shard_map/ppermute | solution.py:16
  202.0 2.2 collective-permute-start.37
  205.0 8.5 %collective-permute-done.36 = bf16[768,256]{1,0:T(8,128)(2,1)S(1)} collective-permute-done((bf16[768,256]{1,0:T(8,128)(2,1)S(1)}, bf16[768,256]{1,0:T(8,128)(2,1)S(1)}, u32[]{:S(2)}, u32[]{:S(2)}) %collective-permute-start.36) | collective-permute-done | bytes 393248 | tf_op jit(solution)/shard_map/ppermute | solution.py:21
  213.5 8.0 %collective-permute-done.37 = bf16[768,256]{1,0:T(8,128)(2,1)S(1)} collective-permute-done((bf16[768,256]{1,0:T(8,128)(2,1)S(1)}, bf16[768,256]{1,0:T(8,128)(2,1)S(1)}, u32[]{:S(2)}, u32[]{:S(2)}) %collective-permute-start.37) | collective-permute-done | bytes 393248 | tf_op jit(solution)/shard_map/ppermute | solution.py:21
  (148 shorter events, 42.0 us)
Async XLA Ops:
  6.5 81.2 %all-gather.3.cloned.1.call-start = ((), (), s32[]{:S(2)}) async-start(), calls=%async_computation | async-start | bytes 1671168 | tf_op jit(solution)/shard_map/all_gather | solution.py:403
  9.0 31.0 %collective-permute-start.2 = (bf16[1408,128]{1,0:T(8,128)(2,1)}, bf16[1408,128]{1,0:T(8,128)(2,1)S(1)}, u32[]{:S(2)}, u32[]{:S(2)}) collective-permute-start(bf16[1408,128]{1,0:T(8,128)(2,1)} %get-tuple-element.29.refs_10_), channel_id=1, source_target_pairs={{0,120},{8,0},{16,8},{24,16},{32,24},{40,32},{48,40},{56,48},{64,5... | collective-permute-start | bytes 1081352 | tf_op jit(solution)/shard_map/ppermute | solution.py:62
  32.0 11.4 %collective-permute-start = (bf16[1408,128]{1,0:T(8,128)(2,1)}, bf16[1408,128]{1,0:T(8,128)(2,1)S(1)}, u32[]{:S(2)}, u32[]{:S(2)}) collective-permute-start(bf16[1408,128]{1,0:T(8,128)(2,1)} %get-tuple-element.29.refs_10_), channel_id=1, source_target_pairs={{0,8},{8,16},{16,24},{24,32},{32,40},{40,48},{48,56},{56,64},{64,7... | collective-permute-start | bytes 1081352 | tf_op jit(solution)/shard_map/ppermute | solution.py:62
  32.0 11.7 %collective-permute-start.10 = (bf16[768,256]{1,0:T(8,128)(2,1)}, bf16[768,256]{1,0:T(8,128)(2,1)S(1)}, u32[]{:S(2)}, u32[]{:S(2)}) collective-permute-start(bf16[768,256]{1,0:T(8,128)(2,1)} %refs_0_), channel_id=1, source_target_pairs={{0,2},{1,3},{2,4},{3,5},{4,6},{5,7},{6,0},{7,1},{8,10},{9,11},{10,... | collective-permute-start | bytes 1179656 | tf_op jit(solution)/shard_map/ppermute | solution.py:21
  40.0 13.2 %collective-permute-start.4 = (bf16[1408,128]{1,0:T(8,128)(2,1)S(1)}, bf16[1408,128]{1,0:T(8,128)(2,1)S(1)}, u32[]{:S(2)}, u32[]{:S(2)}) collective-permute-start(bf16[1408,128]{1,0:T(8,128)(2,1)S(1)} %collective-permute-done.2.refs_12_), channel_id=1, source_target_pairs={{0,120},{8,0},{16,8},{24,16},{32,24},{40,32},{48,40},{56,48},{64,5... | collective-permute-start | bytes 1081352 | tf_op jit(solution)/shard_map/ppermute | solution.py:62
  43.4 13.4 %collective-permute-start.1 = (bf16[1408,128]{1,0:T(8,128)(2,1)S(1)}, bf16[1408,128]{1,0:T(8,128)(2,1)S(1)}, u32[]{:S(2)}, u32[]{:S(2)}) collective-permute-start(bf16[1408,128]{1,0:T(8,128)(2,1)S(1)} %collective-permute-done.refs_11_), channel_id=1, source_target_pairs={{0,8},{8,16},{16,24},{24,32},{32,40},{40,48},{48,56},{56,64},{64,7... | collective-permute-start | bytes 1081352 | tf_op jit(solution)/shard_map/ppermute | solution.py:62
  43.8 28.2 %collective-permute-start.12 = (bf16[2,768,256]{2,1,0:T(8,128)(2,1)S(1)}, bf16[2,768,256]{2,1,0:T(8,128)(2,1)S(1)}, u32[]{:S(2)}, u32[]{:S(2)}) collective-permute-start(bf16[2,768,256]{2,1,0:T(8,128)(2,1)S(1)} %pad_maximum_fusion), channel_id=1, source_target_pairs={{0,1},{1,0},{2,3},{3,2},{4,5},{5,4},{6,7},{7,6},{8,9},{9,8},{10,11... | collective-permute-start | bytes 2359304 | tf_op jit(solution)/shard_map/ppermute | solution.py:16
  45.8 14.3 %collective-permute-start.13 = (bf16[768,256]{1,0:T(8,128)(2,1)S(1)}, bf16[768,256]{1,0:T(8,128)(2,1)S(1)}, u32[]{:S(2)}, u32[]{:S(2)}) collective-permute-start(bf16[768,256]{1,0:T(8,128)(2,1)S(1)} %copy-done.1), channel_id=1, source_target_pairs={{0,4},{1,5},{2,6},{3,7},{4,0},{5,1},{6,2},{7,3},{8,12},{9,13},{10,... | collective-permute-start | bytes 1179656 | tf_op jit(solution)/shard_map/ppermute | solution.py:21
  53.1 12.2 %collective-permute-start.6 = (bf16[1408,128]{1,0:T(8,128)(2,1)S(1)}, bf16[1408,128]{1,0:T(8,128)(2,1)S(1)}, u32[]{:S(2)}, u32[]{:S(2)}) collective-permute-start(bf16[1408,128]{1,0:T(8,128)(2,1)S(1)} %collective-permute-done.4.refs_14_), channel_id=1, source_target_pairs={{0,120},{8,0},{16,8},{24,16},{32,24},{40,32},{48,40},{56,48},{64,5... | collective-permute-start | bytes 1081352 | tf_op jit(solution)/shard_map/ppermute | solution.py:62
  56.8 12.1 %collective-permute-start.3 = (bf16[1408,128]{1,0:T(8,128)(2,1)S(1)}, bf16[1408,128]{1,0:T(8,128)(2,1)S(1)}, u32[]{:S(2)}, u32[]{:S(2)}) collective-permute-start(bf16[1408,128]{1,0:T(8,128)(2,1)S(1)} %collective-permute-done.1.refs_13_), channel_id=1, source_target_pairs={{0,8},{8,16},{16,24},{24,32},{32,40},{40,48},{48,56},{56,64},{64,7... | collective-permute-start | bytes 1081352 | tf_op jit(solution)/shard_map/ppermute | solution.py:62
  56.9 18.1 %collective-permute-start.8 = (bf16[2816,128]{1,0:T(8,128)(2,1)S(1)}, bf16[2816,128]{1,0:T(8,128)(2,1)S(1)}, u32[]{:S(2)}, u32[]{:S(2)}) collective-permute-start(bf16[2816,128]{1,0:T(8,128)(2,1)S(1)} %pad_maximum_fusion.2), channel_id=1, source_target_pairs={{0,128},{128,0},{1,129},{129,1},{2,130},{130,2},{3,131},{131,3},{4... | collective-permute-start | bytes 2162696 | tf_op jit(solution)/shard_map/ppermute | solution.py:101
  60.1 25.8 %collective-permute-start.9 = (bf16[768,256]{1,0:T(8,128)(2,1)S(1)}, bf16[768,256]{1,0:T(8,128)(2,1)S(1)}, u32[]{:S(2)}, u32[]{:S(2)}) collective-permute-start(bf16[768,256]{1,0:T(8,128)(2,1)S(1)} %copy-done.1), channel_id=1, source_target_pairs={{0,1},{1,0},{2,3},{3,2},{4,5},{5,4},{6,7},{7,6},{8,9},{9,8},{10,11... | collective-permute-start | bytes 1179656 | tf_op jit(solution)/shard_map/ppermute | solution.py:16
  65.3 21.3 %collective-permute-start.14 = (bf16[768,256]{1,0:T(8,128)(2,1)S(1)}, bf16[768,256]{1,0:T(8,128)(2,1)S(1)}, u32[]{:S(2)}, u32[]{:S(2)}) collective-permute-start(bf16[768,256]{1,0:T(8,128)(2,1)S(1)} %collective-permute-done.13.refs_4_), channel_id=1, source_target_pairs={{0,1},{1,0},{2,3},{3,2},{4,5},{5,4},{6,7},{7,6},{8,9},{9,8},{10,11... | collective-permute-start | bytes 1179656 | tf_op jit(solution)/shard_map/ppermute | solution.py:16
  68.9 14.6 %collective-permute-start.7 = (bf16[1408,128]{1,0:T(8,128)(2,1)S(1)}, bf16[1408,128]{1,0:T(8,128)(2,1)S(1)}, u32[]{:S(2)}, u32[]{:S(2)}) collective-permute-start(bf16[1408,128]{1,0:T(8,128)(2,1)S(1)} %collective-permute-done.6.refs_16_), channel_id=1, source_target_pairs={{0,120},{8,0},{16,8},{24,16},{32,24},{40,32},{48,40},{56,48},{64,5... | collective-permute-start | bytes 1081352 | tf_op jit(solution)/shard_map/ppermute | solution.py:62
  72.1 13.8 %collective-permute-start.5 = (bf16[1408,128]{1,0:T(8,128)(2,1)S(1)}, bf16[1408,128]{1,0:T(8,128)(2,1)S(1)}, u32[]{:S(2)}, u32[]{:S(2)}) collective-permute-start(bf16[1408,128]{1,0:T(8,128)(2,1)S(1)} %collective-permute-done.3.refs_15_), channel_id=1, source_target_pairs={{0,8},{8,16},{16,24},{24,32},{32,40},{40,48},{48,56},{56,64},{64,7... | collective-permute-start | bytes 1081352 | tf_op jit(solution)/shard_map/ppermute | solution.py:62
  96.4 12.3 %collective-permute-start.15 = (bf16[4,768,256]{2,1,0:T(8,128)(2,1)S(1)}, bf16[4,768,256]{2,1,0:T(8,128)(2,1)S(1)}, u32[]{:S(2)}, u32[]{:S(2)}) collective-permute-start(bf16[4,768,256]{2,1,0:T(8,128)(2,1)S(1)} %get-tuple-element.39), channel_id=1, source_target_pairs={{0,1},{1,0},{2,3},{3,2},{4,5},{5,4},{6,7},{7,6},{8,9},{9,8},{10,11... | collective-permute-start | bytes 4718600 | tf_op jit(solution)/shard_map/ppermute | solution.py:16
  105.7 11.3 %collective-permute-start.25 = (bf16[1408,128]{1,0:T(8,128)(2,1)S(1)}, bf16[1408,128]{1,0:T(8,128)(2,1)S(1)}, u32[]{:S(2)}, u32[]{:S(2)}) collective-permute-start(bf16[1408,128]{1,0:T(8,128)(2,1)S(1)} %copy-done.19), channel_id=1, source_target_pairs={{0,8},{8,16},{16,24},{24,32},{32,40},{40,48},{48,56},{56,64},{64,7... | collective-permute-start | bytes 1081352 | tf_op jit(solution)/shard_map/ppermute | solution.py:62
  109.0 12.1 %collective-permute-start.16 = (bf16[768,256]{1,0:T(8,128)(2,1)S(1)}, bf16[768,256]{1,0:T(8,128)(2,1)S(1)}, u32[]{:S(2)}, u32[]{:S(2)}) collective-permute-start(bf16[768,256]{1,0:T(8,128)(2,1)S(1)} %get-tuple-element.54), channel_id=1, source_target_pairs={{0,2},{1,3},{2,4},{3,5},{4,6},{5,7},{6,0},{7,1},{8,10},{9,11},{10,... | collective-permute-start | bytes 1179656 | tf_op jit(solution)/shard_map/ppermute | solution.py:21
  110.4 26.8 %collective-permute-start.29 = (bf16[2816,128]{1,0:T(8,128)(2,1)S(1)}, bf16[2816,128]{1,0:T(8,128)(2,1)S(1)}, u32[]{:S(2)}, u32[]{:S(2)}) collective-permute-start(bf16[2816,128]{1,0:T(8,128)(2,1)S(1)} %pad_maximum_fusion.3), channel_id=1, source_target_pairs={{0,128},{128,0},{1,129},{129,1},{2,130},{130,2},{3,131},{131,3},{4... | collective-permute-start | bytes 2162696 | tf_op jit(solution)/shard_map/ppermute | solution.py:101
  111.9 18.6 %collective-permute-start.17 = (bf16[768,256]{1,0:T(8,128)(2,1)S(1)}, bf16[768,256]{1,0:T(8,128)(2,1)S(1)}, u32[]{:S(2)}, u32[]{:S(2)}) collective-permute-start(bf16[768,256]{1,0:T(8,128)(2,1)S(1)} %get-tuple-element.56), channel_id=1, source_target_pairs={{0,4},{1,5},{2,6},{3,7},{4,0},{5,1},{6,2},{7,3},{8,12},{9,13},{10,... | collective-permute-start | bytes 1179656 | tf_op jit(solution)/shard_map/ppermute | solution.py:21
  114.2 16.9 %collective-permute-start.18 = (bf16[768,256]{1,0:T(8,128)(2,1)S(1)}, bf16[768,256]{1,0:T(8,128)(2,1)S(1)}, u32[]{:S(2)}, u32[]{:S(2)}) collective-permute-start(bf16[768,256]{1,0:T(8,128)(2,1)S(1)} %get-tuple-element.55), channel_id=1, source_target_pairs={{0,6},{1,7},{2,0},{3,1},{4,2},{5,3},{6,4},{7,5},{8,14},{9,15},{10,... | collective-permute-start | bytes 1179656 | tf_op jit(solution)/shard_map/ppermute | solution.py:21
  117.0 18.1 %collective-permute-start.26 = (bf16[1408,128]{1,0:T(8,128)(2,1)S(1)}, bf16[1408,128]{1,0:T(8,128)(2,1)S(1)}, u32[]{:S(2)}, u32[]{:S(2)}) collective-permute-start(bf16[1408,128]{1,0:T(8,128)(2,1)S(1)} %copy-done.7), channel_id=1, source_target_pairs={{0,120},{8,0},{16,8},{24,16},{32,24},{40,32},{48,40},{56,48},{64,5... | collective-permute-start | bytes 1081352 | tf_op jit(solution)/shard_map/ppermute | solution.py:62
  121.1 16.1 %collective-permute-start.27 = (bf16[1408,128]{1,0:T(8,128)(2,1)S(1)}, bf16[1408,128]{1,0:T(8,128)(2,1)S(1)}, u32[]{:S(2)}, u32[]{:S(2)}) collective-permute-start(bf16[1408,128]{1,0:T(8,128)(2,1)S(1)} %collective-permute-done.25.refs_19_), channel_id=1, source_target_pairs={{0,8},{8,16},{16,24},{24,32},{32,40},{40,48},{48,56},{56,64},{64,7... | collective-permute-start | bytes 1081352 | tf_op jit(solution)/shard_map/ppermute | solution.py:62
  131.4 16.1 %collective-permute-start.20 = (bf16[768,256]{1,0:T(8,128)(2,1)S(1)}, bf16[768,256]{1,0:T(8,128)(2,1)S(1)}, u32[]{:S(2)}, u32[]{:S(2)}) collective-permute-start(bf16[768,256]{1,0:T(8,128)(2,1)S(1)} %fusion.7.refs_0_), channel_id=1, source_target_pairs={{0,2},{1,3},{2,4},{3,5},{4,6},{5,7},{6,0},{7,1},{8,10},{9,11},{10,... | collective-permute-start | bytes 1179656 | tf_op jit(solution)/shard_map/ppermute | solution.py:21
  133.7 13.9 %collective-permute-start.21 = (bf16[768,256]{1,0:T(8,128)(2,1)S(1)}, bf16[768,256]{1,0:T(8,128)(2,1)S(1)}, u32[]{:S(2)}, u32[]{:S(2)}) collective-permute-start(bf16[768,256]{1,0:T(8,128)(2,1)S(1)} %fusion.7.refs_0_), channel_id=1, source_target_pairs={{0,6},{1,7},{2,0},{3,1},{4,2},{5,3},{6,4},{7,5},{8,14},{9,15},{10,... | collective-permute-start | bytes 1179656 | tf_op jit(solution)/shard_map/ppermute | solution.py:21
  147.7 18.3 %collective-permute-start.22 = (bf16[2,768,256]{2,1,0:T(8,128)(2,1)S(1)}, bf16[2,768,256]{2,1,0:T(8,128)(2,1)S(1)}, u32[]{:S(2)}, u32[]{:S(2)}) collective-permute-start(bf16[2,768,256]{2,1,0:T(8,128)(2,1)S(1)} %pad_maximum_fusion.1), channel_id=1, source_target_pairs={{0,1},{1,0},{2,3},{3,2},{4,5},{5,4},{6,7},{7,6},{8,9},{9,8},{10,11... | collective-permute-start | bytes 2359304 | tf_op jit(solution)/shard_map/ppermute | solution.py:16
  150.3 17.4 %collective-permute-start.33 = (bf16[2816,128]{1,0:T(8,128)(2,1)S(1)}, bf16[2816,128]{1,0:T(8,128)(2,1)S(1)}, u32[]{:S(2)}, u32[]{:S(2)}) collective-permute-start(bf16[2816,128]{1,0:T(8,128)(2,1)S(1)} %pad_maximum_fusion.4), channel_id=1, source_target_pairs={{0,128},{128,0},{1,129},{129,1},{2,130},{130,2},{3,131},{131,3},{4... | collective-permute-start | bytes 2162696 | tf_op jit(solution)/shard_map/ppermute | solution.py:101
  156.4 22.9 %collective-permute-start.34 = (bf16[2112,128]{1,0:T(8,128)(2,1)S(1)}, bf16[2112,128]{1,0:T(8,128)(2,1)S(1)}, u32[]{:S(2)}, u32[]{:S(2)}) collective-permute-start(bf16[2112,128]{1,0:T(8,128)(2,1)S(1)} %pad_maximum_fusion.5), channel_id=1, source_target_pairs={{0,128},{128,0},{1,129},{129,1},{2,130},{130,2},{3,131},{131,3},{4... | collective-permute-start | bytes 1622024 | tf_op jit(solution)/shard_map/ppermute | solution.py:101
  156.7 11.1 %collective-permute-start.19 = (bf16[768,256]{1,0:T(8,128)(2,1)S(1)}, bf16[768,256]{1,0:T(8,128)(2,1)S(1)}, u32[]{:S(2)}, u32[]{:S(2)}) collective-permute-start(bf16[768,256]{1,0:T(8,128)(2,1)S(1)} %fusion.7.refs_0_), channel_id=1, source_target_pairs={{0,1},{1,0},{2,3},{3,2},{4,5},{5,4},{6,7},{7,6},{8,9},{9,8},{10,11... | collective-permute-start | bytes 1179656 | tf_op jit(solution)/shard_map/ppermute | solution.py:16
  201.6 11.9 %collective-permute-start.36 = (bf16[768,256]{1,0:T(8,128)(2,1)S(1)}, bf16[768,256]{1,0:T(8,128)(2,1)S(1)}, u32[]{:S(2)}, u32[]{:S(2)}) collective-permute-start(bf16[768,256]{1,0:T(8,128)(2,1)S(1)} %get-tuple-element.51), channel_id=1, source_target_pairs={{0,2},{1,3},{2,4},{3,5},{4,6},{5,7},{6,0},{7,1},{8,10},{9,11},{10,... | collective-permute-start | bytes 1179656 | tf_op jit(solution)/shard_map/ppermute | solution.py:21
  202.0 19.5 %collective-permute-start.37 = (bf16[768,256]{1,0:T(8,128)(2,1)S(1)}, bf16[768,256]{1,0:T(8,128)(2,1)S(1)}, u32[]{:S(2)}, u32[]{:S(2)}) collective-permute-start(bf16[768,256]{1,0:T(8,128)(2,1)S(1)} %get-tuple-element.53), channel_id=1, source_target_pairs={{0,4},{1,5},{2,6},{3,7},{4,0},{5,1},{6,2},{7,3},{8,12},{9,13},{10,... | collective-permute-start | bytes 1179656 | tf_op jit(solution)/shard_map/ppermute | solution.py:21
  204.2 17.8 %collective-permute-start.38 = (bf16[768,256]{1,0:T(8,128)(2,1)S(1)}, bf16[768,256]{1,0:T(8,128)(2,1)S(1)}, u32[]{:S(2)}, u32[]{:S(2)}) collective-permute-start(bf16[768,256]{1,0:T(8,128)(2,1)S(1)} %get-tuple-element.52), channel_id=1, source_target_pairs={{0,6},{1,7},{2,0},{3,1},{4,2},{5,3},{6,4},{7,5},{8,14},{9,15},{10,... | collective-permute-start | bytes 1179656 | tf_op jit(solution)/shard_map/ppermute | solution.py:21
  (43 other events, 561.8 us)
Sparse Core Ops, SparseCore 0:
  9.1 78.5 all-gather.2

commit v2 on v0

--- a/solution.py
+++ b/solution.py
@@ -21,12 +21,16 @@
     return lax.ppermute(x, "tp", [(i, (i + CORES * step) % count) for i in range(count)])
 
 
-def gather_features(shard):
+def gather_features(shard, together=False):
     chips = lax.axis_size("tp") // CORES
-    got = [to_chip(shard, step) for step in range(1, chips)]
-    near = swap_cores(jnp.stack([got[0], got[-1]]))
-    swapped = [near[0], *[swap_cores(g) for g in got[1:-1]], near[1]]
-    return [shard, swap_cores(shard), *[p for pair in zip(got, swapped) for p in pair]]
+    got = [shard]
+    got += [to_chip(shard, step) for step in range(1, chips)]
+    if together:
+        other = swap_cores(jnp.stack(got[1:]))
+        swapped = [swap_cores(shard), *[other[i] for i in range(chips - 1)]]
+    else:
+        swapped = [swap_cores(g) for g in got]
+    return [piece for pair in zip(got, swapped) for piece in pair]
 
 
 def chunk_order(me, count):
@@ -69,9 +73,6 @@
         self.held = [shard]
         self.before = [shard, shard]
         self.step = 0
-
-    def after(self, *others):
-        self.ahead, *_ = lax.optimization_barrier((self.ahead, *others))
 
     def advance(self):
         self.step += 1
@@ -128,7 +129,7 @@
     return lax.rsqrt(jnp.mean(wide * wide, axis=1, keepdims=True) + eps)
 
 
-def store_shares(value, weights, chunks, rows, mine_ref, theirs_ref):
+def store_shares(value, weights, chunks, rows, mine_ref, theirs_ref, unroll=False):
     width = mine_ref.shape[2]
     chips = chunks // CORES
     me = lax.axis_index("tp")
@@ -141,41 +142,43 @@
             ref[step, rows, :] = dot_f32(value, w).astype(jnp.bfloat16)
             return carry
 
-        lax.fori_loop(0, chips, share, 0)
+        lax.fori_loop(0, chips, share, 0, unroll=unroll)
 
     fill(mine_ref, core)
     fill(theirs_ref, 1 - core)
 
 
+def take_rows(xs, places, rows, buf):
+    width = xs[0].shape[1]
+    squares = None
+    for place, x_ref in zip(places, xs):
+        x = x_ref[rows, :]
+        buf[:, lane_block(place, width)] = x
+        wide = x.astype(jnp.float32)
+        sq = jnp.sum(wide * wide, axis=1, keepdims=True)
+        squares = sq if squares is None else squares + sq
+    return lax.rsqrt(squares * (1.0 / (len(xs) * width)) + eps)
+
+
 def gating_kernel(*refs, chunks, shards, tall):
-    xs, refs = refs[:chunks], refs[chunks:]
-    near_ref, spatial_ref, bias_ref, mine_ref, theirs_ref, x_buf, in_buf, out_buf, sems = refs
+    xs, ws = refs[:chunks], refs[chunks : chunks + shards]
+    spatial_ref, bias_ref, mine_ref, theirs_ref, x_buf, in_buf, out_buf = refs[chunks + shards :]
     span = spatial_ref.shape[0]
-    lanes = near_ref.shape[2] - 2 * span
-    x_here, at = load_rows(xs, x_buf, sems, 0)
-    in_here, at = copy_all([(near_ref.at[:, :, : 2 * span], in_buf)], sems, at)
-    out_here, at = copy_all(
-        [
-            (near_ref.at[z, :, 2 * span :], out_buf.at[:, z * lanes : (z + 1) * lanes])
-            for z in range(shards)
-        ],
-        sems,
-        at,
-    )
+    depth = ws[0].shape[0]
+    sources = chunk_order(lax.axis_index("tp"), chunks)
+    for z, w in zip(ring_order(lax.axis_index("fs"), shards), ws):
+        in_buf[lane_block(z, depth), :] = w[:, : 2 * span]
+        out_buf[:, lane_block(z, w.shape[1] - 2 * span)] = w[:, 2 * span :]
     later = lax.broadcasted_iota(jnp.int32, (span, span), 0)
     earlier = lax.broadcasted_iota(jnp.int32, (span, span), 1)
     bias = jnp.broadcast_to(bias_ref[...], (span, span)).T
     mixing = spatial_ref[...]
     mixing = jnp.where(later >= earlier, mixing, jnp.zeros_like(mixing))
-    x_here()
-    in_here()
-    out_here()
 
     def block(i, carry):
         rows = pl.ds(pl.multiple_of(i * tall, tall), tall)
-        x = x_buf[rows, :]
-        weights = in_buf[...].reshape(x.shape[1], 2 * span)
-        pre = dot_f32(x, weights) * row_factor(x)
+        factor = take_rows(xs, sources, rows, x_buf)
+        pre = dot_f32(x_buf[...], in_buf[...]) * factor
         act = 0.5 * pre * (1.0 + lax.erf(pre * (0.5**0.5)))
         u = act[:, :span]
         v = act[:, span:].astype(jnp.bfloat16)
@@ -193,42 +196,54 @@
 
 def channel_kernel(*refs, chunks, shards, tall):
     xs, refs = refs[:chunks], refs[chunks:]
-    gate_scale_ref, up_scale_ref, refs = *refs[:2], refs[2:]
-    ring, refs = refs[:shards], refs[shards:]
-    mine_ref, theirs_ref, x_buf, gate_buf, up_buf, down_buf, sems = refs
-    lanes = ring[0].shape[1]
+    gate_scale_ref, up_scale_ref, far_ref, mine_ref, theirs_ref = refs[:5]
+    x_buf, first_buf, down_buf, wide_buf, sems = refs[5:]
+    lanes = far_ref.shape[2]
     hidden = down_buf.shape[0]
-    around = ring_order(lax.axis_index("fs"), shards)
 
     def load(part, buf, base):
         rows = slice(part * hidden, (part + 1) * hidden)
         return copy_all(
-            [(w.at[rows, :], buf.at[:, lane_block(z, lanes)]) for z, w in zip(around, ring)],
+            [
+                (far_ref.at[z, rows, :], buf.at[:, z * lanes : (z + 1) * lanes])
+                for z in range(shards)
+            ],
             sems,
             base,
         )
 
     x_here, at = load_rows(xs, x_buf, sems, 0)
-    gate_here, at = load(0, gate_buf, at)
-    up_here, at = load(1, up_buf, at)
+    gate_here, at = load(0, first_buf.at[0], at)
+    up_here, at = load(1, first_buf.at[1], at)
     down_here, at = load(2, down_buf, at)
     across = (((1,), (1,)), ((), ()))
+    blocks = xs[0].shape[0] // tall
     x_here()
     gate_here()
-    up_here()
+
+    def project(step, carry):
+        pl.when(step == 1)(up_here)
+
+        def block(i, carry):
+            rows = pl.ds(pl.multiple_of(i * tall, tall), tall)
+            wide_buf[step, rows, :] = dot_f32(x_buf[rows, :], first_buf[step], across)
+            return carry
+
+        return lax.fori_loop(0, blocks, block, carry)
+
+    lax.fori_loop(0, 2, project, 0)
     down_here()
 
     def block(i, carry):
         rows = pl.ds(pl.multiple_of(i * tall, tall), tall)
-        x = x_buf[rows, :]
-        factor = row_factor(x)
-        gate = dot_f32(x, gate_buf[...], across) * factor * gate_scale_ref[...][None, :]
-        up = dot_f32(x, up_buf[...], across) * factor * up_scale_ref[...][None, :]
+        factor = row_factor(x_buf[rows, :])
+        gate = wide_buf[0, rows, :] * factor * gate_scale_ref[...][None, :]
+        up = wide_buf[1, rows, :] * factor * up_scale_ref[...][None, :]
         act = (gate / (1.0 + jnp.exp(-gate)) * up).astype(jnp.bfloat16)
-        store_shares(act, lambda at: down_buf[:, at], chunks, rows, mine_ref, theirs_ref)
+        store_shares(act, lambda at: down_buf[:, at], chunks, rows, mine_ref, theirs_ref, True)
         return carry
 
-    lax.fori_loop(0, xs[0].shape[0] // tall, block, 0)
+    lax.fori_loop(0, blocks, block, 0)
 
 
 def gain_rows(gain_ref):
@@ -301,32 +316,32 @@
     )(*operands)
 
 
-def gating(pieces, near, spatial, bias):
-    chunks, shards, tall = len(pieces), near.shape[0], 256
+def gating(pieces, weights, spatial, bias):
+    chunks, shards, tall = len(pieces), len(weights), 256
     rows, width = pieces[0].shape
     span = spatial.shape[0]
     model = chunks * width
     flops = 2 * rows * (model * 2 * span + span * span + span * model)
-    scratch = [
-        (rows, model),
-        (shards, model // shards, 2 * span),
-        (span, model),
-        pltpu.SemaphoreType.DMA((chunks + 1 + shards,)),
-    ]
-    operands = [*pieces, near, spatial, bias]
-    specs = [pl.BlockSpec(memory_space=pl.ANY)] * (chunks + 1) + [None] * 2
+    scratch = [(tall, model), (model, 2 * span), (span, model)]
+    operands = [*pieces, *weights, spatial, bias]
+    specs = [None] * len(operands)
     return call(gating_kernel, "gating", operands, specs, chunks, shards, tall, scratch, flops, 16)
 
 
-def channel(pieces, gate_scale, up_scale, ring):
-    chunks, shards, tall = len(pieces), len(ring), 256
+def channel(pieces, gate_scale, up_scale, far):
+    chunks, shards, tall = len(pieces), far.shape[0], 256
     rows, width = pieces[0].shape
     hidden = gate_scale.shape[0]
     model = chunks * width
     flops = 2 * rows * model * 3 * hidden
-    scratch = [(rows, model), *[(hidden, model)] * 3]
-    scratch.append(pltpu.SemaphoreType.DMA((chunks + 3 * shards,)))
-    operands = [*pieces, gate_scale, up_scale, *ring]
+    scratch = [
+        (rows, model),
+        (2, hidden, model),
+        (hidden, model),
+        pltpu.VMEM((2, rows, hidden), jnp.float32),
+        pltpu.SemaphoreType.DMA((chunks + 3 * shards,)),
+    ]
+    operands = [*pieces, gate_scale, up_scale, far]
     specs = [pl.BlockSpec(memory_space=pl.ANY)] * len(operands)
     specs[chunks] = specs[chunks + 1] = None
     return call(channel_kernel, "channel", operands, specs, chunks, shards, tall, scratch, flops, 57)
@@ -369,24 +384,13 @@
         down_scale,
     )
 
-    near = lax.all_gather(near, "fs")
-    ring = Ring(far)
-    steps = ring.count // 2
-    pieces = gather_features(tokens)
-    early = steps // 2
-    for _ in range(early):
+    far = lax.all_gather(far, "fs")
+    ring = Ring(near)
+    for _ in range(ring.count // 2):
         ring.advance()
-    pieces[0], *_ = lax.optimization_barrier((pieces[0], *ring.held[-2:]))
-    mine, theirs = gating(pieces, near, spatial[0], spatial_bias)
-    ring.advance()
-    pair = chip_sums(mine, theirs)
-    ring.after(*pair[1:])
-    ring.advance()
-    resid = (tokens.astype(jnp.float32) + sum_chips(pair)).astype(jnp.bfloat16)
-    ring.after(resid)
-    while ring.step < steps:
-        ring.advance()
-    mine, theirs = channel(gather_features(resid), gate_scale, up_scale, ring.held)
+    mine, theirs = gating(gather_features(tokens, True), ring.held, spatial[0], spatial_bias)
+    resid = (tokens.astype(jnp.float32) + sum_chips(chip_sums(mine, theirs))).astype(jnp.bfloat16)
+    mine, theirs = channel(gather_features(resid), gate_scale, up_scale, far)
     pair = chip_sums(mine, theirs)
     return (resid.astype(jnp.float32) + sum_chips(pair)).astype(jnp.bfloat16)
 

time: 224 us -> 226 us (level)
  waiting for transfers between devices: 90.8 us -> 105 us
  Pallas kernels: 29.5 us -> 24.6 us
  starting transfers between devices: 81.2 us -> 76.9 us
  local copies, waits for them, and re-layouts: 4.3 us -> 0.83 us
    ppermute x12, waiting for transfers between devices: 39.9 us -> 59.2 us  [to_chip(): lax.ppermute(x, 'tp', [(i, (i + CORES * step) % count) for i in range(cou...]
    ppermute x15, starting transfers between devices: 39 us -> 28 us  [pass_on(): lax.ppermute(x, 'fs', [(i, (i + step) % count) for i in range(count)])]
    ppermute x15, waiting for transfers between devices: 44.2 us -> 38.4 us  [pass_on(): lax.ppermute(x, 'fs', [(i, (i + step) % count) for i in range(count)])]
    ppermute x8, starting transfers between devices: 25.2 us -> 30.4 us  [swap_cores(): return lax.ppermute(x, 'tp', [(i, i ^ 1) for i in range(count)])]
    pallas_call x2, Pallas kernels: 27.1 us -> 22.2 us  [call(): pl.pallas_call(functools.partial(kernel, chunks=chunks, shards=shards, ta...]
    unnamed x56 -> x26, local copies, waits for them, and re-layouts: 3.3 us -> 0.75 us
  transfers between devices with their start and end apart: 36 -> 36, of which waited for: 20 -> 23; matrix products, arithmetic and copies ran while one was open for 1% -> 0% of each run, Pallas kernels for 0% -> 3%
where the time goes in v2:
time: 226 us
  waiting for transfers between devices  105 us (46%)
  starting transfers between devices  76.9 us (34%)
  Pallas kernels  24.6 us (11%)
  between operations  13.6 us (6%)
  other arithmetic  4.46 us (2%)
    ppermute x12, waiting for transfers between devices, to_chip(): lax.ppermute(x, 'tp', [(i, (i + CORES * step) % count) for i in range(cou...  59.2 us
    ppermute x15, waiting for transfers between devices, pass_on(): lax.ppermute(x, 'fs', [(i, (i + step) % count) for i in range(count)])  38.4 us
    ppermute x8, starting transfers between devices, swap_cores(): return lax.ppermute(x, 'tp', [(i, i ^ 1) for i in range(count)])  30.4 us
    ppermute x15, starting transfers between devices, pass_on(): lax.ppermute(x, 'fs', [(i, (i + step) % count) for i in range(count)])  28 us
    pallas_call x2, Pallas kernels, call(): pl.pallas_call(functools.partial(kernel, chunks=chunks, shards=shards, ta...  22.2 us
    ppermute x12, starting transfers between devices, to_chip(): lax.ppermute(x, 'tp', [(i, (i + CORES * step) % count) for i in range(cou...  18.4 us
    ppermute x8, waiting for transfers between devices, swap_cores(): return lax.ppermute(x, 'tp', [(i, i ^ 1) for i in range(count)])  7.82 us
  transfers between devices with their start and end apart: 36, of which 23 were waited for; matrix products, arithmetic and copies ran while one was open for 0% of the time, Pallas kernels for 3%

profile of v2, /device:TPU:33, one launch (start us, length us, event | category | flops | bytes accessed | tf_op | source)
XLA Modules:
  0.0 225.8 jit_solution(6649038423623665519)
XLA Ops:
  6.6 2.4 %fold.1 = (bf16[128,384]{1,0:T(8,128)(2,1)}, bf16[2112,128]{1,0:T(8,128)(2,1)}) custom-call(f32[16,128]{1,0:T(8,128)} %bitcast.55, f32[128,128]{1,0:T(8,128)} %u_ref.1, f32[128,128]{1,0:T(8,128)} %v_ref.1, f32[128,128]{1,0:T(8,128)} %mix_ref.1, f32[1,128]{1,0:T(1,128)} %bitcast.57, f32[1,128]{1,0:T(1,128)} %bitcast.58, f32[1,128]{1,0:T(1,128)} %mix_scale_ref.1, ...), custom_call_target="tpu_custom_call" | custom-call | flops 4194304 | bytes 1048576 | tf_op jit(solution)/shard_map/fold/pallas_call | solution.py:288
  11.3 2.7 %collective-permute-start.2 = (bf16[768,256]{1,0:T(8,128)(2,1)S(1)}, bf16[768,256]{1,0:T(8,128)(2,1)S(1)}, u32[]{:S(2)}, u32[]{:S(2)}) collective-permute-start(bf16[768,256]{1,0:T(8,128)(2,1)S(1)} %copy-done), channel_id=1, source_target_pairs={{0,4},{1,5},{2,6},{3,7},{4,0},{5,1},{6,2},{7,3},{8,12},{9,13},{10,... | collective-permute-start | bytes 1179656 | tf_op jit(solution)/shard_map/ppermute | solution.py:21
  15.0 3.0 %collective-permute-done.1.refs_2_ = bf16[768,256]{1,0:T(8,128)(2,1)S(1)} collective-permute-done((bf16[768,256]{1,0:T(8,128)(2,1)S(1)}, bf16[768,256]{1,0:T(8,128)(2,1)S(1)}, u32[]{:S(2)}, u32[]{:S(2)}) %collective-permute-start.1) | collective-permute-done | bytes 393248 | tf_op jit(solution)/shard_map/ppermute | solution.py:21
  18.0 9.6 %collective-permute-done.2.refs_4_ = bf16[768,256]{1,0:T(8,128)(2,1)S(1)} collective-permute-done((bf16[768,256]{1,0:T(8,128)(2,1)S(1)}, bf16[768,256]{1,0:T(8,128)(2,1)S(1)}, u32[]{:S(2)}, u32[]{:S(2)}) %collective-permute-start.2) | collective-permute-done | bytes 393248 | tf_op jit(solution)/shard_map/ppermute | solution.py:21
  27.7 16.2 %collective-permute-start.4 = (bf16[3,768,256]{2,1,0:T(8,128)(2,1)S(1)}, bf16[3,768,256]{2,1,0:T(8,128)(2,1)S(1)}, u32[]{:S(2)}, u32[]{:S(2)}) collective-permute-start(bf16[3,768,256]{2,1,0:T(8,128)(2,1)S(1)} %pad_maximum_fusion), channel_id=1, source_target_pairs={{0,1},{1,0},{2,3},{3,2},{4,5},{5,4},{6,7},{7,6},{8,9},{9,8},{10,11... | collective-permute-start | bytes 3538952 | tf_op jit(solution)/shard_map/ppermute | solution.py:16
  43.9 11.0 %collective-permute-start.6 = (bf16[128,384]{1,0:T(8,128)(2,1)S(1)}, bf16[128,384]{1,0:T(8,128)(2,1)S(1)}, u32[]{:S(2)}, u32[]{:S(2)}) collective-permute-start(bf16[128,384]{1,0:T(8,128)(2,1)S(1)} %copy-done.1), channel_id=1, source_target_pairs={{0,120},{8,0},{16,8},{24,16},{32,24},{40,32},{48,40},{56,48},{64,5... | collective-permute-start | bytes 294920 | tf_op jit(solution)/shard_map/ppermute | solution.py:66
  54.9 5.6 %collective-permute-done.5.refs_9_ = bf16[128,384]{1,0:T(8,128)(2,1)S(1)} collective-permute-done((bf16[128,384]{1,0:T(8,128)(2,1)S(1)}, bf16[128,384]{1,0:T(8,128)(2,1)S(1)}, u32[]{:S(2)}, u32[]{:S(2)}) %collective-permute-start.5) | collective-permute-done | bytes 98336 | tf_op jit(solution)/shard_map/ppermute | solution.py:66
  60.5 2.7 %collective-permute-start.8 = (bf16[128,384]{1,0:T(8,128)(2,1)S(1)}, bf16[128,384]{1,0:T(8,128)(2,1)S(1)}, u32[]{:S(2)}, u32[]{:S(2)}) collective-permute-start(bf16[128,384]{1,0:T(8,128)(2,1)S(1)} %collective-permute-done.6.refs_10_), channel_id=1, source_target_pairs={{0,120},{8,0},{16,8},{24,16},{32,24},{40,32},{48,40},{56,48},{64,5... | collective-permute-start | bytes 294920 | tf_op jit(solution)/shard_map/ppermute | solution.py:66
  63.2 5.4 %collective-permute-done.7.refs_11_ = bf16[128,384]{1,0:T(8,128)(2,1)S(1)} collective-permute-done((bf16[128,384]{1,0:T(8,128)(2,1)S(1)}, bf16[128,384]{1,0:T(8,128)(2,1)S(1)}, u32[]{:S(2)}, u32[]{:S(2)}) %collective-permute-start.7) | collective-permute-done | bytes 98336 | tf_op jit(solution)/shard_map/ppermute | solution.py:66
  68.6 2.7 %collective-permute-start.10 = (bf16[128,384]{1,0:T(8,128)(2,1)S(1)}, bf16[128,384]{1,0:T(8,128)(2,1)S(1)}, u32[]{:S(2)}, u32[]{:S(2)}) collective-permute-start(bf16[128,384]{1,0:T(8,128)(2,1)S(1)} %collective-permute-done.8.refs_12_), channel_id=1, source_target_pairs={{0,120},{8,0},{16,8},{24,16},{32,24},{40,32},{48,40},{56,48},{64,5... | collective-permute-start | bytes 294920 | tf_op jit(solution)/shard_map/ppermute | solution.py:66
  71.2 5.2 %collective-permute-done.9.refs_13_ = bf16[128,384]{1,0:T(8,128)(2,1)S(1)} collective-permute-done((bf16[128,384]{1,0:T(8,128)(2,1)S(1)}, bf16[128,384]{1,0:T(8,128)(2,1)S(1)}, u32[]{:S(2)}, u32[]{:S(2)}) %collective-permute-start.9) | collective-permute-done | bytes 98336 | tf_op jit(solution)/shard_map/ppermute | solution.py:66
  76.4 2.7 %collective-permute-start.12 = (bf16[128,384]{1,0:T(8,128)(2,1)S(1)}, bf16[128,384]{1,0:T(8,128)(2,1)S(1)}, u32[]{:S(2)}, u32[]{:S(2)}) collective-permute-start(bf16[128,384]{1,0:T(8,128)(2,1)S(1)} %collective-permute-done.10.refs_14_), channel_id=1, source_target_pairs={{0,120},{8,0},{16,8},{24,16},{32,24},{40,32},{48,40},{56,48},{64,5... | collective-permute-start | bytes 294920 | tf_op jit(solution)/shard_map/ppermute | solution.py:66
  79.1 5.0 %collective-permute-done.11.refs_15_ = bf16[128,384]{1,0:T(8,128)(2,1)S(1)} collective-permute-done((bf16[128,384]{1,0:T(8,128)(2,1)S(1)}, bf16[128,384]{1,0:T(8,128)(2,1)S(1)}, u32[]{:S(2)}, u32[]{:S(2)}) %collective-permute-start.11) | collective-permute-done | bytes 98336 | tf_op jit(solution)/shard_map/ppermute | solution.py:66
  84.1 2.7 %collective-permute-start.14 = (bf16[128,384]{1,0:T(8,128)(2,1)S(1)}, bf16[128,384]{1,0:T(8,128)(2,1)S(1)}, u32[]{:S(2)}, u32[]{:S(2)}) collective-permute-start(bf16[128,384]{1,0:T(8,128)(2,1)S(1)} %collective-permute-done.12.refs_16_), channel_id=1, source_target_pairs={{0,120},{8,0},{16,8},{24,16},{32,24},{40,32},{48,40},{56,48},{64,5... | collective-permute-start | bytes 294920 | tf_op jit(solution)/shard_map/ppermute | solution.py:66
  86.8 4.8 %collective-permute-done.13.refs_17_ = bf16[128,384]{1,0:T(8,128)(2,1)S(1)} collective-permute-done((bf16[128,384]{1,0:T(8,128)(2,1)S(1)}, bf16[128,384]{1,0:T(8,128)(2,1)S(1)}, u32[]{:S(2)}, u32[]{:S(2)}) %collective-permute-start.13) | collective-permute-done | bytes 98336 | tf_op jit(solution)/shard_map/ppermute | solution.py:66
  91.6 3.0 %collective-permute-start = (bf16[768,256]{1,0:T(8,128)(2,1)S(1)}, bf16[768,256]{1,0:T(8,128)(2,1)S(1)}, u32[]{:S(2)}, u32[]{:S(2)}) collective-permute-start(bf16[768,256]{1,0:T(8,128)(2,1)S(1)} %copy-done), channel_id=1, source_target_pairs={{0,1},{1,0},{2,3},{3,2},{4,5},{5,4},{6,7},{7,6},{8,9},{9,8},{10,11... | collective-permute-start | bytes 1179656 | tf_op jit(solution)/shard_map/ppermute | solution.py:16
  94.6 3.0 %collective-permute-start.16 = (bf16[128,384]{1,0:T(8,128)(2,1)S(1)}, bf16[128,384]{1,0:T(8,128)(2,1)S(1)}, u32[]{:S(2)}, u32[]{:S(2)}) collective-permute-start(bf16[128,384]{1,0:T(8,128)(2,1)S(1)} %collective-permute-done.14.refs_18_), channel_id=1, source_target_pairs={{0,120},{8,0},{16,8},{24,16},{32,24},{40,32},{48,40},{56,48},{64,5... | collective-permute-start | bytes 294920 | tf_op jit(solution)/shard_map/ppermute | solution.py:66
  98.9 2.7 %collective-permute-done.16.refs_20_ = bf16[128,384]{1,0:T(8,128)(2,1)S(1)} collective-permute-done((bf16[128,384]{1,0:T(8,128)(2,1)S(1)}, bf16[128,384]{1,0:T(8,128)(2,1)S(1)}, u32[]{:S(2)}, u32[]{:S(2)}) %collective-permute-start.16) | collective-permute-done | bytes 98336 | tf_op jit(solution)/shard_map/ppermute | solution.py:66
  101.6 3.4 %collective-permute-start.18 = (bf16[128,384]{1,0:T(8,128)(2,1)S(1)}, bf16[128,384]{1,0:T(8,128)(2,1)S(1)}, u32[]{:S(2)}, u32[]{:S(2)}) collective-permute-start(bf16[128,384]{1,0:T(8,128)(2,1)S(1)} %collective-permute-done.16.refs_20_), channel_id=1, source_target_pairs={{0,120},{8,0},{16,8},{24,16},{32,24},{40,32},{48,40},{56,48},{64,5... | collective-permute-start | bytes 294920 | tf_op jit(solution)/shard_map/ppermute | solution.py:66
  106.3 2.6 %collective-permute-done.18.refs_22_ = bf16[128,384]{1,0:T(8,128)(2,1)S(1)} collective-permute-done((bf16[128,384]{1,0:T(8,128)(2,1)S(1)}, bf16[128,384]{1,0:T(8,128)(2,1)S(1)}, u32[]{:S(2)}, u32[]{:S(2)}) %collective-permute-start.18) | collective-permute-done | bytes 98336 | tf_op jit(solution)/shard_map/ppermute | solution.py:66
  108.9 4.5 %collective-permute-done.19.refs_23_ = bf16[128,384]{1,0:T(8,128)(2,1)S(1)} collective-permute-done((bf16[128,384]{1,0:T(8,128)(2,1)S(1)}, bf16[128,384]{1,0:T(8,128)(2,1)S(1)}, u32[]{:S(2)}, u32[]{:S(2)}) %collective-permute-start.19) | collective-permute-done | bytes 98336 | tf_op jit(solution)/shard_map/ppermute | solution.py:66
  113.4 7.0 %gating.1 = (bf16[4,768,256]{2,1,0:T(8,128)(2,1)S(1)}, bf16[4,768,256]{2,1,0:T(8,128)(2,1)S(1)}) custom-call(bf16[768,256]{1,0:T(8,128)(2,1)S(1)} %copy-done, bf16[768,256]{1,0:T(8,128)(2,1)S(1)} %collective-permute-done.refs_1_, bf16[768,256]{1,0:T(8,128)(2,1)S(1)} %collective-permute-done.1.refs_2_, bf16[768,256]{1,0:T(8,128)(2,1)S(1)} %get-tuple-element.53.refs_3_, ...), custom_call_target="tpu_custom_call" | custom-call | flops 1233125376 | bytes 1048576 | tf_op jit(solution)/shard_map/gating/pallas_call | solution.py:304
  120.4 5.5 %collective-permute-start.20 = (bf16[4,768,256]{2,1,0:T(8,128)(2,1)S(1)}, bf16[4,768,256]{2,1,0:T(8,128)(2,1)S(1)}, u32[]{:S(2)}, u32[]{:S(2)}) collective-permute-start(bf16[4,768,256]{2,1,0:T(8,128)(2,1)S(1)} %get-tuple-element.41), channel_id=1, source_target_pairs={{0,1},{1,0},{2,3},{3,2},{4,5},{5,4},{6,7},{7,6},{8,9},{9,8},{10,11... | collective-permute-start | bytes 4718600 | tf_op jit(solution)/shard_map/ppermute | solution.py:16
  125.9 3.0 %collective-permute-done.20 = bf16[4,768,256]{2,1,0:T(8,128)(2,1)S(1)} collective-permute-done((bf16[4,768,256]{2,1,0:T(8,128)(2,1)S(1)}, bf16[4,768,256]{2,1,0:T(8,128)(2,1)S(1)}, u32[]{:S(2)}, u32[]{:S(2)}) %collective-permute-start.20) | collective-permute-done | bytes 1572896 | tf_op jit(solution)/shard_map/ppermute | solution.py:16
  133.7 7.3 %collective-permute-done.21 = bf16[768,256]{1,0:T(8,128)(2,1)S(1)} collective-permute-done((bf16[768,256]{1,0:T(8,128)(2,1)S(1)}, bf16[768,256]{1,0:T(8,128)(2,1)S(1)}, u32[]{:S(2)}, u32[]{:S(2)}) %collective-permute-start.21) | collective-permute-done | bytes 393248 | tf_op jit(solution)/shard_map/ppermute | solution.py:21
  141.0 8.8 %collective-permute-done.22 = bf16[768,256]{1,0:T(8,128)(2,1)S(1)} collective-permute-done((bf16[768,256]{1,0:T(8,128)(2,1)S(1)}, bf16[768,256]{1,0:T(8,128)(2,1)S(1)}, u32[]{:S(2)}, u32[]{:S(2)}) %collective-permute-start.22) | collective-permute-done | bytes 393248 | tf_op jit(solution)/shard_map/ppermute | solution.py:21
  156.8 5.1 %collective-permute-done.25.refs_2_ = bf16[768,256]{1,0:T(8,128)(2,1)S(1)} collective-permute-done((bf16[768,256]{1,0:T(8,128)(2,1)S(1)}, bf16[768,256]{1,0:T(8,128)(2,1)S(1)}, u32[]{:S(2)}, u32[]{:S(2)}) %collective-permute-start.25) | collective-permute-done | bytes 393248 | tf_op jit(solution)/shard_map/ppermute | solution.py:21
  163.6 8.2 %collective-permute-done.27.refs_4_ = bf16[768,256]{1,0:T(8,128)(2,1)S(1)} collective-permute-done((bf16[768,256]{1,0:T(8,128)(2,1)S(1)}, bf16[768,256]{1,0:T(8,128)(2,1)S(1)}, u32[]{:S(2)}, u32[]{:S(2)}) %collective-permute-start.27) | collective-permute-done | bytes 393248 | tf_op jit(solution)/shard_map/ppermute | solution.py:21
  175.9 15.2 %channel.1 = (bf16[4,768,256]{2,1,0:T(8,128)(2,1)}, bf16[4,768,256]{2,1,0:T(8,128)(2,1)}) custom-call(bf16[768,256]{1,0:T(8,128)(2,1)} %copy-done.4, bf16[768,256]{1,0:T(8,128)(2,1)} %copy-done.9, bf16[768,256]{1,0:T(8,128)(2,1)} %copy-done.6, bf16[768,256]{1,0:T(8,128)(2,1)} %copy-done.10, bf16[768,256]{1,0:T(8,128)(2,1)} %copy-done.7, ...), custom_call_target="tpu_custom_call" | custom-call | flops 6643777536 | bytes 1048576 | tf_op jit(solution)/shard_map/channel/pallas_call | solution.py:304
  191.6 3.2 %collective-permute-done.31 = bf16[4,768,256]{2,1,0:T(8,128)(2,1)S(1)} collective-permute-done((bf16[4,768,256]{2,1,0:T(8,128)(2,1)}, bf16[4,768,256]{2,1,0:T(8,128)(2,1)S(1)}, u32[]{:S(2)}, u32[]{:S(2)}) %collective-permute-start.31) | collective-permute-done | bytes 1572896 | tf_op jit(solution)/shard_map/ppermute | solution.py:16
  199.6 8.5 %collective-permute-done.32 = bf16[768,256]{1,0:T(8,128)(2,1)S(1)} collective-permute-done((bf16[768,256]{1,0:T(8,128)(2,1)S(1)}, bf16[768,256]{1,0:T(8,128)(2,1)S(1)}, u32[]{:S(2)}, u32[]{:S(2)}) %collective-permute-start.32) | collective-permute-done | bytes 393248 | tf_op jit(solution)/shard_map/ppermute | solution.py:21
  208.1 8.4 %collective-permute-done.33 = bf16[768,256]{1,0:T(8,128)(2,1)S(1)} collective-permute-done((bf16[768,256]{1,0:T(8,128)(2,1)S(1)}, bf16[768,256]{1,0:T(8,128)(2,1)S(1)}, u32[]{:S(2)}, u32[]{:S(2)}) %collective-permute-start.33) | collective-permute-done | bytes 393248 | tf_op jit(solution)/shard_map/ppermute | solution.py:21
  (76 shorter events, 31.2 us)
Async XLA Ops:
  6.5 168.6 %all-gather.3.cloned.1.call-start = ((), (), s32[]{:S(2)}) async-start(), calls=%async_computation | async-start | bytes 9191424 | tf_op jit(solution)/shard_map/all_gather | solution.py:387
  9.0 9.0 %collective-permute-start.1 = (bf16[768,256]{1,0:T(8,128)(2,1)S(1)}, bf16[768,256]{1,0:T(8,128)(2,1)S(1)}, u32[]{:S(2)}, u32[]{:S(2)}) collective-permute-start(bf16[768,256]{1,0:T(8,128)(2,1)S(1)} %copy-done), channel_id=1, source_target_pairs={{0,2},{1,3},{2,4},{3,5},{4,6},{5,7},{6,0},{7,1},{8,10},{9,11},{10,... | collective-permute-start | bytes 1179656 | tf_op jit(solution)/shard_map/ppermute | solution.py:21
  11.3 16.3 %collective-permute-start.2 = (bf16[768,256]{1,0:T(8,128)(2,1)S(1)}, bf16[768,256]{1,0:T(8,128)(2,1)S(1)}, u32[]{:S(2)}, u32[]{:S(2)}) collective-permute-start(bf16[768,256]{1,0:T(8,128)(2,1)S(1)} %copy-done), channel_id=1, source_target_pairs={{0,4},{1,5},{2,6},{3,7},{4,0},{5,1},{6,2},{7,3},{8,12},{9,13},{10,... | collective-permute-start | bytes 1179656 | tf_op jit(solution)/shard_map/ppermute | solution.py:21
  14.0 13.6 %collective-permute-start.3 = (bf16[768,256]{1,0:T(8,128)(2,1)S(1)}, bf16[768,256]{1,0:T(8,128)(2,1)S(1)}, u32[]{:S(2)}, u32[]{:S(2)}) collective-permute-start(bf16[768,256]{1,0:T(8,128)(2,1)S(1)} %copy-done), channel_id=1, source_target_pairs={{0,6},{1,7},{2,0},{3,1},{4,2},{5,3},{6,4},{7,5},{8,14},{9,15},{10,... | collective-permute-start | bytes 1179656 | tf_op jit(solution)/shard_map/ppermute | solution.py:21
  27.7 78.4 %collective-permute-start.4 = (bf16[3,768,256]{2,1,0:T(8,128)(2,1)S(1)}, bf16[3,768,256]{2,1,0:T(8,128)(2,1)S(1)}, u32[]{:S(2)}, u32[]{:S(2)}) collective-permute-start(bf16[3,768,256]{2,1,0:T(8,128)(2,1)S(1)} %pad_maximum_fusion), channel_id=1, source_target_pairs={{0,1},{1,0},{2,3},{3,2},{4,5},{5,4},{6,7},{7,6},{8,9},{9,8},{10,11... | collective-permute-start | bytes 3538952 | tf_op jit(solution)/shard_map/ppermute | solution.py:16
  43.9 16.6 %collective-permute-start.5 = (bf16[128,384]{1,0:T(8,128)(2,1)S(1)}, bf16[128,384]{1,0:T(8,128)(2,1)S(1)}, u32[]{:S(2)}, u32[]{:S(2)}) collective-permute-start(bf16[128,384]{1,0:T(8,128)(2,1)S(1)} %copy-done.1), channel_id=1, source_target_pairs={{0,8},{8,16},{16,24},{24,32},{32,40},{40,48},{48,56},{56,64},{64,7... | collective-permute-start | bytes 294920 | tf_op jit(solution)/shard_map/ppermute | solution.py:66
  43.9 16.6 %collective-permute-start.6 = (bf16[128,384]{1,0:T(8,128)(2,1)S(1)}, bf16[128,384]{1,0:T(8,128)(2,1)S(1)}, u32[]{:S(2)}, u32[]{:S(2)}) collective-permute-start(bf16[128,384]{1,0:T(8,128)(2,1)S(1)} %copy-done.1), channel_id=1, source_target_pairs={{0,120},{8,0},{16,8},{24,16},{32,24},{40,32},{48,40},{56,48},{64,5... | collective-permute-start | bytes 294920 | tf_op jit(solution)/shard_map/ppermute | solution.py:66
  60.5 8.1 %collective-permute-start.7 = (bf16[128,384]{1,0:T(8,128)(2,1)S(1)}, bf16[128,384]{1,0:T(8,128)(2,1)S(1)}, u32[]{:S(2)}, u32[]{:S(2)}) collective-permute-start(bf16[128,384]{1,0:T(8,128)(2,1)S(1)} %collective-permute-done.5.refs_9_), channel_id=1, source_target_pairs={{0,8},{8,16},{16,24},{24,32},{32,40},{40,48},{48,56},{56,64},{64,7... | collective-permute-start | bytes 294920 | tf_op jit(solution)/shard_map/ppermute | solution.py:66
  60.5 8.1 %collective-permute-start.8 = (bf16[128,384]{1,0:T(8,128)(2,1)S(1)}, bf16[128,384]{1,0:T(8,128)(2,1)S(1)}, u32[]{:S(2)}, u32[]{:S(2)}) collective-permute-start(bf16[128,384]{1,0:T(8,128)(2,1)S(1)} %collective-permute-done.6.refs_10_), channel_id=1, source_target_pairs={{0,120},{8,0},{16,8},{24,16},{32,24},{40,32},{48,40},{56,48},{64,5... | collective-permute-start | bytes 294920 | tf_op jit(solution)/shard_map/ppermute | solution.py:66
  68.6 7.9 %collective-permute-start.9 = (bf16[128,384]{1,0:T(8,128)(2,1)S(1)}, bf16[128,384]{1,0:T(8,128)(2,1)S(1)}, u32[]{:S(2)}, u32[]{:S(2)}) collective-permute-start(bf16[128,384]{1,0:T(8,128)(2,1)S(1)} %collective-permute-done.7.refs_11_), channel_id=1, source_target_pairs={{0,8},{8,16},{16,24},{24,32},{32,40},{40,48},{48,56},{56,64},{64,7... | collective-permute-start | bytes 294920 | tf_op jit(solution)/shard_map/ppermute | solution.py:66
  68.6 7.9 %collective-permute-start.10 = (bf16[128,384]{1,0:T(8,128)(2,1)S(1)}, bf16[128,384]{1,0:T(8,128)(2,1)S(1)}, u32[]{:S(2)}, u32[]{:S(2)}) collective-permute-start(bf16[128,384]{1,0:T(8,128)(2,1)S(1)} %collective-permute-done.8.refs_12_), channel_id=1, source_target_pairs={{0,120},{8,0},{16,8},{24,16},{32,24},{40,32},{48,40},{56,48},{64,5... | collective-permute-start | bytes 294920 | tf_op jit(solution)/shard_map/ppermute | solution.py:66
  76.4 7.7 %collective-permute-start.11 = (bf16[128,384]{1,0:T(8,128)(2,1)S(1)}, bf16[128,384]{1,0:T(8,128)(2,1)S(1)}, u32[]{:S(2)}, u32[]{:S(2)}) collective-permute-start(bf16[128,384]{1,0:T(8,128)(2,1)S(1)} %collective-permute-done.9.refs_13_), channel_id=1, source_target_pairs={{0,8},{8,16},{16,24},{24,32},{32,40},{40,48},{48,56},{56,64},{64,7... | collective-permute-start | bytes 294920 | tf_op jit(solution)/shard_map/ppermute | solution.py:66
  76.4 7.7 %collective-permute-start.12 = (bf16[128,384]{1,0:T(8,128)(2,1)S(1)}, bf16[128,384]{1,0:T(8,128)(2,1)S(1)}, u32[]{:S(2)}, u32[]{:S(2)}) collective-permute-start(bf16[128,384]{1,0:T(8,128)(2,1)S(1)} %collective-permute-done.10.refs_14_), channel_id=1, source_target_pairs={{0,120},{8,0},{16,8},{24,16},{32,24},{40,32},{48,40},{56,48},{64,5... | collective-permute-start | bytes 294920 | tf_op jit(solution)/shard_map/ppermute | solution.py:66
  84.1 7.5 %collective-permute-start.13 = (bf16[128,384]{1,0:T(8,128)(2,1)S(1)}, bf16[128,384]{1,0:T(8,128)(2,1)S(1)}, u32[]{:S(2)}, u32[]{:S(2)}) collective-permute-start(bf16[128,384]{1,0:T(8,128)(2,1)S(1)} %collective-permute-done.11.refs_15_), channel_id=1, source_target_pairs={{0,8},{8,16},{16,24},{24,32},{32,40},{40,48},{48,56},{56,64},{64,7... | collective-permute-start | bytes 294920 | tf_op jit(solution)/shard_map/ppermute | solution.py:66
  84.1 10.5 %collective-permute-start.14 = (bf16[128,384]{1,0:T(8,128)(2,1)S(1)}, bf16[128,384]{1,0:T(8,128)(2,1)S(1)}, u32[]{:S(2)}, u32[]{:S(2)}) collective-permute-start(bf16[128,384]{1,0:T(8,128)(2,1)S(1)} %collective-permute-done.12.refs_16_), channel_id=1, source_target_pairs={{0,120},{8,0},{16,8},{24,16},{32,24},{40,32},{48,40},{56,48},{64,5... | collective-permute-start | bytes 294920 | tf_op jit(solution)/shard_map/ppermute | solution.py:66
  91.6 7.3 %collective-permute-start.15 = (bf16[128,384]{1,0:T(8,128)(2,1)S(1)}, bf16[128,384]{1,0:T(8,128)(2,1)S(1)}, u32[]{:S(2)}, u32[]{:S(2)}) collective-permute-start(bf16[128,384]{1,0:T(8,128)(2,1)S(1)} %collective-permute-done.13.refs_17_), channel_id=1, source_target_pairs={{0,8},{8,16},{16,24},{24,32},{32,40},{40,48},{48,56},{56,64},{64,7... | collective-permute-start | bytes 294920 | tf_op jit(solution)/shard_map/ppermute | solution.py:66
  91.6 14.7 %collective-permute-start = (bf16[768,256]{1,0:T(8,128)(2,1)S(1)}, bf16[768,256]{1,0:T(8,128)(2,1)S(1)}, u32[]{:S(2)}, u32[]{:S(2)}) collective-permute-start(bf16[768,256]{1,0:T(8,128)(2,1)S(1)} %copy-done), channel_id=1, source_target_pairs={{0,1},{1,0},{2,3},{3,2},{4,5},{5,4},{6,7},{7,6},{8,9},{9,8},{10,11... | collective-permute-start | bytes 1179656 | tf_op jit(solution)/shard_map/ppermute | solution.py:16
  98.9 7.3 %collective-permute-start.17 = (bf16[128,384]{1,0:T(8,128)(2,1)S(1)}, bf16[128,384]{1,0:T(8,128)(2,1)S(1)}, u32[]{:S(2)}, u32[]{:S(2)}) collective-permute-start(bf16[128,384]{1,0:T(8,128)(2,1)S(1)} %collective-permute-done.15.refs_19_), channel_id=1, source_target_pairs={{0,8},{8,16},{16,24},{24,32},{32,40},{40,48},{48,56},{56,64},{64,7... | collective-permute-start | bytes 294920 | tf_op jit(solution)/shard_map/ppermute | solution.py:66
  101.6 7.3 %collective-permute-start.18 = (bf16[128,384]{1,0:T(8,128)(2,1)S(1)}, bf16[128,384]{1,0:T(8,128)(2,1)S(1)}, u32[]{:S(2)}, u32[]{:S(2)}) collective-permute-start(bf16[128,384]{1,0:T(8,128)(2,1)S(1)} %collective-permute-done.16.refs_20_), channel_id=1, source_target_pairs={{0,120},{8,0},{16,8},{24,16},{32,24},{40,32},{48,40},{56,48},{64,5... | collective-permute-start | bytes 294920 | tf_op jit(solution)/shard_map/ppermute | solution.py:66
  106.2 7.2 %collective-permute-start.19 = (bf16[128,384]{1,0:T(8,128)(2,1)S(1)}, bf16[128,384]{1,0:T(8,128)(2,1)S(1)}, u32[]{:S(2)}, u32[]{:S(2)}) collective-permute-start(bf16[128,384]{1,0:T(8,128)(2,1)S(1)} %collective-permute-done.17.refs_21_), channel_id=1, source_target_pairs={{0,8},{8,16},{16,24},{24,32},{32,40},{40,48},{48,56},{56,64},{64,7... | collective-permute-start | bytes 294920 | tf_op jit(solution)/shard_map/ppermute | solution.py:66
  120.4 8.6 %collective-permute-start.20 = (bf16[4,768,256]{2,1,0:T(8,128)(2,1)S(1)}, bf16[4,768,256]{2,1,0:T(8,128)(2,1)S(1)}, u32[]{:S(2)}, u32[]{:S(2)}) collective-permute-start(bf16[4,768,256]{2,1,0:T(8,128)(2,1)S(1)} %get-tuple-element.41), channel_id=1, source_target_pairs={{0,1},{1,0},{2,3},{3,2},{4,5},{5,4},{6,7},{7,6},{8,9},{9,8},{10,11... | collective-permute-start | bytes 4718600 | tf_op jit(solution)/shard_map/ppermute | solution.py:16
  129.3 11.7 %collective-permute-start.21 = (bf16[768,256]{1,0:T(8,128)(2,1)S(1)}, bf16[768,256]{1,0:T(8,128)(2,1)S(1)}, u32[]{:S(2)}, u32[]{:S(2)}) collective-permute-start(bf16[768,256]{1,0:T(8,128)(2,1)S(1)} %get-tuple-element.48), channel_id=1, source_target_pairs={{0,2},{1,3},{2,4},{3,5},{4,6},{5,7},{6,0},{7,1},{8,10},{9,11},{10,... | collective-permute-start | bytes 1179656 | tf_op jit(solution)/shard_map/ppermute | solution.py:21
  130.4 19.4 %collective-permute-start.22 = (bf16[768,256]{1,0:T(8,128)(2,1)S(1)}, bf16[768,256]{1,0:T(8,128)(2,1)S(1)}, u32[]{:S(2)}, u32[]{:S(2)}) collective-permute-start(bf16[768,256]{1,0:T(8,128)(2,1)S(1)} %get-tuple-element.50), channel_id=1, source_target_pairs={{0,4},{1,5},{2,6},{3,7},{4,0},{5,1},{6,2},{7,3},{8,12},{9,13},{10,... | collective-permute-start | bytes 1179656 | tf_op jit(solution)/shard_map/ppermute | solution.py:21
  132.5 17.3 %collective-permute-start.23 = (bf16[768,256]{1,0:T(8,128)(2,1)S(1)}, bf16[768,256]{1,0:T(8,128)(2,1)S(1)}, u32[]{:S(2)}, u32[]{:S(2)}) collective-permute-start(bf16[768,256]{1,0:T(8,128)(2,1)S(1)} %get-tuple-element.49), channel_id=1, source_target_pairs={{0,6},{1,7},{2,0},{3,1},{4,2},{5,3},{6,4},{7,5},{8,14},{9,15},{10,... | collective-permute-start | bytes 1179656 | tf_op jit(solution)/shard_map/ppermute | solution.py:21
  150.1 11.8 %collective-permute-start.25 = (bf16[768,256]{1,0:T(8,128)(2,1)S(1)}, bf16[768,256]{1,0:T(8,128)(2,1)S(1)}, u32[]{:S(2)}, u32[]{:S(2)}) collective-permute-start(bf16[768,256]{1,0:T(8,128)(2,1)S(1)} %fusion.7.refs_0_), channel_id=1, source_target_pairs={{0,2},{1,3},{2,4},{3,5},{4,6},{5,7},{6,0},{7,1},{8,10},{9,11},{10,... | collective-permute-start | bytes 1179656 | tf_op jit(solution)/shard_map/ppermute | solution.py:21
  152.4 19.4 %collective-permute-start.27 = (bf16[768,256]{1,0:T(8,128)(2,1)S(1)}, bf16[768,256]{1,0:T(8,128)(2,1)S(1)}, u32[]{:S(2)}, u32[]{:S(2)}) collective-permute-start(bf16[768,256]{1,0:T(8,128)(2,1)S(1)} %fusion.7.refs_0_), channel_id=1, source_target_pairs={{0,4},{1,5},{2,6},{3,7},{4,0},{5,1},{6,2},{7,3},{8,12},{9,13},{10,... | collective-permute-start | bytes 1179656 | tf_op jit(solution)/shard_map/ppermute | solution.py:21
  154.7 18.5 %collective-permute-start.29 = (bf16[768,256]{1,0:T(8,128)(2,1)S(1)}, bf16[768,256]{1,0:T(8,128)(2,1)S(1)}, u32[]{:S(2)}, u32[]{:S(2)}) collective-permute-start(bf16[768,256]{1,0:T(8,128)(2,1)S(1)} %fusion.7.refs_0_), channel_id=1, source_target_pairs={{0,6},{1,7},{2,0},{3,1},{4,2},{5,3},{6,4},{7,5},{8,14},{9,15},{10,... | collective-permute-start | bytes 1179656 | tf_op jit(solution)/shard_map/ppermute | solution.py:21
  155.0 18.6 %collective-permute-start.24 = (bf16[768,256]{1,0:T(8,128)(2,1)S(1)}, bf16[768,256]{1,0:T(8,128)(2,1)S(1)}, u32[]{:S(2)}, u32[]{:S(2)}) collective-permute-start(bf16[768,256]{1,0:T(8,128)(2,1)S(1)} %fusion.7.refs_0_), channel_id=1, source_target_pairs={{0,1},{1,0},{2,3},{3,2},{4,5},{5,4},{6,7},{7,6},{8,9},{9,8},{10,11... | collective-permute-start | bytes 1179656 | tf_op jit(solution)/shard_map/ppermute | solution.py:16
  161.9 11.6 %collective-permute-start.26 = (bf16[768,256]{1,0:T(8,128)(2,1)S(1)}, bf16[768,256]{1,0:T(8,128)(2,1)S(1)}, u32[]{:S(2)}, u32[]{:S(2)}) collective-permute-start(bf16[768,256]{1,0:T(8,128)(2,1)S(1)} %collective-permute-done.25.refs_2_), channel_id=1, source_target_pairs={{0,1},{1,0},{2,3},{3,2},{4,5},{5,4},{6,7},{7,6},{8,9},{9,8},{10,11... | collective-permute-start | bytes 1179656 | tf_op jit(solution)/shard_map/ppermute | solution.py:16
  196.5 11.7 %collective-permute-start.32 = (bf16[768,256]{1,0:T(8,128)(2,1)S(1)}, bf16[768,256]{1,0:T(8,128)(2,1)S(1)}, u32[]{:S(2)}, u32[]{:S(2)}) collective-permute-start(bf16[768,256]{1,0:T(8,128)(2,1)S(1)} %get-tuple-element.45), channel_id=1, source_target_pairs={{0,2},{1,3},{2,4},{3,5},{4,6},{5,7},{6,0},{7,1},{8,10},{9,11},{10,... | collective-permute-start | bytes 1179656 | tf_op jit(solution)/shard_map/ppermute | solution.py:21
  196.9 19.7 %collective-permute-start.33 = (bf16[768,256]{1,0:T(8,128)(2,1)S(1)}, bf16[768,256]{1,0:T(8,128)(2,1)S(1)}, u32[]{:S(2)}, u32[]{:S(2)}) collective-permute-start(bf16[768,256]{1,0:T(8,128)(2,1)S(1)} %get-tuple-element.47), channel_id=1, source_target_pairs={{0,4},{1,5},{2,6},{3,7},{4,0},{5,1},{6,2},{7,3},{8,12},{9,13},{10,... | collective-permute-start | bytes 1179656 | tf_op jit(solution)/shard_map/ppermute | solution.py:21
  199.2 17.7 %collective-permute-start.34 = (bf16[768,256]{1,0:T(8,128)(2,1)S(1)}, bf16[768,256]{1,0:T(8,128)(2,1)S(1)}, u32[]{:S(2)}, u32[]{:S(2)}) collective-permute-start(bf16[768,256]{1,0:T(8,128)(2,1)S(1)} %get-tuple-element.46), channel_id=1, source_target_pairs={{0,6},{1,7},{2,0},{3,1},{4,2},{5,3},{6,4},{7,5},{8,14},{9,15},{10,... | collective-permute-start | bytes 1179656 | tf_op jit(solution)/shard_map/ppermute | solution.py:21
  (17 other events, 294.2 us)
Sparse Core Ops, SparseCore 0:
  9.1 137.9 all-gather.2

commit v3 on v2

--- a/solution.py
+++ b/solution.py
@@ -21,16 +21,14 @@
     return lax.ppermute(x, "tp", [(i, (i + CORES * step) % count) for i in range(count)])
 
 
-def gather_features(shard, together=False):
+def from_chips(shard):
     chips = lax.axis_size("tp") // CORES
-    got = [shard]
-    got += [to_chip(shard, step) for step in range(1, chips)]
-    if together:
-        other = swap_cores(jnp.stack(got[1:]))
-        swapped = [swap_cores(shard), *[other[i] for i in range(chips - 1)]]
-    else:
-        swapped = [swap_cores(g) for g in got]
-    return [piece for pair in zip(got, swapped) for piece in pair]
+    return [to_chip(shard, step) for step in range(1, chips)]
+
+
+def gather_features(shard):
+    got = [shard, *from_chips(shard)]
+    return [piece for g in got for piece in (g, swap_cores(g))]
 
 
 def chunk_order(me, count):
@@ -344,7 +342,7 @@
     operands = [*pieces, gate_scale, up_scale, far]
     specs = [pl.BlockSpec(memory_space=pl.ANY)] * len(operands)
     specs[chunks] = specs[chunks + 1] = None
-    return call(channel_kernel, "channel", operands, specs, chunks, shards, tall, scratch, flops, 57)
+    return call(channel_kernel, "channel", operands, specs, chunks, shards, tall, scratch, flops, 50)
 
 
 def local(
@@ -386,9 +384,20 @@
 
     far = lax.all_gather(far, "fs")
     ring = Ring(near)
-    for _ in range(ring.count // 2):
+    steps = ring.count // 2
+    ring.advance()
+    shard, *_ = lax.optimization_barrier((tokens, *ring.advance()))
+    got = from_chips(shard)
+    while ring.step < steps - 2:
         ring.advance()
-    mine, theirs = gating(gather_features(tokens, True), ring.held, spatial[0], spatial_bias)
+    *got, _, _ = lax.optimization_barrier((*got, *ring.held[-2:]))
+    other = swap_cores(jnp.stack(got))
+    while ring.step < steps:
+        ring.advance()
+    pieces = [tokens, swap_cores(shard)]
+    for i, piece in enumerate(got):
+        pieces += [piece, other[i]]
+    mine, theirs = gating(pieces, ring.held, spatial[0], spatial_bias)
     resid = (tokens.astype(jnp.float32) + sum_chips(chip_sums(mine, theirs))).astype(jnp.bfloat16)
     mine, theirs = channel(gather_features(resid), gate_scale, up_scale, far)
     pair = chip_sums(mine, theirs)

time: 226 us -> 202 us (0.89)
  waiting for transfers between devices: 105 us -> 89.9 us
  starting transfers between devices: 76.9 us -> 70.4 us
    ppermute x8, starting transfers between devices: 30.4 us -> 12.8 us  [swap_cores(): return lax.ppermute(x, 'tp', [(i, i ^ 1) for i in range(count)])]
    ppermute x15, starting transfers between devices: 28 us -> 40.2 us  [pass_on(): lax.ppermute(x, 'fs', [(i, (i + step) % count) for i in range(count)])]
    ppermute x12, waiting for transfers between devices: 59.2 us -> 49.1 us  [to_chip(): lax.ppermute(x, 'tp', [(i, (i + CORES * step) % count) for i in range(cou...]
    ppermute x15, waiting for transfers between devices: 38.4 us -> 32.5 us  [pass_on(): lax.ppermute(x, 'fs', [(i, (i + step) % count) for i in range(count)])]
  transfers between devices with their start and end apart: 36 -> 36, of which waited for: 23 -> 20; matrix products, arithmetic and copies ran while one was open for 0% -> 0% of each run, Pallas kernels for 3% -> 3%
where the time goes in v3:
time: 202 us
  waiting for transfers between devices  89.9 us (45%)
  starting transfers between devices  70.4 us (35%)
  Pallas kernels  23.5 us (12%)
  between operations  13.6 us (7%)
  other arithmetic  4.36 us (2%)
    ppermute x12, waiting for transfers between devices, to_chip(): lax.ppermute(x, 'tp', [(i, (i + CORES * step) % count) for i in range(cou...  49.1 us
    ppermute x15, starting transfers between devices, pass_on(): lax.ppermute(x, 'fs', [(i, (i + step) % count) for i in range(count)])  40.2 us
    ppermute x15, waiting for transfers between devices, pass_on(): lax.ppermute(x, 'fs', [(i, (i + step) % count) for i in range(count)])  32.5 us
    pallas_call x2, Pallas kernels, call(): pl.pallas_call(functools.partial(kernel, chunks=chunks, shards=shards, ta...  21.1 us
    ppermute x12, starting transfers between devices, to_chip(): lax.ppermute(x, 'tp', [(i, (i + CORES * step) % count) for i in range(cou...  17.4 us
    ppermute x8, starting transfers between devices, swap_cores(): return lax.ppermute(x, 'tp', [(i, i ^ 1) for i in range(count)])  12.8 us
    ppermute x8, waiting for transfers between devices, swap_cores(): return lax.ppermute(x, 'tp', [(i, i ^ 1) for i in range(count)])  8.23 us
  transfers between devices with their start and end apart: 36, of which 20 were waited for; matrix products, arithmetic and copies ran while one was open for 0% of the time, Pallas kernels for 3%

profile of v3, /device:TPU:33, one launch (start us, length us, event | category | flops | bytes accessed | tf_op | source)
XLA Modules:
  0.0 201.8 jit_solution(6378108795877409544)
XLA Ops:
  6.6 2.4 %fold.1 = (bf16[128,384]{1,0:T(8,128)(2,1)}, bf16[2112,128]{1,0:T(8,128)(2,1)}) custom-call(f32[16,128]{1,0:T(8,128)} %bitcast.55, f32[128,128]{1,0:T(8,128)} %u_ref.1, f32[128,128]{1,0:T(8,128)} %v_ref.1, f32[128,128]{1,0:T(8,128)} %mix_ref.1, f32[1,128]{1,0:T(1,128)} %bitcast.57, f32[1,128]{1,0:T(1,128)} %bitcast.58, f32[1,128]{1,0:T(1,128)} %mix_scale_ref.1, ...), custom_call_target="tpu_custom_call" | custom-call | flops 4194304 | bytes 1048576 | tf_op jit(solution)/shard_map/fold/pallas_call | solution.py:286
  9.0 3.4 %collective-permute-start = (bf16[128,384]{1,0:T(8,128)(2,1)}, bf16[128,384]{1,0:T(8,128)(2,1)S(1)}, u32[]{:S(2)}, u32[]{:S(2)}) collective-permute-start(bf16[128,384]{1,0:T(8,128)(2,1)} %get-tuple-element.30.refs_8_), channel_id=1, source_target_pairs={{0,8},{8,16},{16,24},{24,32},{32,40},{40,48},{48,56},{56,64},{64,7... | collective-permute-start | bytes 294920 | tf_op jit(solution)/shard_map/ppermute | solution.py:64
  12.4 19.7 %collective-permute-start.2 = (bf16[128,384]{1,0:T(8,128)(2,1)}, bf16[128,384]{1,0:T(8,128)(2,1)S(1)}, u32[]{:S(2)}, u32[]{:S(2)}) collective-permute-start(bf16[128,384]{1,0:T(8,128)(2,1)} %get-tuple-element.30.refs_8_), channel_id=1, source_target_pairs={{0,120},{8,0},{16,8},{24,16},{32,24},{40,32},{48,40},{56,48},{64,5... | collective-permute-start | bytes 294920 | tf_op jit(solution)/shard_map/ppermute | solution.py:64
  32.1 2.6 %collective-permute-done.refs_9_ = bf16[128,384]{1,0:T(8,128)(2,1)S(1)} collective-permute-done((bf16[128,384]{1,0:T(8,128)(2,1)}, bf16[128,384]{1,0:T(8,128)(2,1)S(1)}, u32[]{:S(2)}, u32[]{:S(2)}) %collective-permute-start) | collective-permute-done | bytes 98336 | tf_op jit(solution)/shard_map/ppermute | solution.py:64
  34.8 2.7 %collective-permute-start.3 = (bf16[128,384]{1,0:T(8,128)(2,1)S(1)}, bf16[128,384]{1,0:T(8,128)(2,1)S(1)}, u32[]{:S(2)}, u32[]{:S(2)}) collective-permute-start(bf16[128,384]{1,0:T(8,128)(2,1)S(1)} %collective-permute-done.2.refs_10_), channel_id=1, source_target_pairs={{0,120},{8,0},{16,8},{24,16},{32,24},{40,32},{48,40},{56,48},{64,5... | collective-permute-start | bytes 294920 | tf_op jit(solution)/shard_map/ppermute | solution.py:64
  37.5 2.0 collective-permute-done.1.refs_11_
  39.6 3.1 %collective-permute-start.10 = (bf16[128,384]{1,0:T(8,128)(2,1)S(1)}, bf16[128,384]{1,0:T(8,128)(2,1)S(1)}, u32[]{:S(2)}, u32[]{:S(2)}) collective-permute-start(bf16[128,384]{1,0:T(8,128)(2,1)S(1)} %collective-permute-done.3.refs_12_), channel_id=1, source_target_pairs={{0,120},{8,0},{16,8},{24,16},{32,24},{40,32},{48,40},{56,48},{64,5... | collective-permute-start | bytes 294920 | tf_op jit(solution)/shard_map/ppermute | solution.py:64
  42.7 2.1 %collective-permute-start.5 = (bf16[768,256]{1,0:T(8,128)(2,1)S(1)}, bf16[768,256]{1,0:T(8,128)(2,1)S(1)}, u32[]{:S(2)}, u32[]{:S(2)}) collective-permute-start(bf16[768,256]{1,0:T(8,128)(2,1)S(1)} %copy-done), channel_id=1, source_target_pairs={{0,2},{1,3},{2,4},{3,5},{4,6},{5,7},{6,0},{7,1},{8,10},{9,11},{10,... | collective-permute-start | bytes 1179656 | tf_op jit(solution)/shard_map/ppermute | solution.py:21
  44.9 3.5 %collective-permute-start.6 = (bf16[768,256]{1,0:T(8,128)(2,1)S(1)}, bf16[768,256]{1,0:T(8,128)(2,1)S(1)}, u32[]{:S(2)}, u32[]{:S(2)}) collective-permute-start(bf16[768,256]{1,0:T(8,128)(2,1)S(1)} %copy-done), channel_id=1, source_target_pairs={{0,4},{1,5},{2,6},{3,7},{4,0},{5,1},{6,2},{7,3},{8,12},{9,13},{10,... | collective-permute-start | bytes 1179656 | tf_op jit(solution)/shard_map/ppermute | solution.py:21
  49.0 2.7 %collective-permute-start.12 = (bf16[128,384]{1,0:T(8,128)(2,1)S(1)}, bf16[128,384]{1,0:T(8,128)(2,1)S(1)}, u32[]{:S(2)}, u32[]{:S(2)}) collective-permute-start(bf16[128,384]{1,0:T(8,128)(2,1)S(1)} %collective-permute-done.10.refs_14_), channel_id=1, source_target_pairs={{0,120},{8,0},{16,8},{24,16},{32,24},{40,32},{48,40},{56,48},{64,5... | collective-permute-start | bytes 294920 | tf_op jit(solution)/shard_map/ppermute | solution.py:64
  51.7 4.6 %collective-permute-done.9.refs_15_ = bf16[128,384]{1,0:T(8,128)(2,1)S(1)} collective-permute-done((bf16[128,384]{1,0:T(8,128)(2,1)S(1)}, bf16[128,384]{1,0:T(8,128)(2,1)S(1)}, u32[]{:S(2)}, u32[]{:S(2)}) %collective-permute-start.9) | collective-permute-done | bytes 98336 | tf_op jit(solution)/shard_map/ppermute | solution.py:64
  56.3 2.7 %collective-permute-start.14 = (bf16[128,384]{1,0:T(8,128)(2,1)S(1)}, bf16[128,384]{1,0:T(8,128)(2,1)S(1)}, u32[]{:S(2)}, u32[]{:S(2)}) collective-permute-start(bf16[128,384]{1,0:T(8,128)(2,1)S(1)} %collective-permute-done.12.refs_16_), channel_id=1, source_target_pairs={{0,120},{8,0},{16,8},{24,16},{32,24},{40,32},{48,40},{56,48},{64,5... | collective-permute-start | bytes 294920 | tf_op jit(solution)/shard_map/ppermute | solution.py:64
  59.0 4.7 %collective-permute-done.11.refs_17_ = bf16[128,384]{1,0:T(8,128)(2,1)S(1)} collective-permute-done((bf16[128,384]{1,0:T(8,128)(2,1)S(1)}, bf16[128,384]{1,0:T(8,128)(2,1)S(1)}, u32[]{:S(2)}, u32[]{:S(2)}) %collective-permute-start.11) | collective-permute-done | bytes 98336 | tf_op jit(solution)/shard_map/ppermute | solution.py:64
  63.7 2.8 %collective-permute-start.15 = (bf16[128,384]{1,0:T(8,128)(2,1)S(1)}, bf16[128,384]{1,0:T(8,128)(2,1)S(1)}, u32[]{:S(2)}, u32[]{:S(2)}) collective-permute-start(bf16[128,384]{1,0:T(8,128)(2,1)S(1)} %collective-permute-done.14.refs_18_), channel_id=1, source_target_pairs={{0,120},{8,0},{16,8},{24,16},{32,24},{40,32},{48,40},{56,48},{64,5... | collective-permute-start | bytes 294920 | tf_op jit(solution)/shard_map/ppermute | solution.py:64
  66.5 4.9 %collective-permute-done.13.refs_19_ = bf16[128,384]{1,0:T(8,128)(2,1)S(1)} collective-permute-done((bf16[128,384]{1,0:T(8,128)(2,1)S(1)}, bf16[128,384]{1,0:T(8,128)(2,1)S(1)}, u32[]{:S(2)}, u32[]{:S(2)}) %collective-permute-start.13) | collective-permute-done | bytes 98336 | tf_op jit(solution)/shard_map/ppermute | solution.py:64
  71.6 6.8 %collective-permute-start.16 = (bf16[3,768,256]{2,1,0:T(8,128)(2,1)S(1)}, bf16[3,768,256]{2,1,0:T(8,128)(2,1)S(1)}, u32[]{:S(2)}, u32[]{:S(2)}) collective-permute-start(bf16[3,768,256]{2,1,0:T(8,128)(2,1)S(1)} %pad_maximum_fusion), channel_id=1, source_target_pairs={{0,1},{1,0},{2,3},{3,2},{4,5},{5,4},{6,7},{7,6},{8,9},{9,8},{10,11... | collective-permute-start | bytes 3538952 | tf_op jit(solution)/shard_map/ppermute | solution.py:16
  78.6 3.1 %collective-permute-start.18 = (bf16[128,384]{1,0:T(8,128)(2,1)S(1)}, bf16[128,384]{1,0:T(8,128)(2,1)S(1)}, u32[]{:S(2)}, u32[]{:S(2)}) collective-permute-start(bf16[128,384]{1,0:T(8,128)(2,1)S(1)} %collective-permute-done.15.refs_20_), channel_id=1, source_target_pairs={{0,120},{8,0},{16,8},{24,16},{32,24},{40,32},{48,40},{56,48},{64,5... | collective-permute-start | bytes 294920 | tf_op jit(solution)/shard_map/ppermute | solution.py:64
  81.7 5.5 %collective-permute-done.17.refs_21_ = bf16[128,384]{1,0:T(8,128)(2,1)S(1)} collective-permute-done((bf16[128,384]{1,0:T(8,128)(2,1)S(1)}, bf16[128,384]{1,0:T(8,128)(2,1)S(1)}, u32[]{:S(2)}, u32[]{:S(2)}) %collective-permute-start.17) | collective-permute-done | bytes 98336 | tf_op jit(solution)/shard_map/ppermute | solution.py:64
  87.3 7.9 %collective-permute-done.19.refs_23_ = bf16[128,384]{1,0:T(8,128)(2,1)S(1)} collective-permute-done((bf16[128,384]{1,0:T(8,128)(2,1)S(1)}, bf16[128,384]{1,0:T(8,128)(2,1)S(1)}, u32[]{:S(2)}, u32[]{:S(2)}) %collective-permute-start.19) | collective-permute-done | bytes 98336 | tf_op jit(solution)/shard_map/ppermute | solution.py:64
  95.3 7.0 %gating.1 = (bf16[4,768,256]{2,1,0:T(8,128)(2,1)S(1)}, bf16[4,768,256]{2,1,0:T(8,128)(2,1)S(1)}) custom-call(bf16[768,256]{1,0:T(8,128)(2,1)S(1)} %copy-done, bf16[768,256]{1,0:T(8,128)(2,1)S(1)} %collective-permute-done.4.refs_1_, bf16[768,256]{1,0:T(8,128)(2,1)S(1)} %collective-permute-done.5.refs_2_, bf16[768,256]{1,0:T(8,128)(2,1)S(1)} %get-tuple-element.61.refs_3_, ...), custom_call_target="tpu_custom_call" | custom-call | flops 1233125376 | bytes 1048576 | tf_op jit(solution)/shard_map/gating/pallas_call | solution.py:302
  103.7 3.0 %collective-permute-done.20 = bf16[4,768,256]{2,1,0:T(8,128)(2,1)S(1)} collective-permute-done((bf16[4,768,256]{2,1,0:T(8,128)(2,1)S(1)}, bf16[4,768,256]{2,1,0:T(8,128)(2,1)S(1)}, u32[]{:S(2)}, u32[]{:S(2)}) %collective-permute-start.20) | collective-permute-done | bytes 1572896 | tf_op jit(solution)/shard_map/ppermute | solution.py:16
  110.7 8.4 %collective-permute-done.21 = bf16[768,256]{1,0:T(8,128)(2,1)S(1)} collective-permute-done((bf16[768,256]{1,0:T(8,128)(2,1)S(1)}, bf16[768,256]{1,0:T(8,128)(2,1)S(1)}, u32[]{:S(2)}, u32[]{:S(2)}) %collective-permute-start.21) | collective-permute-done | bytes 393248 | tf_op jit(solution)/shard_map/ppermute | solution.py:21
  119.2 7.6 %collective-permute-done.22 = bf16[768,256]{1,0:T(8,128)(2,1)S(1)} collective-permute-done((bf16[768,256]{1,0:T(8,128)(2,1)S(1)}, bf16[768,256]{1,0:T(8,128)(2,1)S(1)}, u32[]{:S(2)}, u32[]{:S(2)}) %collective-permute-start.22) | collective-permute-done | bytes 393248 | tf_op jit(solution)/shard_map/ppermute | solution.py:21
  129.9 2.7 %collective-permute-start.27 = (bf16[768,256]{1,0:T(8,128)(2,1)S(1)}, bf16[768,256]{1,0:T(8,128)(2,1)S(1)}, u32[]{:S(2)}, u32[]{:S(2)}) collective-permute-start(bf16[768,256]{1,0:T(8,128)(2,1)S(1)} %fusion.7.refs_0_), channel_id=1, source_target_pairs={{0,4},{1,5},{2,6},{3,7},{4,0},{5,1},{6,2},{7,3},{8,12},{9,13},{10,... | collective-permute-start | bytes 1179656 | tf_op jit(solution)/shard_map/ppermute | solution.py:21
  133.8 6.2 %collective-permute-done.25.refs_2_ = bf16[768,256]{1,0:T(8,128)(2,1)S(1)} collective-permute-done((bf16[768,256]{1,0:T(8,128)(2,1)S(1)}, bf16[768,256]{1,0:T(8,128)(2,1)S(1)}, u32[]{:S(2)}, u32[]{:S(2)}) %collective-permute-start.25) | collective-permute-done | bytes 393248 | tf_op jit(solution)/shard_map/ppermute | solution.py:21
  141.5 8.3 %collective-permute-done.27.refs_4_ = bf16[768,256]{1,0:T(8,128)(2,1)S(1)} collective-permute-done((bf16[768,256]{1,0:T(8,128)(2,1)S(1)}, bf16[768,256]{1,0:T(8,128)(2,1)S(1)}, u32[]{:S(2)}, u32[]{:S(2)}) %collective-permute-start.27) | collective-permute-done | bytes 393248 | tf_op jit(solution)/shard_map/ppermute | solution.py:21
  153.0 14.2 %channel.1 = (bf16[4,768,256]{2,1,0:T(8,128)(2,1)}, bf16[4,768,256]{2,1,0:T(8,128)(2,1)}) custom-call(bf16[768,256]{1,0:T(8,128)(2,1)S(1)} %fusion.7.refs_0_, bf16[768,256]{1,0:T(8,128)(2,1)S(1)} %collective-permute-done.24.refs_1_, bf16[768,256]{1,0:T(8,128)(2,1)S(1)} %collective-permute-done.25.refs_2_, ...), custom_call_target="tpu_custom_call" | custom-call | flops 6643777536 | bytes 1048576 | tf_op jit(solution)/shard_map/channel/pallas_call | solution.py:302
  167.6 3.3 %collective-permute-done.31 = bf16[4,768,256]{2,1,0:T(8,128)(2,1)S(1)} collective-permute-done((bf16[4,768,256]{2,1,0:T(8,128)(2,1)}, bf16[4,768,256]{2,1,0:T(8,128)(2,1)S(1)}, u32[]{:S(2)}, u32[]{:S(2)}) %collective-permute-start.31) | collective-permute-done | bytes 1572896 | tf_op jit(solution)/shard_map/ppermute | solution.py:16
  172.6 2.5 %collective-permute-start.33 = (bf16[768,256]{1,0:T(8,128)(2,1)S(1)}, bf16[768,256]{1,0:T(8,128)(2,1)S(1)}, u32[]{:S(2)}, u32[]{:S(2)}) collective-permute-start(bf16[768,256]{1,0:T(8,128)(2,1)S(1)} %get-tuple-element.55), channel_id=1, source_target_pairs={{0,4},{1,5},{2,6},{3,7},{4,0},{5,1},{6,2},{7,3},{8,12},{9,13},{10,... | collective-permute-start | bytes 1179656 | tf_op jit(solution)/shard_map/ppermute | solution.py:21
  175.2 9.0 %collective-permute-done.32 = bf16[768,256]{1,0:T(8,128)(2,1)S(1)} collective-permute-done((bf16[768,256]{1,0:T(8,128)(2,1)S(1)}, bf16[768,256]{1,0:T(8,128)(2,1)S(1)}, u32[]{:S(2)}, u32[]{:S(2)}) %collective-permute-start.32) | collective-permute-done | bytes 393248 | tf_op jit(solution)/shard_map/ppermute | solution.py:21
  184.3 8.1 %collective-permute-done.33 = bf16[768,256]{1,0:T(8,128)(2,1)S(1)} collective-permute-done((bf16[768,256]{1,0:T(8,128)(2,1)S(1)}, bf16[768,256]{1,0:T(8,128)(2,1)S(1)}, u32[]{:S(2)}, u32[]{:S(2)}) %collective-permute-start.33) | collective-permute-done | bytes 393248 | tf_op jit(solution)/shard_map/ppermute | solution.py:21
  192.9 2.1 %fusion.3 = bf16[768,256]{1,0:T(8,128)(2,1)} fusion(bf16[768,256]{1,0:T(8,128)(2,1)S(1)} %collective-permute-done.34, bf16[768,256]{1,0:T(8,128)(2,1)S(1)} %collective-permute-done.33, bf16[768,256]{1,0:T(8,128)(2,1)S(1)} %collective-permute-done.32, bf16[768,256]{1,0:T(8,128)(2,1)S(1)} %fusion.7.refs_0_, ...), kind=kLoop, calls=%fused_computation.5 | loop fusion | flops 2359296 | bytes 2752512 | tf_op jit(solution)/shard_map/convert_element_type | solution.py:404
  (62 shorter events, 18.3 us)
Async XLA Ops:
  6.5 146.4 %all-gather.3.cloned.1.call-start = ((), (), s32[]{:S(2)}) async-start(), calls=%async_computation | async-start | bytes 9191424 | tf_op jit(solution)/shard_map/all_gather | solution.py:385
  9.0 25.8 %collective-permute-start = (bf16[128,384]{1,0:T(8,128)(2,1)}, bf16[128,384]{1,0:T(8,128)(2,1)S(1)}, u32[]{:S(2)}, u32[]{:S(2)}) collective-permute-start(bf16[128,384]{1,0:T(8,128)(2,1)} %get-tuple-element.30.refs_8_), channel_id=1, source_target_pairs={{0,8},{8,16},{16,24},{24,32},{32,40},{40,48},{48,56},{56,64},{64,7... | collective-permute-start | bytes 294920 | tf_op jit(solution)/shard_map/ppermute | solution.py:64
  12.4 22.4 %collective-permute-start.2 = (bf16[128,384]{1,0:T(8,128)(2,1)}, bf16[128,384]{1,0:T(8,128)(2,1)S(1)}, u32[]{:S(2)}, u32[]{:S(2)}) collective-permute-start(bf16[128,384]{1,0:T(8,128)(2,1)} %get-tuple-element.30.refs_8_), channel_id=1, source_target_pairs={{0,120},{8,0},{16,8},{24,16},{32,24},{40,32},{48,40},{56,48},{64,5... | collective-permute-start | bytes 294920 | tf_op jit(solution)/shard_map/ppermute | solution.py:64
  34.8 4.7 %collective-permute-start.1 = (bf16[128,384]{1,0:T(8,128)(2,1)S(1)}, bf16[128,384]{1,0:T(8,128)(2,1)S(1)}, u32[]{:S(2)}, u32[]{:S(2)}) collective-permute-start(bf16[128,384]{1,0:T(8,128)(2,1)S(1)} %collective-permute-done.refs_9_), channel_id=1, source_target_pairs={{0,8},{8,16},{16,24},{24,32},{32,40},{40,48},{48,56},{56,64},{64,7... | collective-permute-start | bytes 294920 | tf_op jit(solution)/shard_map/ppermute | solution.py:64
  34.8 4.8 %collective-permute-start.3 = (bf16[128,384]{1,0:T(8,128)(2,1)S(1)}, bf16[128,384]{1,0:T(8,128)(2,1)S(1)}, u32[]{:S(2)}, u32[]{:S(2)}) collective-permute-start(bf16[128,384]{1,0:T(8,128)(2,1)S(1)} %collective-permute-done.2.refs_10_), channel_id=1, source_target_pairs={{0,120},{8,0},{16,8},{24,16},{32,24},{40,32},{48,40},{56,48},{64,5... | collective-permute-start | bytes 294920 | tf_op jit(solution)/shard_map/ppermute | solution.py:64
  39.5 9.5 %collective-permute-start.8 = (bf16[128,384]{1,0:T(8,128)(2,1)S(1)}, bf16[128,384]{1,0:T(8,128)(2,1)S(1)}, u32[]{:S(2)}, u32[]{:S(2)}) collective-permute-start(bf16[128,384]{1,0:T(8,128)(2,1)S(1)} %collective-permute-done.1.refs_11_), channel_id=1, source_target_pairs={{0,8},{8,16},{16,24},{24,32},{32,40},{40,48},{48,56},{56,64},{64,7... | collective-permute-start | bytes 294920 | tf_op jit(solution)/shard_map/ppermute | solution.py:64
  39.6 9.4 %collective-permute-start.10 = (bf16[128,384]{1,0:T(8,128)(2,1)S(1)}, bf16[128,384]{1,0:T(8,128)(2,1)S(1)}, u32[]{:S(2)}, u32[]{:S(2)}) collective-permute-start(bf16[128,384]{1,0:T(8,128)(2,1)S(1)} %collective-permute-done.3.refs_12_), channel_id=1, source_target_pairs={{0,120},{8,0},{16,8},{24,16},{32,24},{40,32},{48,40},{56,48},{64,5... | collective-permute-start | bytes 294920 | tf_op jit(solution)/shard_map/ppermute | solution.py:64
  42.7 28.7 %collective-permute-start.5 = (bf16[768,256]{1,0:T(8,128)(2,1)S(1)}, bf16[768,256]{1,0:T(8,128)(2,1)S(1)}, u32[]{:S(2)}, u32[]{:S(2)}) collective-permute-start(bf16[768,256]{1,0:T(8,128)(2,1)S(1)} %copy-done), channel_id=1, source_target_pairs={{0,2},{1,3},{2,4},{3,5},{4,6},{5,7},{6,0},{7,1},{8,10},{9,11},{10,... | collective-permute-start | bytes 1179656 | tf_op jit(solution)/shard_map/ppermute | solution.py:21
  44.9 26.5 %collective-permute-start.6 = (bf16[768,256]{1,0:T(8,128)(2,1)S(1)}, bf16[768,256]{1,0:T(8,128)(2,1)S(1)}, u32[]{:S(2)}, u32[]{:S(2)}) collective-permute-start(bf16[768,256]{1,0:T(8,128)(2,1)S(1)} %copy-done), channel_id=1, source_target_pairs={{0,4},{1,5},{2,6},{3,7},{4,0},{5,1},{6,2},{7,3},{8,12},{9,13},{10,... | collective-permute-start | bytes 1179656 | tf_op jit(solution)/shard_map/ppermute | solution.py:21
  48.4 23.0 %collective-permute-start.7 = (bf16[768,256]{1,0:T(8,128)(2,1)S(1)}, bf16[768,256]{1,0:T(8,128)(2,1)S(1)}, u32[]{:S(2)}, u32[]{:S(2)}) collective-permute-start(bf16[768,256]{1,0:T(8,128)(2,1)S(1)} %copy-done), channel_id=1, source_target_pairs={{0,6},{1,7},{2,0},{3,1},{4,2},{5,3},{6,4},{7,5},{8,14},{9,15},{10,... | collective-permute-start | bytes 1179656 | tf_op jit(solution)/shard_map/ppermute | solution.py:21
  49.0 7.3 %collective-permute-start.9 = (bf16[128,384]{1,0:T(8,128)(2,1)S(1)}, bf16[128,384]{1,0:T(8,128)(2,1)S(1)}, u32[]{:S(2)}, u32[]{:S(2)}) collective-permute-start(bf16[128,384]{1,0:T(8,128)(2,1)S(1)} %collective-permute-done.8.refs_13_), channel_id=1, source_target_pairs={{0,8},{8,16},{16,24},{24,32},{32,40},{40,48},{48,56},{56,64},{64,7... | collective-permute-start | bytes 294920 | tf_op jit(solution)/shard_map/ppermute | solution.py:64
  49.0 7.3 %collective-permute-start.12 = (bf16[128,384]{1,0:T(8,128)(2,1)S(1)}, bf16[128,384]{1,0:T(8,128)(2,1)S(1)}, u32[]{:S(2)}, u32[]{:S(2)}) collective-permute-start(bf16[128,384]{1,0:T(8,128)(2,1)S(1)} %collective-permute-done.10.refs_14_), channel_id=1, source_target_pairs={{0,120},{8,0},{16,8},{24,16},{32,24},{40,32},{48,40},{56,48},{64,5... | collective-permute-start | bytes 294920 | tf_op jit(solution)/shard_map/ppermute | solution.py:64
  56.3 7.4 %collective-permute-start.11 = (bf16[128,384]{1,0:T(8,128)(2,1)S(1)}, bf16[128,384]{1,0:T(8,128)(2,1)S(1)}, u32[]{:S(2)}, u32[]{:S(2)}) collective-permute-start(bf16[128,384]{1,0:T(8,128)(2,1)S(1)} %collective-permute-done.9.refs_15_), channel_id=1, source_target_pairs={{0,8},{8,16},{16,24},{24,32},{32,40},{40,48},{48,56},{56,64},{64,7... | collective-permute-start | bytes 294920 | tf_op jit(solution)/shard_map/ppermute | solution.py:64
  56.3 7.4 %collective-permute-start.14 = (bf16[128,384]{1,0:T(8,128)(2,1)S(1)}, bf16[128,384]{1,0:T(8,128)(2,1)S(1)}, u32[]{:S(2)}, u32[]{:S(2)}) collective-permute-start(bf16[128,384]{1,0:T(8,128)(2,1)S(1)} %collective-permute-done.12.refs_16_), channel_id=1, source_target_pairs={{0,120},{8,0},{16,8},{24,16},{32,24},{40,32},{48,40},{56,48},{64,5... | collective-permute-start | bytes 294920 | tf_op jit(solution)/shard_map/ppermute | solution.py:64
  63.7 7.7 %collective-permute-start.13 = (bf16[128,384]{1,0:T(8,128)(2,1)S(1)}, bf16[128,384]{1,0:T(8,128)(2,1)S(1)}, u32[]{:S(2)}, u32[]{:S(2)}) collective-permute-start(bf16[128,384]{1,0:T(8,128)(2,1)S(1)} %collective-permute-done.11.refs_17_), channel_id=1, source_target_pairs={{0,8},{8,16},{16,24},{24,32},{32,40},{40,48},{48,56},{56,64},{64,7... | collective-permute-start | bytes 294920 | tf_op jit(solution)/shard_map/ppermute | solution.py:64
  63.7 7.7 %collective-permute-start.15 = (bf16[128,384]{1,0:T(8,128)(2,1)S(1)}, bf16[128,384]{1,0:T(8,128)(2,1)S(1)}, u32[]{:S(2)}, u32[]{:S(2)}) collective-permute-start(bf16[128,384]{1,0:T(8,128)(2,1)S(1)} %collective-permute-done.14.refs_18_), channel_id=1, source_target_pairs={{0,120},{8,0},{16,8},{24,16},{32,24},{40,32},{48,40},{56,48},{64,5... | collective-permute-start | bytes 294920 | tf_op jit(solution)/shard_map/ppermute | solution.py:64
  71.6 15.6 %collective-permute-start.16 = (bf16[3,768,256]{2,1,0:T(8,128)(2,1)S(1)}, bf16[3,768,256]{2,1,0:T(8,128)(2,1)S(1)}, u32[]{:S(2)}, u32[]{:S(2)}) collective-permute-start(bf16[3,768,256]{2,1,0:T(8,128)(2,1)S(1)} %pad_maximum_fusion), channel_id=1, source_target_pairs={{0,1},{1,0},{2,3},{3,2},{4,5},{5,4},{6,7},{7,6},{8,9},{9,8},{10,11... | collective-permute-start | bytes 3538952 | tf_op jit(solution)/shard_map/ppermute | solution.py:16
  78.4 8.9 %collective-permute-start.4 = (bf16[768,256]{1,0:T(8,128)(2,1)S(1)}, bf16[768,256]{1,0:T(8,128)(2,1)S(1)}, u32[]{:S(2)}, u32[]{:S(2)}) collective-permute-start(bf16[768,256]{1,0:T(8,128)(2,1)S(1)} %copy-done), channel_id=1, source_target_pairs={{0,1},{1,0},{2,3},{3,2},{4,5},{5,4},{6,7},{7,6},{8,9},{9,8},{10,11... | collective-permute-start | bytes 1179656 | tf_op jit(solution)/shard_map/ppermute | solution.py:16
  78.6 8.7 %collective-permute-start.17 = (bf16[128,384]{1,0:T(8,128)(2,1)S(1)}, bf16[128,384]{1,0:T(8,128)(2,1)S(1)}, u32[]{:S(2)}, u32[]{:S(2)}) collective-permute-start(bf16[128,384]{1,0:T(8,128)(2,1)S(1)} %collective-permute-done.13.refs_19_), channel_id=1, source_target_pairs={{0,8},{8,16},{16,24},{24,32},{32,40},{40,48},{48,56},{56,64},{64,7... | collective-permute-start | bytes 294920 | tf_op jit(solution)/shard_map/ppermute | solution.py:64
  78.6 8.8 %collective-permute-start.18 = (bf16[128,384]{1,0:T(8,128)(2,1)S(1)}, bf16[128,384]{1,0:T(8,128)(2,1)S(1)}, u32[]{:S(2)}, u32[]{:S(2)}) collective-permute-start(bf16[128,384]{1,0:T(8,128)(2,1)S(1)} %collective-permute-done.15.refs_20_), channel_id=1, source_target_pairs={{0,120},{8,0},{16,8},{24,16},{32,24},{40,32},{48,40},{56,48},{64,5... | collective-permute-start | bytes 294920 | tf_op jit(solution)/shard_map/ppermute | solution.py:64
  87.2 8.0 %collective-permute-start.19 = (bf16[128,384]{1,0:T(8,128)(2,1)S(1)}, bf16[128,384]{1,0:T(8,128)(2,1)S(1)}, u32[]{:S(2)}, u32[]{:S(2)}) collective-permute-start(bf16[128,384]{1,0:T(8,128)(2,1)S(1)} %collective-permute-done.17.refs_21_), channel_id=1, source_target_pairs={{0,8},{8,16},{16,24},{24,32},{32,40},{40,48},{48,56},{56,64},{64,7... | collective-permute-start | bytes 294920 | tf_op jit(solution)/shard_map/ppermute | solution.py:64
  107.1 12.1 %collective-permute-start.21 = (bf16[768,256]{1,0:T(8,128)(2,1)S(1)}, bf16[768,256]{1,0:T(8,128)(2,1)S(1)}, u32[]{:S(2)}, u32[]{:S(2)}) collective-permute-start(bf16[768,256]{1,0:T(8,128)(2,1)S(1)} %get-tuple-element.56), channel_id=1, source_target_pairs={{0,2},{1,3},{2,4},{3,5},{4,6},{5,7},{6,0},{7,1},{8,10},{9,11},{10,... | collective-permute-start | bytes 1179656 | tf_op jit(solution)/shard_map/ppermute | solution.py:21
  107.6 19.2 %collective-permute-start.22 = (bf16[768,256]{1,0:T(8,128)(2,1)S(1)}, bf16[768,256]{1,0:T(8,128)(2,1)S(1)}, u32[]{:S(2)}, u32[]{:S(2)}) collective-permute-start(bf16[768,256]{1,0:T(8,128)(2,1)S(1)} %get-tuple-element.58), channel_id=1, source_target_pairs={{0,4},{1,5},{2,6},{3,7},{4,0},{5,1},{6,2},{7,3},{8,12},{9,13},{10,... | collective-permute-start | bytes 1179656 | tf_op jit(solution)/shard_map/ppermute | solution.py:21
  109.5 18.1 %collective-permute-start.23 = (bf16[768,256]{1,0:T(8,128)(2,1)S(1)}, bf16[768,256]{1,0:T(8,128)(2,1)S(1)}, u32[]{:S(2)}, u32[]{:S(2)}) collective-permute-start(bf16[768,256]{1,0:T(8,128)(2,1)S(1)} %get-tuple-element.57), channel_id=1, source_target_pairs={{0,6},{1,7},{2,0},{3,1},{4,2},{5,3},{6,4},{7,5},{8,14},{9,15},{10,... | collective-permute-start | bytes 1179656 | tf_op jit(solution)/shard_map/ppermute | solution.py:21
  127.9 12.1 %collective-permute-start.25 = (bf16[768,256]{1,0:T(8,128)(2,1)S(1)}, bf16[768,256]{1,0:T(8,128)(2,1)S(1)}, u32[]{:S(2)}, u32[]{:S(2)}) collective-permute-start(bf16[768,256]{1,0:T(8,128)(2,1)S(1)} %fusion.7.refs_0_), channel_id=1, source_target_pairs={{0,2},{1,3},{2,4},{3,5},{4,6},{5,7},{6,0},{7,1},{8,10},{9,11},{10,... | collective-permute-start | bytes 1179656 | tf_op jit(solution)/shard_map/ppermute | solution.py:21
  129.9 19.9 %collective-permute-start.27 = (bf16[768,256]{1,0:T(8,128)(2,1)S(1)}, bf16[768,256]{1,0:T(8,128)(2,1)S(1)}, u32[]{:S(2)}, u32[]{:S(2)}) collective-permute-start(bf16[768,256]{1,0:T(8,128)(2,1)S(1)} %fusion.7.refs_0_), channel_id=1, source_target_pairs={{0,4},{1,5},{2,6},{3,7},{4,0},{5,1},{6,2},{7,3},{8,12},{9,13},{10,... | collective-permute-start | bytes 1179656 | tf_op jit(solution)/shard_map/ppermute | solution.py:21
  132.6 18.5 %collective-permute-start.29 = (bf16[768,256]{1,0:T(8,128)(2,1)S(1)}, bf16[768,256]{1,0:T(8,128)(2,1)S(1)}, u32[]{:S(2)}, u32[]{:S(2)}) collective-permute-start(bf16[768,256]{1,0:T(8,128)(2,1)S(1)} %fusion.7.refs_0_), channel_id=1, source_target_pairs={{0,6},{1,7},{2,0},{3,1},{4,2},{5,3},{6,4},{7,5},{8,14},{9,15},{10,... | collective-permute-start | bytes 1179656 | tf_op jit(solution)/shard_map/ppermute | solution.py:21
  132.6 18.5 %collective-permute-start.24 = (bf16[768,256]{1,0:T(8,128)(2,1)S(1)}, bf16[768,256]{1,0:T(8,128)(2,1)S(1)}, u32[]{:S(2)}, u32[]{:S(2)}) collective-permute-start(bf16[768,256]{1,0:T(8,128)(2,1)S(1)} %fusion.7.refs_0_), channel_id=1, source_target_pairs={{0,1},{1,0},{2,3},{3,2},{4,5},{5,4},{6,7},{7,6},{8,9},{9,8},{10,11... | collective-permute-start | bytes 1179656 | tf_op jit(solution)/shard_map/ppermute | solution.py:16
  140.0 11.1 %collective-permute-start.26 = (bf16[768,256]{1,0:T(8,128)(2,1)S(1)}, bf16[768,256]{1,0:T(8,128)(2,1)S(1)}, u32[]{:S(2)}, u32[]{:S(2)}) collective-permute-start(bf16[768,256]{1,0:T(8,128)(2,1)S(1)} %collective-permute-done.25.refs_2_), channel_id=1, source_target_pairs={{0,1},{1,0},{2,3},{3,2},{4,5},{5,4},{6,7},{7,6},{8,9},{9,8},{10,11... | collective-permute-start | bytes 1179656 | tf_op jit(solution)/shard_map/ppermute | solution.py:16
  172.4 11.8 %collective-permute-start.32 = (bf16[768,256]{1,0:T(8,128)(2,1)S(1)}, bf16[768,256]{1,0:T(8,128)(2,1)S(1)}, u32[]{:S(2)}, u32[]{:S(2)}) collective-permute-start(bf16[768,256]{1,0:T(8,128)(2,1)S(1)} %get-tuple-element.53), channel_id=1, source_target_pairs={{0,2},{1,3},{2,4},{3,5},{4,6},{5,7},{6,0},{7,1},{8,10},{9,11},{10,... | collective-permute-start | bytes 1179656 | tf_op jit(solution)/shard_map/ppermute | solution.py:21
  172.6 19.8 %collective-permute-start.33 = (bf16[768,256]{1,0:T(8,128)(2,1)S(1)}, bf16[768,256]{1,0:T(8,128)(2,1)S(1)}, u32[]{:S(2)}, u32[]{:S(2)}) collective-permute-start(bf16[768,256]{1,0:T(8,128)(2,1)S(1)} %get-tuple-element.55), channel_id=1, source_target_pairs={{0,4},{1,5},{2,6},{3,7},{4,0},{5,1},{6,2},{7,3},{8,12},{9,13},{10,... | collective-permute-start | bytes 1179656 | tf_op jit(solution)/shard_map/ppermute | solution.py:21
  175.1 17.8 %collective-permute-start.34 = (bf16[768,256]{1,0:T(8,128)(2,1)S(1)}, bf16[768,256]{1,0:T(8,128)(2,1)S(1)}, u32[]{:S(2)}, u32[]{:S(2)}) collective-permute-start(bf16[768,256]{1,0:T(8,128)(2,1)S(1)} %get-tuple-element.54), channel_id=1, source_target_pairs={{0,6},{1,7},{2,0},{3,1},{4,2},{5,3},{6,4},{7,5},{8,14},{9,15},{10,... | collective-permute-start | bytes 1179656 | tf_op jit(solution)/shard_map/ppermute | solution.py:21
  (10 other events, 211.8 us)
Sparse Core Ops, SparseCore 0:
  9.1 133.6 all-gather.2

commit v4 on v3

--- a/solution.py
+++ b/solution.py
@@ -342,7 +342,7 @@
     operands = [*pieces, gate_scale, up_scale, far]
     specs = [pl.BlockSpec(memory_space=pl.ANY)] * len(operands)
     specs[chunks] = specs[chunks + 1] = None
-    return call(channel_kernel, "channel", operands, specs, chunks, shards, tall, scratch, flops, 50)
+    return call(channel_kernel, "channel", operands, specs, chunks, shards, tall, scratch, flops, 44)
 
 
 def local(

time: 202 us -> 198 us (0.980)
  other arithmetic: 4.36 us -> 2.12 us
  transfers between devices with their start and end apart: 36 -> 36, of which waited for: 20 -> 20; matrix products, arithmetic and copies ran while one was open for 0% -> 0% of each run, Pallas kernels for 3% -> 4%
where the time goes in v4:
time: 198 us
  waiting for transfers between devices  89.6 us (45%)
  starting transfers between devices  70.4 us (36%)
  Pallas kernels  22.2 us (11%)
  between operations  13.6 us (7%)
  other arithmetic  2.12 us (1%)
    ppermute x12, waiting for transfers between devices, to_chip(): lax.ppermute(x, 'tp', [(i, (i + CORES * step) % count) for i in range(cou...  49 us
    ppermute x15, starting transfers between devices, pass_on(): lax.ppermute(x, 'fs', [(i, (i + step) % count) for i in range(count)])  40.2 us
    ppermute x15, waiting for transfers between devices, pass_on(): lax.ppermute(x, 'fs', [(i, (i + step) % count) for i in range(count)])  32.5 us
    pallas_call x2, Pallas kernels, call(): pl.pallas_call(functools.partial(kernel, chunks=chunks, shards=shards, ta...  19.9 us
    ppermute x12, starting transfers between devices, to_chip(): lax.ppermute(x, 'tp', [(i, (i + CORES * step) % count) for i in range(cou...  17.4 us
    ppermute x8, starting transfers between devices, swap_cores(): return lax.ppermute(x, 'tp', [(i, i ^ 1) for i in range(count)])  12.8 us
    ppermute x8, waiting for transfers between devices, swap_cores(): return lax.ppermute(x, 'tp', [(i, i ^ 1) for i in range(count)])  7.99 us
  transfers between devices with their start and end apart: 36, of which 20 were waited for; matrix products, arithmetic and copies ran while one was open for 0% of the time, Pallas kernels for 4%

profile of v4, /device:TPU:33, one launch (start us, length us, event | category | flops | bytes accessed | tf_op | source)
XLA Modules:
  0.0 198.1 jit_solution(2361254871948054165)
XLA Ops:
  6.6 2.4 %fold.1 = (bf16[128,384]{1,0:T(8,128)(2,1)}, bf16[2112,128]{1,0:T(8,128)(2,1)}) custom-call(f32[16,128]{1,0:T(8,128)} %bitcast.55, f32[128,128]{1,0:T(8,128)} %u_ref.1, f32[128,128]{1,0:T(8,128)} %v_ref.1, f32[128,128]{1,0:T(8,128)} %mix_ref.1, f32[1,128]{1,0:T(1,128)} %bitcast.57, f32[1,128]{1,0:T(1,128)} %bitcast.58, f32[1,128]{1,0:T(1,128)} %mix_scale_ref.1, ...), custom_call_target="tpu_custom_call" | custom-call | flops 4194304 | bytes 1048576 | tf_op jit(solution)/shard_map/fold/pallas_call | solution.py:286
  9.0 3.4 %collective-permute-start = (bf16[128,384]{1,0:T(8,128)(2,1)}, bf16[128,384]{1,0:T(8,128)(2,1)S(1)}, u32[]{:S(2)}, u32[]{:S(2)}) collective-permute-start(bf16[128,384]{1,0:T(8,128)(2,1)} %get-tuple-element.30.refs_8_), channel_id=1, source_target_pairs={{0,8},{8,16},{16,24},{24,32},{32,40},{40,48},{48,56},{56,64},{64,7... | collective-permute-start | bytes 294920 | tf_op jit(solution)/shard_map/ppermute | solution.py:64
  12.4 19.7 %collective-permute-start.2 = (bf16[128,384]{1,0:T(8,128)(2,1)}, bf16[128,384]{1,0:T(8,128)(2,1)S(1)}, u32[]{:S(2)}, u32[]{:S(2)}) collective-permute-start(bf16[128,384]{1,0:T(8,128)(2,1)} %get-tuple-element.30.refs_8_), channel_id=1, source_target_pairs={{0,120},{8,0},{16,8},{24,16},{32,24},{40,32},{48,40},{56,48},{64,5... | collective-permute-start | bytes 294920 | tf_op jit(solution)/shard_map/ppermute | solution.py:64
  32.1 2.6 %collective-permute-done.refs_9_ = bf16[128,384]{1,0:T(8,128)(2,1)S(1)} collective-permute-done((bf16[128,384]{1,0:T(8,128)(2,1)}, bf16[128,384]{1,0:T(8,128)(2,1)S(1)}, u32[]{:S(2)}, u32[]{:S(2)}) %collective-permute-start) | collective-permute-done | bytes 98336 | tf_op jit(solution)/shard_map/ppermute | solution.py:64
  34.8 2.7 %collective-permute-start.3 = (bf16[128,384]{1,0:T(8,128)(2,1)S(1)}, bf16[128,384]{1,0:T(8,128)(2,1)S(1)}, u32[]{:S(2)}, u32[]{:S(2)}) collective-permute-start(bf16[128,384]{1,0:T(8,128)(2,1)S(1)} %collective-permute-done.2.refs_10_), channel_id=1, source_target_pairs={{0,120},{8,0},{16,8},{24,16},{32,24},{40,32},{48,40},{56,48},{64,5... | collective-permute-start | bytes 294920 | tf_op jit(solution)/shard_map/ppermute | solution.py:64
  37.5 2.0 %collective-permute-done.1.refs_11_ = bf16[128,384]{1,0:T(8,128)(2,1)S(1)} collective-permute-done((bf16[128,384]{1,0:T(8,128)(2,1)S(1)}, bf16[128,384]{1,0:T(8,128)(2,1)S(1)}, u32[]{:S(2)}, u32[]{:S(2)}) %collective-permute-start.1) | collective-permute-done | bytes 98336 | tf_op jit(solution)/shard_map/ppermute | solution.py:64
  39.6 3.1 %collective-permute-start.10 = (bf16[128,384]{1,0:T(8,128)(2,1)S(1)}, bf16[128,384]{1,0:T(8,128)(2,1)S(1)}, u32[]{:S(2)}, u32[]{:S(2)}) collective-permute-start(bf16[128,384]{1,0:T(8,128)(2,1)S(1)} %collective-permute-done.3.refs_12_), channel_id=1, source_target_pairs={{0,120},{8,0},{16,8},{24,16},{32,24},{40,32},{48,40},{56,48},{64,5... | collective-permute-start | bytes 294920 | tf_op jit(solution)/shard_map/ppermute | solution.py:64
  42.7 2.1 %collective-permute-start.5 = (bf16[768,256]{1,0:T(8,128)(2,1)S(1)}, bf16[768,256]{1,0:T(8,128)(2,1)S(1)}, u32[]{:S(2)}, u32[]{:S(2)}) collective-permute-start(bf16[768,256]{1,0:T(8,128)(2,1)S(1)} %copy-done), channel_id=1, source_target_pairs={{0,2},{1,3},{2,4},{3,5},{4,6},{5,7},{6,0},{7,1},{8,10},{9,11},{10,... | collective-permute-start | bytes 1179656 | tf_op jit(solution)/shard_map/ppermute | solution.py:21
  44.9 3.5 %collective-permute-start.6 = (bf16[768,256]{1,0:T(8,128)(2,1)S(1)}, bf16[768,256]{1,0:T(8,128)(2,1)S(1)}, u32[]{:S(2)}, u32[]{:S(2)}) collective-permute-start(bf16[768,256]{1,0:T(8,128)(2,1)S(1)} %copy-done), channel_id=1, source_target_pairs={{0,4},{1,5},{2,6},{3,7},{4,0},{5,1},{6,2},{7,3},{8,12},{9,13},{10,... | collective-permute-start | bytes 1179656 | tf_op jit(solution)/shard_map/ppermute | solution.py:21
  49.0 2.7 %collective-permute-start.12 = (bf16[128,384]{1,0:T(8,128)(2,1)S(1)}, bf16[128,384]{1,0:T(8,128)(2,1)S(1)}, u32[]{:S(2)}, u32[]{:S(2)}) collective-permute-start(bf16[128,384]{1,0:T(8,128)(2,1)S(1)} %collective-permute-done.10.refs_14_), channel_id=1, source_target_pairs={{0,120},{8,0},{16,8},{24,16},{32,24},{40,32},{48,40},{56,48},{64,5... | collective-permute-start | bytes 294920 | tf_op jit(solution)/shard_map/ppermute | solution.py:64
  51.7 4.6 %collective-permute-done.9.refs_15_ = bf16[128,384]{1,0:T(8,128)(2,1)S(1)} collective-permute-done((bf16[128,384]{1,0:T(8,128)(2,1)S(1)}, bf16[128,384]{1,0:T(8,128)(2,1)S(1)}, u32[]{:S(2)}, u32[]{:S(2)}) %collective-permute-start.9) | collective-permute-done | bytes 98336 | tf_op jit(solution)/shard_map/ppermute | solution.py:64
  56.3 2.7 %collective-permute-start.14 = (bf16[128,384]{1,0:T(8,128)(2,1)S(1)}, bf16[128,384]{1,0:T(8,128)(2,1)S(1)}, u32[]{:S(2)}, u32[]{:S(2)}) collective-permute-start(bf16[128,384]{1,0:T(8,128)(2,1)S(1)} %collective-permute-done.12.refs_16_), channel_id=1, source_target_pairs={{0,120},{8,0},{16,8},{24,16},{32,24},{40,32},{48,40},{56,48},{64,5... | collective-permute-start | bytes 294920 | tf_op jit(solution)/shard_map/ppermute | solution.py:64
  59.0 4.7 %collective-permute-done.11.refs_17_ = bf16[128,384]{1,0:T(8,128)(2,1)S(1)} collective-permute-done((bf16[128,384]{1,0:T(8,128)(2,1)S(1)}, bf16[128,384]{1,0:T(8,128)(2,1)S(1)}, u32[]{:S(2)}, u32[]{:S(2)}) %collective-permute-start.11) | collective-permute-done | bytes 98336 | tf_op jit(solution)/shard_map/ppermute | solution.py:64
  63.7 2.8 %collective-permute-start.15 = (bf16[128,384]{1,0:T(8,128)(2,1)S(1)}, bf16[128,384]{1,0:T(8,128)(2,1)S(1)}, u32[]{:S(2)}, u32[]{:S(2)}) collective-permute-start(bf16[128,384]{1,0:T(8,128)(2,1)S(1)} %collective-permute-done.14.refs_18_), channel_id=1, source_target_pairs={{0,120},{8,0},{16,8},{24,16},{32,24},{40,32},{48,40},{56,48},{64,5... | collective-permute-start | bytes 294920 | tf_op jit(solution)/shard_map/ppermute | solution.py:64
  66.5 4.9 %collective-permute-done.13.refs_19_ = bf16[128,384]{1,0:T(8,128)(2,1)S(1)} collective-permute-done((bf16[128,384]{1,0:T(8,128)(2,1)S(1)}, bf16[128,384]{1,0:T(8,128)(2,1)S(1)}, u32[]{:S(2)}, u32[]{:S(2)}) %collective-permute-start.13) | collective-permute-done | bytes 98336 | tf_op jit(solution)/shard_map/ppermute | solution.py:64
  71.6 6.8 %collective-permute-start.16 = (bf16[3,768,256]{2,1,0:T(8,128)(2,1)S(1)}, bf16[3,768,256]{2,1,0:T(8,128)(2,1)S(1)}, u32[]{:S(2)}, u32[]{:S(2)}) collective-permute-start(bf16[3,768,256]{2,1,0:T(8,128)(2,1)S(1)} %pad_maximum_fusion), channel_id=1, source_target_pairs={{0,1},{1,0},{2,3},{3,2},{4,5},{5,4},{6,7},{7,6},{8,9},{9,8},{10,11... | collective-permute-start | bytes 3538952 | tf_op jit(solution)/shard_map/ppermute | solution.py:16
  78.6 3.1 %collective-permute-start.18 = (bf16[128,384]{1,0:T(8,128)(2,1)S(1)}, bf16[128,384]{1,0:T(8,128)(2,1)S(1)}, u32[]{:S(2)}, u32[]{:S(2)}) collective-permute-start(bf16[128,384]{1,0:T(8,128)(2,1)S(1)} %collective-permute-done.15.refs_20_), channel_id=1, source_target_pairs={{0,120},{8,0},{16,8},{24,16},{32,24},{40,32},{48,40},{56,48},{64,5... | collective-permute-start | bytes 294920 | tf_op jit(solution)/shard_map/ppermute | solution.py:64
  81.7 5.5 %collective-permute-done.17.refs_21_ = bf16[128,384]{1,0:T(8,128)(2,1)S(1)} collective-permute-done((bf16[128,384]{1,0:T(8,128)(2,1)S(1)}, bf16[128,384]{1,0:T(8,128)(2,1)S(1)}, u32[]{:S(2)}, u32[]{:S(2)}) %collective-permute-start.17) | collective-permute-done | bytes 98336 | tf_op jit(solution)/shard_map/ppermute | solution.py:64
  87.3 7.9 %collective-permute-done.19.refs_23_ = bf16[128,384]{1,0:T(8,128)(2,1)S(1)} collective-permute-done((bf16[128,384]{1,0:T(8,128)(2,1)S(1)}, bf16[128,384]{1,0:T(8,128)(2,1)S(1)}, u32[]{:S(2)}, u32[]{:S(2)}) %collective-permute-start.19) | collective-permute-done | bytes 98336 | tf_op jit(solution)/shard_map/ppermute | solution.py:64
  95.3 7.0 %gating.1 = (bf16[4,768,256]{2,1,0:T(8,128)(2,1)S(1)}, bf16[4,768,256]{2,1,0:T(8,128)(2,1)S(1)}) custom-call(bf16[768,256]{1,0:T(8,128)(2,1)S(1)} %copy-done, bf16[768,256]{1,0:T(8,128)(2,1)S(1)} %collective-permute-done.4.refs_1_, bf16[768,256]{1,0:T(8,128)(2,1)S(1)} %collective-permute-done.5.refs_2_, bf16[768,256]{1,0:T(8,128)(2,1)S(1)} %get-tuple-element.61.refs_3_, ...), custom_call_target="tpu_custom_call" | custom-call | flops 1233125376 | bytes 1048576 | tf_op jit(solution)/shard_map/gating/pallas_call | solution.py:302
  103.7 3.0 %collective-permute-done.20 = bf16[4,768,256]{2,1,0:T(8,128)(2,1)S(1)} collective-permute-done((bf16[4,768,256]{2,1,0:T(8,128)(2,1)S(1)}, bf16[4,768,256]{2,1,0:T(8,128)(2,1)S(1)}, u32[]{:S(2)}, u32[]{:S(2)}) %collective-permute-start.20) | collective-permute-done | bytes 1572896 | tf_op jit(solution)/shard_map/ppermute | solution.py:16
  110.7 8.4 %collective-permute-done.21 = bf16[768,256]{1,0:T(8,128)(2,1)S(1)} collective-permute-done((bf16[768,256]{1,0:T(8,128)(2,1)S(1)}, bf16[768,256]{1,0:T(8,128)(2,1)S(1)}, u32[]{:S(2)}, u32[]{:S(2)}) %collective-permute-start.21) | collective-permute-done | bytes 393248 | tf_op jit(solution)/shard_map/ppermute | solution.py:21
  119.2 7.6 %collective-permute-done.22 = bf16[768,256]{1,0:T(8,128)(2,1)S(1)} collective-permute-done((bf16[768,256]{1,0:T(8,128)(2,1)S(1)}, bf16[768,256]{1,0:T(8,128)(2,1)S(1)}, u32[]{:S(2)}, u32[]{:S(2)}) %collective-permute-start.22) | collective-permute-done | bytes 393248 | tf_op jit(solution)/shard_map/ppermute | solution.py:21
  127.9 2.0 collective-permute-start.25
  129.9 2.7 %collective-permute-start.27 = (bf16[768,256]{1,0:T(8,128)(2,1)S(1)}, bf16[768,256]{1,0:T(8,128)(2,1)S(1)}, u32[]{:S(2)}, u32[]{:S(2)}) collective-permute-start(bf16[768,256]{1,0:T(8,128)(2,1)S(1)} %fusion.7.refs_0_), channel_id=1, source_target_pairs={{0,4},{1,5},{2,6},{3,7},{4,0},{5,1},{6,2},{7,3},{8,12},{9,13},{10,... | collective-permute-start | bytes 1179656 | tf_op jit(solution)/shard_map/ppermute | solution.py:21
  133.8 6.2 %collective-permute-done.25.refs_2_ = bf16[768,256]{1,0:T(8,128)(2,1)S(1)} collective-permute-done((bf16[768,256]{1,0:T(8,128)(2,1)S(1)}, bf16[768,256]{1,0:T(8,128)(2,1)S(1)}, u32[]{:S(2)}, u32[]{:S(2)}) %collective-permute-start.25) | collective-permute-done | bytes 393248 | tf_op jit(solution)/shard_map/ppermute | solution.py:21
  141.5 8.3 %collective-permute-done.27.refs_4_ = bf16[768,256]{1,0:T(8,128)(2,1)S(1)} collective-permute-done((bf16[768,256]{1,0:T(8,128)(2,1)S(1)}, bf16[768,256]{1,0:T(8,128)(2,1)S(1)}, u32[]{:S(2)}, u32[]{:S(2)}) %collective-permute-start.27) | collective-permute-done | bytes 393248 | tf_op jit(solution)/shard_map/ppermute | solution.py:21
  153.0 12.9 %channel.1 = (bf16[4,768,256]{2,1,0:T(8,128)(2,1)S(1)}, bf16[4,768,256]{2,1,0:T(8,128)(2,1)S(1)}) custom-call(bf16[768,256]{1,0:T(8,128)(2,1)S(1)} %fusion.7.refs_0_, bf16[768,256]{1,0:T(8,128)(2,1)S(1)} %collective-permute-done.24.refs_1_, bf16[768,256]{1,0:T(8,128)(2,1)S(1)} %collective-permute-done.25.refs_2_, ...), custom_call_target="tpu_custom_call" | custom-call | flops 6643777536 | bytes 1048576 | tf_op jit(solution)/shard_map/channel/pallas_call | solution.py:302
  166.3 3.1 %collective-permute-done.31 = bf16[4,768,256]{2,1,0:T(8,128)(2,1)S(1)} collective-permute-done((bf16[4,768,256]{2,1,0:T(8,128)(2,1)S(1)}, bf16[4,768,256]{2,1,0:T(8,128)(2,1)S(1)}, u32[]{:S(2)}, u32[]{:S(2)}) %collective-permute-start.31) | collective-permute-done | bytes 1572896 | tf_op jit(solution)/shard_map/ppermute | solution.py:16
  169.9 2.6 %collective-permute-start.33 = (bf16[768,256]{1,0:T(8,128)(2,1)S(1)}, bf16[768,256]{1,0:T(8,128)(2,1)S(1)}, u32[]{:S(2)}, u32[]{:S(2)}) collective-permute-start(bf16[768,256]{1,0:T(8,128)(2,1)S(1)} %get-tuple-element.55), channel_id=1, source_target_pairs={{0,4},{1,5},{2,6},{3,7},{4,0},{5,1},{6,2},{7,3},{8,12},{9,13},{10,... | collective-permute-start | bytes 1179656 | tf_op jit(solution)/shard_map/ppermute | solution.py:21
  172.5 9.0 %collective-permute-done.32 = bf16[768,256]{1,0:T(8,128)(2,1)S(1)} collective-permute-done((bf16[768,256]{1,0:T(8,128)(2,1)S(1)}, bf16[768,256]{1,0:T(8,128)(2,1)S(1)}, u32[]{:S(2)}, u32[]{:S(2)}) %collective-permute-start.32) | collective-permute-done | bytes 393248 | tf_op jit(solution)/shard_map/ppermute | solution.py:21
  181.5 8.2 %collective-permute-done.33 = bf16[768,256]{1,0:T(8,128)(2,1)S(1)} collective-permute-done((bf16[768,256]{1,0:T(8,128)(2,1)S(1)}, bf16[768,256]{1,0:T(8,128)(2,1)S(1)}, u32[]{:S(2)}, u32[]{:S(2)}) %collective-permute-start.33) | collective-permute-done | bytes 393248 | tf_op jit(solution)/shard_map/ppermute | solution.py:21
  (62 shorter events, 16.1 us)
Async XLA Ops:
  6.5 146.4 %all-gather.3.cloned.1.call-start = ((), (), s32[]{:S(2)}) async-start(), calls=%async_computation | async-start | bytes 9191424 | tf_op jit(solution)/shard_map/all_gather | solution.py:385
  9.0 25.8 %collective-permute-start = (bf16[128,384]{1,0:T(8,128)(2,1)}, bf16[128,384]{1,0:T(8,128)(2,1)S(1)}, u32[]{:S(2)}, u32[]{:S(2)}) collective-permute-start(bf16[128,384]{1,0:T(8,128)(2,1)} %get-tuple-element.30.refs_8_), channel_id=1, source_target_pairs={{0,8},{8,16},{16,24},{24,32},{32,40},{40,48},{48,56},{56,64},{64,7... | collective-permute-start | bytes 294920 | tf_op jit(solution)/shard_map/ppermute | solution.py:64
  12.4 22.4 %collective-permute-start.2 = (bf16[128,384]{1,0:T(8,128)(2,1)}, bf16[128,384]{1,0:T(8,128)(2,1)S(1)}, u32[]{:S(2)}, u32[]{:S(2)}) collective-permute-start(bf16[128,384]{1,0:T(8,128)(2,1)} %get-tuple-element.30.refs_8_), channel_id=1, source_target_pairs={{0,120},{8,0},{16,8},{24,16},{32,24},{40,32},{48,40},{56,48},{64,5... | collective-permute-start | bytes 294920 | tf_op jit(solution)/shard_map/ppermute | solution.py:64
  34.8 4.7 %collective-permute-start.1 = (bf16[128,384]{1,0:T(8,128)(2,1)S(1)}, bf16[128,384]{1,0:T(8,128)(2,1)S(1)}, u32[]{:S(2)}, u32[]{:S(2)}) collective-permute-start(bf16[128,384]{1,0:T(8,128)(2,1)S(1)} %collective-permute-done.refs_9_), channel_id=1, source_target_pairs={{0,8},{8,16},{16,24},{24,32},{32,40},{40,48},{48,56},{56,64},{64,7... | collective-permute-start | bytes 294920 | tf_op jit(solution)/shard_map/ppermute | solution.py:64
  34.8 4.8 %collective-permute-start.3 = (bf16[128,384]{1,0:T(8,128)(2,1)S(1)}, bf16[128,384]{1,0:T(8,128)(2,1)S(1)}, u32[]{:S(2)}, u32[]{:S(2)}) collective-permute-start(bf16[128,384]{1,0:T(8,128)(2,1)S(1)} %collective-permute-done.2.refs_10_), channel_id=1, source_target_pairs={{0,120},{8,0},{16,8},{24,16},{32,24},{40,32},{48,40},{56,48},{64,5... | collective-permute-start | bytes 294920 | tf_op jit(solution)/shard_map/ppermute | solution.py:64
  39.5 9.5 %collective-permute-start.8 = (bf16[128,384]{1,0:T(8,128)(2,1)S(1)}, bf16[128,384]{1,0:T(8,128)(2,1)S(1)}, u32[]{:S(2)}, u32[]{:S(2)}) collective-permute-start(bf16[128,384]{1,0:T(8,128)(2,1)S(1)} %collective-permute-done.1.refs_11_), channel_id=1, source_target_pairs={{0,8},{8,16},{16,24},{24,32},{32,40},{40,48},{48,56},{56,64},{64,7... | collective-permute-start | bytes 294920 | tf_op jit(solution)/shard_map/ppermute | solution.py:64
  39.6 9.4 %collective-permute-start.10 = (bf16[128,384]{1,0:T(8,128)(2,1)S(1)}, bf16[128,384]{1,0:T(8,128)(2,1)S(1)}, u32[]{:S(2)}, u32[]{:S(2)}) collective-permute-start(bf16[128,384]{1,0:T(8,128)(2,1)S(1)} %collective-permute-done.3.refs_12_), channel_id=1, source_target_pairs={{0,120},{8,0},{16,8},{24,16},{32,24},{40,32},{48,40},{56,48},{64,5... | collective-permute-start | bytes 294920 | tf_op jit(solution)/shard_map/ppermute | solution.py:64
  42.7 28.7 %collective-permute-start.5 = (bf16[768,256]{1,0:T(8,128)(2,1)S(1)}, bf16[768,256]{1,0:T(8,128)(2,1)S(1)}, u32[]{:S(2)}, u32[]{:S(2)}) collective-permute-start(bf16[768,256]{1,0:T(8,128)(2,1)S(1)} %copy-done), channel_id=1, source_target_pairs={{0,2},{1,3},{2,4},{3,5},{4,6},{5,7},{6,0},{7,1},{8,10},{9,11},{10,... | collective-permute-start | bytes 1179656 | tf_op jit(solution)/shard_map/ppermute | solution.py:21
  44.9 26.5 %collective-permute-start.6 = (bf16[768,256]{1,0:T(8,128)(2,1)S(1)}, bf16[768,256]{1,0:T(8,128)(2,1)S(1)}, u32[]{:S(2)}, u32[]{:S(2)}) collective-permute-start(bf16[768,256]{1,0:T(8,128)(2,1)S(1)} %copy-done), channel_id=1, source_target_pairs={{0,4},{1,5},{2,6},{3,7},{4,0},{5,1},{6,2},{7,3},{8,12},{9,13},{10,... | collective-permute-start | bytes 1179656 | tf_op jit(solution)/shard_map/ppermute | solution.py:21
  48.4 23.0 %collective-permute-start.7 = (bf16[768,256]{1,0:T(8,128)(2,1)S(1)}, bf16[768,256]{1,0:T(8,128)(2,1)S(1)}, u32[]{:S(2)}, u32[]{:S(2)}) collective-permute-start(bf16[768,256]{1,0:T(8,128)(2,1)S(1)} %copy-done), channel_id=1, source_target_pairs={{0,6},{1,7},{2,0},{3,1},{4,2},{5,3},{6,4},{7,5},{8,14},{9,15},{10,... | collective-permute-start | bytes 1179656 | tf_op jit(solution)/shard_map/ppermute | solution.py:21
  49.0 7.3 %collective-permute-start.9 = (bf16[128,384]{1,0:T(8,128)(2,1)S(1)}, bf16[128,384]{1,0:T(8,128)(2,1)S(1)}, u32[]{:S(2)}, u32[]{:S(2)}) collective-permute-start(bf16[128,384]{1,0:T(8,128)(2,1)S(1)} %collective-permute-done.8.refs_13_), channel_id=1, source_target_pairs={{0,8},{8,16},{16,24},{24,32},{32,40},{40,48},{48,56},{56,64},{64,7... | collective-permute-start | bytes 294920 | tf_op jit(solution)/shard_map/ppermute | solution.py:64
  49.0 7.3 %collective-permute-start.12 = (bf16[128,384]{1,0:T(8,128)(2,1)S(1)}, bf16[128,384]{1,0:T(8,128)(2,1)S(1)}, u32[]{:S(2)}, u32[]{:S(2)}) collective-permute-start(bf16[128,384]{1,0:T(8,128)(2,1)S(1)} %collective-permute-done.10.refs_14_), channel_id=1, source_target_pairs={{0,120},{8,0},{16,8},{24,16},{32,24},{40,32},{48,40},{56,48},{64,5... | collective-permute-start | bytes 294920 | tf_op jit(solution)/shard_map/ppermute | solution.py:64
  56.3 7.4 %collective-permute-start.11 = (bf16[128,384]{1,0:T(8,128)(2,1)S(1)}, bf16[128,384]{1,0:T(8,128)(2,1)S(1)}, u32[]{:S(2)}, u32[]{:S(2)}) collective-permute-start(bf16[128,384]{1,0:T(8,128)(2,1)S(1)} %collective-permute-done.9.refs_15_), channel_id=1, source_target_pairs={{0,8},{8,16},{16,24},{24,32},{32,40},{40,48},{48,56},{56,64},{64,7... | collective-permute-start | bytes 294920 | tf_op jit(solution)/shard_map/ppermute | solution.py:64
  56.3 7.4 %collective-permute-start.14 = (bf16[128,384]{1,0:T(8,128)(2,1)S(1)}, bf16[128,384]{1,0:T(8,128)(2,1)S(1)}, u32[]{:S(2)}, u32[]{:S(2)}) collective-permute-start(bf16[128,384]{1,0:T(8,128)(2,1)S(1)} %collective-permute-done.12.refs_16_), channel_id=1, source_target_pairs={{0,120},{8,0},{16,8},{24,16},{32,24},{40,32},{48,40},{56,48},{64,5... | collective-permute-start | bytes 294920 | tf_op jit(solution)/shard_map/ppermute | solution.py:64
  63.7 7.7 %collective-permute-start.13 = (bf16[128,384]{1,0:T(8,128)(2,1)S(1)}, bf16[128,384]{1,0:T(8,128)(2,1)S(1)}, u32[]{:S(2)}, u32[]{:S(2)}) collective-permute-start(bf16[128,384]{1,0:T(8,128)(2,1)S(1)} %collective-permute-done.11.refs_17_), channel_id=1, source_target_pairs={{0,8},{8,16},{16,24},{24,32},{32,40},{40,48},{48,56},{56,64},{64,7... | collective-permute-start | bytes 294920 | tf_op jit(solution)/shard_map/ppermute | solution.py:64
  63.7 7.7 %collective-permute-start.15 = (bf16[128,384]{1,0:T(8,128)(2,1)S(1)}, bf16[128,384]{1,0:T(8,128)(2,1)S(1)}, u32[]{:S(2)}, u32[]{:S(2)}) collective-permute-start(bf16[128,384]{1,0:T(8,128)(2,1)S(1)} %collective-permute-done.14.refs_18_), channel_id=1, source_target_pairs={{0,120},{8,0},{16,8},{24,16},{32,24},{40,32},{48,40},{56,48},{64,5... | collective-permute-start | bytes 294920 | tf_op jit(solution)/shard_map/ppermute | solution.py:64
  71.6 15.6 %collective-permute-start.16 = (bf16[3,768,256]{2,1,0:T(8,128)(2,1)S(1)}, bf16[3,768,256]{2,1,0:T(8,128)(2,1)S(1)}, u32[]{:S(2)}, u32[]{:S(2)}) collective-permute-start(bf16[3,768,256]{2,1,0:T(8,128)(2,1)S(1)} %pad_maximum_fusion), channel_id=1, source_target_pairs={{0,1},{1,0},{2,3},{3,2},{4,5},{5,4},{6,7},{7,6},{8,9},{9,8},{10,11... | collective-permute-start | bytes 3538952 | tf_op jit(solution)/shard_map/ppermute | solution.py:16
  78.4 8.9 %collective-permute-start.4 = (bf16[768,256]{1,0:T(8,128)(2,1)S(1)}, bf16[768,256]{1,0:T(8,128)(2,1)S(1)}, u32[]{:S(2)}, u32[]{:S(2)}) collective-permute-start(bf16[768,256]{1,0:T(8,128)(2,1)S(1)} %copy-done), channel_id=1, source_target_pairs={{0,1},{1,0},{2,3},{3,2},{4,5},{5,4},{6,7},{7,6},{8,9},{9,8},{10,11... | collective-permute-start | bytes 1179656 | tf_op jit(solution)/shard_map/ppermute | solution.py:16
  78.6 8.7 %collective-permute-start.17 = (bf16[128,384]{1,0:T(8,128)(2,1)S(1)}, bf16[128,384]{1,0:T(8,128)(2,1)S(1)}, u32[]{:S(2)}, u32[]{:S(2)}) collective-permute-start(bf16[128,384]{1,0:T(8,128)(2,1)S(1)} %collective-permute-done.13.refs_19_), channel_id=1, source_target_pairs={{0,8},{8,16},{16,24},{24,32},{32,40},{40,48},{48,56},{56,64},{64,7... | collective-permute-start | bytes 294920 | tf_op jit(solution)/shard_map/ppermute | solution.py:64
  78.6 8.8 %collective-permute-start.18 = (bf16[128,384]{1,0:T(8,128)(2,1)S(1)}, bf16[128,384]{1,0:T(8,128)(2,1)S(1)}, u32[]{:S(2)}, u32[]{:S(2)}) collective-permute-start(bf16[128,384]{1,0:T(8,128)(2,1)S(1)} %collective-permute-done.15.refs_20_), channel_id=1, source_target_pairs={{0,120},{8,0},{16,8},{24,16},{32,24},{40,32},{48,40},{56,48},{64,5... | collective-permute-start | bytes 294920 | tf_op jit(solution)/shard_map/ppermute | solution.py:64
  87.2 8.0 %collective-permute-start.19 = (bf16[128,384]{1,0:T(8,128)(2,1)S(1)}, bf16[128,384]{1,0:T(8,128)(2,1)S(1)}, u32[]{:S(2)}, u32[]{:S(2)}) collective-permute-start(bf16[128,384]{1,0:T(8,128)(2,1)S(1)} %collective-permute-done.17.refs_21_), channel_id=1, source_target_pairs={{0,8},{8,16},{16,24},{24,32},{32,40},{40,48},{48,56},{56,64},{64,7... | collective-permute-start | bytes 294920 | tf_op jit(solution)/shard_map/ppermute | solution.py:64
  107.1 12.1 %collective-permute-start.21 = (bf16[768,256]{1,0:T(8,128)(2,1)S(1)}, bf16[768,256]{1,0:T(8,128)(2,1)S(1)}, u32[]{:S(2)}, u32[]{:S(2)}) collective-permute-start(bf16[768,256]{1,0:T(8,128)(2,1)S(1)} %get-tuple-element.56), channel_id=1, source_target_pairs={{0,2},{1,3},{2,4},{3,5},{4,6},{5,7},{6,0},{7,1},{8,10},{9,11},{10,... | collective-permute-start | bytes 1179656 | tf_op jit(solution)/shard_map/ppermute | solution.py:21
  107.6 19.2 %collective-permute-start.22 = (bf16[768,256]{1,0:T(8,128)(2,1)S(1)}, bf16[768,256]{1,0:T(8,128)(2,1)S(1)}, u32[]{:S(2)}, u32[]{:S(2)}) collective-permute-start(bf16[768,256]{1,0:T(8,128)(2,1)S(1)} %get-tuple-element.58), channel_id=1, source_target_pairs={{0,4},{1,5},{2,6},{3,7},{4,0},{5,1},{6,2},{7,3},{8,12},{9,13},{10,... | collective-permute-start | bytes 1179656 | tf_op jit(solution)/shard_map/ppermute | solution.py:21
  109.5 18.1 %collective-permute-start.23 = (bf16[768,256]{1,0:T(8,128)(2,1)S(1)}, bf16[768,256]{1,0:T(8,128)(2,1)S(1)}, u32[]{:S(2)}, u32[]{:S(2)}) collective-permute-start(bf16[768,256]{1,0:T(8,128)(2,1)S(1)} %get-tuple-element.57), channel_id=1, source_target_pairs={{0,6},{1,7},{2,0},{3,1},{4,2},{5,3},{6,4},{7,5},{8,14},{9,15},{10,... | collective-permute-start | bytes 1179656 | tf_op jit(solution)/shard_map/ppermute | solution.py:21
  127.9 12.1 %collective-permute-start.25 = (bf16[768,256]{1,0:T(8,128)(2,1)S(1)}, bf16[768,256]{1,0:T(8,128)(2,1)S(1)}, u32[]{:S(2)}, u32[]{:S(2)}) collective-permute-start(bf16[768,256]{1,0:T(8,128)(2,1)S(1)} %fusion.7.refs_0_), channel_id=1, source_target_pairs={{0,2},{1,3},{2,4},{3,5},{4,6},{5,7},{6,0},{7,1},{8,10},{9,11},{10,... | collective-permute-start | bytes 1179656 | tf_op jit(solution)/shard_map/ppermute | solution.py:21
  129.9 19.9 %collective-permute-start.27 = (bf16[768,256]{1,0:T(8,128)(2,1)S(1)}, bf16[768,256]{1,0:T(8,128)(2,1)S(1)}, u32[]{:S(2)}, u32[]{:S(2)}) collective-permute-start(bf16[768,256]{1,0:T(8,128)(2,1)S(1)} %fusion.7.refs_0_), channel_id=1, source_target_pairs={{0,4},{1,5},{2,6},{3,7},{4,0},{5,1},{6,2},{7,3},{8,12},{9,13},{10,... | collective-permute-start | bytes 1179656 | tf_op jit(solution)/shard_map/ppermute | solution.py:21
  132.6 18.5 %collective-permute-start.29 = (bf16[768,256]{1,0:T(8,128)(2,1)S(1)}, bf16[768,256]{1,0:T(8,128)(2,1)S(1)}, u32[]{:S(2)}, u32[]{:S(2)}) collective-permute-start(bf16[768,256]{1,0:T(8,128)(2,1)S(1)} %fusion.7.refs_0_), channel_id=1, source_target_pairs={{0,6},{1,7},{2,0},{3,1},{4,2},{5,3},{6,4},{7,5},{8,14},{9,15},{10,... | collective-permute-start | bytes 1179656 | tf_op jit(solution)/shard_map/ppermute | solution.py:21
  132.6 18.5 %collective-permute-start.24 = (bf16[768,256]{1,0:T(8,128)(2,1)S(1)}, bf16[768,256]{1,0:T(8,128)(2,1)S(1)}, u32[]{:S(2)}, u32[]{:S(2)}) collective-permute-start(bf16[768,256]{1,0:T(8,128)(2,1)S(1)} %fusion.7.refs_0_), channel_id=1, source_target_pairs={{0,1},{1,0},{2,3},{3,2},{4,5},{5,4},{6,7},{7,6},{8,9},{9,8},{10,11... | collective-permute-start | bytes 1179656 | tf_op jit(solution)/shard_map/ppermute | solution.py:16
  140.0 11.1 %collective-permute-start.26 = (bf16[768,256]{1,0:T(8,128)(2,1)S(1)}, bf16[768,256]{1,0:T(8,128)(2,1)S(1)}, u32[]{:S(2)}, u32[]{:S(2)}) collective-permute-start(bf16[768,256]{1,0:T(8,128)(2,1)S(1)} %collective-permute-done.25.refs_2_), channel_id=1, source_target_pairs={{0,1},{1,0},{2,3},{3,2},{4,5},{5,4},{6,7},{7,6},{8,9},{9,8},{10,11... | collective-permute-start | bytes 1179656 | tf_op jit(solution)/shard_map/ppermute | solution.py:16
  169.7 11.7 %collective-permute-start.32 = (bf16[768,256]{1,0:T(8,128)(2,1)S(1)}, bf16[768,256]{1,0:T(8,128)(2,1)S(1)}, u32[]{:S(2)}, u32[]{:S(2)}) collective-permute-start(bf16[768,256]{1,0:T(8,128)(2,1)S(1)} %get-tuple-element.53), channel_id=1, source_target_pairs={{0,2},{1,3},{2,4},{3,5},{4,6},{5,7},{6,0},{7,1},{8,10},{9,11},{10,... | collective-permute-start | bytes 1179656 | tf_op jit(solution)/shard_map/ppermute | solution.py:21
  169.9 19.9 %collective-permute-start.33 = (bf16[768,256]{1,0:T(8,128)(2,1)S(1)}, bf16[768,256]{1,0:T(8,128)(2,1)S(1)}, u32[]{:S(2)}, u32[]{:S(2)}) collective-permute-start(bf16[768,256]{1,0:T(8,128)(2,1)S(1)} %get-tuple-element.55), channel_id=1, source_target_pairs={{0,4},{1,5},{2,6},{3,7},{4,0},{5,1},{6,2},{7,3},{8,12},{9,13},{10,... | collective-permute-start | bytes 1179656 | tf_op jit(solution)/shard_map/ppermute | solution.py:21
  172.4 17.8 %collective-permute-start.34 = (bf16[768,256]{1,0:T(8,128)(2,1)S(1)}, bf16[768,256]{1,0:T(8,128)(2,1)S(1)}, u32[]{:S(2)}, u32[]{:S(2)}) collective-permute-start(bf16[768,256]{1,0:T(8,128)(2,1)S(1)} %get-tuple-element.54), channel_id=1, source_target_pairs={{0,6},{1,7},{2,0},{3,1},{4,2},{5,3},{6,4},{7,5},{8,14},{9,15},{10,... | collective-permute-start | bytes 1179656 | tf_op jit(solution)/shard_map/ppermute | solution.py:21
  (10 other events, 211.6 us)
Sparse Core Ops, SparseCore 0:
  9.1 133.6 all-gather.2
